TPU v7x, 128 devices: a whole 4x4x4 slice. The times are simulated.
128 devices in a mesh: sp: 16 (over z, y), tp: 8 (over x, core).
Axes of the slice: x: 4, y: 4, z: 4, core: 2. Of those that a mesh axis runs over, the one named last changes fastest.
Arguments:
- tokens: bfloat16 [4096, 4096], P('sp'), may hold values from -64 to 64
- norm_gain: float32 [4096], replicated, may hold values from 0.1 to 1.9
- w_query: bfloat16 [4096, 2048], P('sp', 'tp'), may hold values from -1.09375 to 1.09375
- w_key: bfloat16 [4096, 512], P('sp', 'tp'), may hold values from -0.09375 to 0.09375
- w_value: bfloat16 [4096, 512], P('sp', 'tp'), may hold values from -0.09375 to 0.09375
- w_glu: bfloat16 [4096, 2048], P('sp', 'tp'), may hold values from -0.09375 to 0.09375
- w_gate: bfloat16 [4096, 2048], P('sp', 'tp'), may hold values from -0.09375 to 0.09375
- sink_logit: float32 [32], P('tp'), may hold values from 2 to 6
- conv_taps: bfloat16 [31, 2048], P(None, 'tp'), may hold values from -12.9315817 to 12.9315817
- conv_gain: float32 [2048], P('tp'), may hold values from 0.1 to 1.9
- out_attn: bfloat16 [2048, 4096], P('sp', 'tp'), may hold values from -0.5 to 0.5
- out_conv: bfloat16 [2048, 4096], P('sp', 'tp'), may hold values from -0.125 to 0.125
Outputs:
- mixed: bfloat16 [4096, 4096], P('sp', 'tp')
All inputs are finite; a program needn't handle non-finite values.
Results may differ from a plain program's by a relative error of at most 0.008.
The roundings to bfloat16 on the way count: a program that leaves them out, or rounds other values in their place, can miss the bound.
Values may be sent and summed in bfloat16 or wider, within the bound.
A program may use at most 64 MiB of HBM per device.

v0:
```python
import math

import jax
import jax.numpy as jnp
from jax import lax
from jax.sharding import PartitionSpec as P

HEADS = 32
HEAD = 64
KV = 8
CONV = 2048
KSIZE = 31
WINDOW = 128


def in_one_piece(arrays, axis, dim, along):
    widths = [a.shape[along] for a in arrays]
    both = jnp.concatenate(arrays, axis=along)
    result = lax.all_gather(both, axis, axis=dim, tiled=True)
    return tuple(jnp.split(result, [sum(widths[:k]) for k in range(1, len(widths))], axis=along))


def passed_along(block, axis, distance):
    devices = range(lax.axis_size(axis))
    route = [(i - distance, i) for i in devices if i - distance in devices]
    return lax.ppermute(block, axis, route)


def from_everyone(array, axis):
    devices = lax.axis_size(axis)
    return lax.all_to_all(
        jnp.broadcast_to(array[None], (devices, *array.shape)), axis, 0, 0, tiled=True
    )


def over_copies(array, axis):
    everything = from_everyone(array, axis)
    return jnp.sum(everything, axis=0)


def laid_out(parts, dim):
    parts = jnp.moveaxis(parts, 0, dim)
    shape = parts.shape
    return parts.reshape(*shape[:dim], shape[dim] * shape[dim + 1], *shape[dim + 2 :])


def gather_directly(array, axis, dim):
    parts = from_everyone(array, axis)
    return laid_out(parts, dim)


def rotate_heads(values, positions):
    half_width = values.shape[-1] // 2
    frequency = 10000.0 ** (-jnp.arange(half_width, dtype=jnp.float32) * 2.0 / values.shape[-1])
    angles = positions.astype(jnp.float32)[:, None] * frequency[None, :]
    cosine = jnp.cos(angles)[:, None, :]
    sine_part = jnp.sin(angles)[:, None, :]
    first_half = values[..., :half_width]
    second_half = values[..., half_width:]
    return jnp.concatenate(
        [
            first_half * cosine - second_half * sine_part,
            second_half * cosine + first_half * sine_part,
        ],
        axis=-1,
    )


def per_device(
    tokens,
    norm_gain,
    w_query,
    w_key,
    w_value,
    w_glu,
    w_gate,
    sink_logit,
    conv_taps,
    conv_gain,
    out_attn,
    out_conv,
):
    row_count = tokens.shape[0]
    offset_rows = lax.axis_index("sp") * row_count
    positions = offset_rows + jnp.arange(row_count, dtype=jnp.int32)
    tokens_f = tokens.astype(jnp.float32)
    normed = (
        tokens_f
        * lax.rsqrt(jnp.mean(tokens_f * tokens_f, axis=1, keepdims=True) + 1e-06)
        * norm_gain
    ).astype(jnp.bfloat16)
    local_heads = w_query.shape[1] // HEAD
    local_kv = w_key.shape[1] // HEAD
    group_size = HEADS // KV
    kv_width = local_kv * HEAD
    pieces = in_one_piece((w_query, w_key, w_value, w_glu, w_gate), "sp", 0, 1)
    query_acc, key_acc, value_acc, glu_acc, gate_acc = tuple(
        (
            jnp.dot(normed, weight_piece, preferred_element_type=jnp.float32)
            for weight_piece in pieces
        )
    )
    queries = rotate_heads(query_acc.reshape(row_count, local_heads, HEAD), positions).astype(
        jnp.bfloat16
    )
    keys_rot = rotate_heads(key_acc.reshape(row_count, local_kv, HEAD), positions).astype(
        jnp.bfloat16
    )
    keys_rot = keys_rot.reshape(row_count, kv_width)
    values_bf = value_acc.astype(jnp.bfloat16)
    kv_tail = jnp.concatenate(
        [keys_rot[row_count - WINDOW :], values_bf[row_count - WINDOW :]], axis=1
    )
    kv_rim = passed_along(kv_tail, "sp", 1)
    gated = (glu_acc * jax.nn.sigmoid(gate_acc)).astype(jnp.bfloat16)
    conv_tail = gated[row_count - (KSIZE - 1) :]
    conv_rim = passed_along(conv_tail, "sp", 1)
    block_count = row_count // WINDOW
    keys_all = jnp.concatenate([kv_rim[:, :kv_width], keys_rot], axis=0).reshape(
        block_count + 1, WINDOW, local_kv, HEAD
    )
    vals_all = jnp.concatenate([kv_rim[:, kv_width:], values_bf], axis=0).reshape(
        block_count + 1, WINDOW, local_kv, HEAD
    )
    key_blocks = jnp.concatenate([keys_all[:-1], keys_all[1:]], axis=1)
    value_blocks = jnp.concatenate([vals_all[:-1], vals_all[1:]], axis=1)
    query_block_rows = queries.reshape(block_count, WINDOW, local_kv, group_size, HEAD)
    score_matrix = jnp.einsum(
        "bqhgd,bkhd->bhgqk", query_block_rows, key_blocks, preferred_element_type=jnp.float32
    ) * (1.0 / math.sqrt(HEAD))
    block_ids = jnp.arange(block_count, dtype=jnp.int32)[:, None, None]
    query_pos = (
        offset_rows + block_ids * WINDOW + jnp.arange(WINDOW, dtype=jnp.int32)[None, :, None]
    )
    key_pos = (
        offset_rows
        + (block_ids - 1) * WINDOW
        + jnp.arange(2 * WINDOW, dtype=jnp.int32)[None, None, :]
    )
    distance = query_pos - key_pos
    allowed = (distance >= 0) & (distance < WINDOW) & (key_pos >= 0)
    score_matrix = jnp.where(allowed[:, None, None], score_matrix, -1e30)
    sink_local = sink_logit.reshape(local_kv, group_size)[None, :, :, None, None]
    highest = jnp.maximum(jnp.max(score_matrix, axis=-1, keepdims=True), sink_local)
    weights_exp = jnp.exp(score_matrix - highest)
    denom_total = jnp.sum(weights_exp, axis=-1, keepdims=True) + jnp.exp(sink_local - highest)
    weights_bfloat_half = (weights_exp / denom_total).astype(jnp.bfloat16)
    attended_values = jnp.einsum(
        "bhgqk,bkhd->bqhgd", weights_bfloat_half, value_blocks, preferred_element_type=jnp.float32
    ).astype(jnp.bfloat16)
    attended_values = attended_values.reshape(row_count, local_heads * HEAD)
    extended = jnp.concatenate([conv_rim, gated], axis=0).astype(jnp.float32)
    filtered = lax.conv_general_dilated(
        extended[None],
        conv_taps.astype(jnp.float32)[:, None, :],
        (1,),
        "VALID",
        dimension_numbers=("NWC", "WIO", "NWC"),
        feature_group_count=extended.shape[1],
        precision=lax.Precision.HIGHEST,
    )[0]
    channel_sum, channel_square = (
        over_copies(jnp.sum(filtered, axis=1), "tp"),
        over_copies(jnp.sum(filtered * filtered, axis=1), "tp"),
    )
    mean_value = channel_sum / CONV
    variance = channel_square / CONV - mean_value * mean_value
    scaled = (filtered - mean_value[:, None]) * lax.rsqrt(variance + 1e-05)[:, None] * conv_gain
    conv_out = jax.nn.silu(scaled).astype(jnp.bfloat16)
    attn_rows, conv_rows = in_one_piece((out_attn, out_conv), "sp", 0, 1)
    pieces = (gather_directly(attended_values, "tp", 1), gather_directly(conv_out, "tp", 1))
    mixed = jnp.dot(pieces[0], attn_rows, preferred_element_type=jnp.float32) + jnp.dot(
        pieces[1], conv_rows, preferred_element_type=jnp.float32
    )
    return mixed.astype(jnp.bfloat16)


def solution(mesh):
    return jax.shard_map(
        per_device,
        mesh=mesh,
        in_specs=(
            P("sp", None),
            P(),
            P("sp", "tp"),
            P("sp", "tp"),
            P("sp", "tp"),
            P("sp", "tp"),
            P("sp", "tp"),
            P("tp"),
            P(None, "tp"),
            P("tp"),
            P("sp", "tp"),
            P("sp", "tp"),
        ),
        out_specs=P("sp", "tp"),
        check_vma=False,
    )
```

profile of v0, /device:TPU:1, one launch (start us, length us, event | category | flops | bytes accessed | tf_op | source)
XLA Modules:
  0.0 166.3 jit_solution(16678493036971346051)
XLA Ops:
  6.5 0.0 copy-start
  6.5 0.0 copy-start.1
  6.5 0.0 all-gather.3.cloned.1.call-start
  6.5 1.0 copy.58
  7.6 0.9 copy.59
  8.5 1.9 %concatenate.66 = bf16[256,896]{1,0:T(8,128)(2,1)} concatenate(bf16[256,256]{1,0:T(8,128)(2,1)} %param.14, bf16[256,64]{1,0:T(8,128)(2,1)S(1)} %copy.58, bf16[256,64]{1,0:T(8,128)(2,1)S(1)} %copy.59, bf16[256,256]{1,0:T(8,128)(2,1)} %param.17, bf16[256,256]{1,0:T(8,128)(2,1)} %param.18), dimensions={1} | concatenate | bytes 917504 | tf_op jit(solution)/shard_map/concatenate | solution.py:18
  10.4 0.0 all-gather.3.cloned.1.call-update
  10.4 0.0 all-gather.5.cloned.1.call-start
  10.4 1.7 %pad_maximum_fusion = bf16[128,1024]{1,0:T(8,128)(2,1)} fusion(bf16[128,512]{1,0:T(8,128)(2,1)} %param.23, bf16[128,512]{1,0:T(8,128)(2,1)} %param.22), kind=kLoop, calls=%fused_computation.47 | loop fusion | flops 524288 | bytes 524288 | tf_op jit(solution)/shard_map/concatenate | solution.py:18
  12.1 0.0 all-gather.5.cloned.1.call-update
  12.2 0.1 broadcast_compare_fusion
  12.3 0.1 iota_add_fusion.1
  12.4 2.1 %fusion = f32[256]{0:T(256)S(1)} fusion(bf16[256,4096]{1,0:T(8,128)(2,1)} %param.12), kind=kLoop, calls=%fused_computation.2 | loop fusion | flops 3145472 | bytes 2098176 | tf_op jit(solution)/shard_map/reduce_sum | solution.py:89
  14.5 0.1 iota_add_fusion
  14.5 0.2 multiply_cosine_fusion
  14.7 0.2 fusion.52
  14.9 64.9 %all-gather.3.cloned.1.call-done = bf16[4096,896]{1,0:T(8,128)(2,1)} async-done(((bf16[256,896]{1,0:T(8,128)(2,1)}), bf16[4096,896]{1,0:T(8,128)(2,1)}) %all-gather.3.cloned.1.call-update) | async-done | bytes 7340048 | tf_op jit(solution)/shard_map/all_gather | solution.py:19
  79.8 0.0 copy-done.1
  79.8 0.0 copy-done.5
  79.8 2.8 %convolution_convert_fusion.1 = bf16[256,64]{0,1:T(8,128)(2,1)S(1)} fusion(bf16[4096,896]{1,0:T(8,128)(2,1)} %all-gather.3.cloned.1.call-done, bf16[256,4096]{1,0:T(8,128)(2,1)S(1)} %copy-done.1, f32[4096]{0:T(1024)S(1)} %copy-done.5, f32[256]{0:T(256)S(1)} %add_rsqrt_fusion.1), kind=kOutput, calls=%fused_computation.30 | convolution fusion | flops 138428416 | bytes 3195904 | tf_op jit(solution)/shard_map/dot_general | solution.py:99
  82.6 2.1 %convolution_bitcast_fusion = f32[256,1,64]{0,2,1:T(8,128)S(1)} fusion(bf16[4096,896]{1,0:T(8,128)(2,1)} %all-gather.3.cloned.1.call-done, bf16[256,4096]{1,0:T(8,128)(2,1)S(1)} %copy-done.1, f32[4096]{0:T(1024)S(1)} %copy-done.5, f32[256]{0:T(256)S(1)} %add_rsqrt_fusion.1), kind=kOutput, calls=%fused_computation.29 | convolution fusion | flops 138412032 | bytes 3228672 | tf_op jit(solution)/shard_map/dot_general | solution.py:99
  84.7 0.2 fusion.71
  85.0 3.1 %collective-permute-start = (bf16[128,128]{0,1:T(8,128)(2,1)S(1)}, bf16[128,128]{0,1:T(8,128)(2,1)S(1)}, u32[]{:S(2)}, u32[]{:S(2)}) collective-permute-start(bf16[128,128]{0,1:T(8,128)(2,1)S(1)} %pad_maximum_fusion.4), channel_id=1, source_target_pairs={{0,8},{8,16},{16,24},{24,32},{32,40},{40,48},{48,56},{56,64},{64,7... | collective-permute-start | bytes 98312 | tf_op jit(solution)/shard_map/ppermute | solution.py:26
  88.1 0.0 copy-done.4
  88.1 0.8 fusion.33
  88.9 0.8 fusion.36
  89.7 0.0 copy-start.6
  89.8 3.1 %collective-permute-start.1 = (bf16[30,256]{1,0:T(8,128)(2,1)S(1)}, bf16[30,256]{1,0:T(8,128)(2,1)S(1)}, u32[]{:S(2)}, u32[]{:S(2)}) collective-permute-start(bf16[30,256]{1,0:T(8,128)(2,1)S(1)} %slice.73), channel_id=1, source_target_pairs={{0,8},{8,16},{16,24},{24,32},{32,40},{40,48},{48,56},{56,64},{64,7... | collective-permute-start | bytes 46088 | tf_op jit(solution)/shard_map/ppermute | solution.py:26
  92.9 1.2 fusion.11
  94.1 0.0 collective-permute-done.1
  94.3 0.0 copy-done
  94.3 0.0 copy-done.6
  94.3 0.0 copy-start.3
  94.4 0.7 fusion.87
  95.0 0.1 copy.72
  95.1 0.0 copy-start.2
  95.2 0.1 slice_reduce_fusion.1
  95.3 0.6 broadcast_in_dim.34
  95.9 5.8 %all-to-all-start.1 = ((f32[8,1,256]{2,1,0:T(1,128)}), f32[8,1,256]{2,1,0:T(1,128)S(1)}, u32[]{:S(2)}, u32[]{:S(2)}) async-start(f32[8,1,256]{2,1,0:T(1,128)} %broadcast_in_dim.34), calls=%async_computation.1 | async-start | bytes 16384 | tf_op jit(solution)/shard_map/all_to_all | solution.py:31
  101.7 0.1 copy.74
  101.9 0.1 slice_reduce_fusion
  102.0 4.4 %all-to-all-done.1 = f32[8,1,256]{2,1,0:T(1,128)S(1)} async-done(((f32[8,1,256]{2,1,0:T(1,128)}), f32[8,1,256]{2,1,0:T(1,128)S(1)}, u32[]{:S(2)}, u32[]{:S(2)}) %all-to-all-start.1) | async-done | bytes 8224 | tf_op jit(solution)/shard_map/all_to_all | solution.py:31
  106.3 0.6 broadcast_in_dim.35
  106.9 3.9 %all-to-all-start.2 = ((f32[8,1,256]{2,1,0:T(1,128)}), f32[8,1,256]{2,1,0:T(1,128)S(1)}, u32[]{:S(2)}, u32[]{:S(2)}) async-start(f32[8,1,256]{2,1,0:T(1,128)} %broadcast_in_dim.35), calls=%async_computation.2 | async-start | bytes 16384 | tf_op jit(solution)/shard_map/all_to_all | solution.py:31
  110.9 4.6 %all-to-all-done.2 = f32[8,1,256]{2,1,0:T(1,128)S(1)} async-done(((f32[8,1,256]{2,1,0:T(1,128)}), f32[8,1,256]{2,1,0:T(1,128)S(1)}, u32[]{:S(2)}, u32[]{:S(2)}) %all-to-all-start.2) | async-done | bytes 8224 | tf_op jit(solution)/shard_map/all_to_all | solution.py:31
  115.5 0.0 copy-done.3
  115.5 0.2 fusion.57
  115.7 0.1 copy.76
  115.8 1.0 broadcast_in_dim.37
  116.8 4.2 %all-to-all-start.3 = ((bf16[8,256,256]{1,2,0:T(8,128)(2,1)}), bf16[8,256,256]{1,2,0:T(8,128)(2,1)S(1)}, u32[]{:S(2)}, u32[]{:S(2)}) async-start(bf16[8,256,256]{1,2,0:T(8,128)(2,1)} %broadcast_in_dim.37), calls=%async_computation.3 | async-start | bytes 2097152 | tf_op jit(solution)/shard_map/all_to_all | solution.py:31
  121.0 0.0 collective-permute-done
  121.1 0.4 fusion.88
  121.5 0.0 copy-done.2
  121.5 0.1 broadcast_maximum_fusion
  121.6 0.2 fusion.42
  121.7 0.1 exponential_add_fusion
  121.8 0.3 fusion.39
  122.1 0.1 copy.68
  122.3 13.7 %all-to-all-done.3 = bf16[8,256,256]{1,2,0:T(8,128)(2,1)S(1)} async-done(((bf16[8,256,256]{1,2,0:T(8,128)(2,1)}), bf16[8,256,256]{1,2,0:T(8,128)(2,1)S(1)}, u32[]{:S(2)}, u32[]{:S(2)}) %all-to-all-start.3) | async-done | bytes 1048608 | tf_op jit(solution)/shard_map/all_to_all | solution.py:31
  136.0 1.0 broadcast_in_dim.31
  137.0 4.4 %all-to-all-start = ((bf16[8,256,256]{1,2,0:T(8,128)(2,1)}), bf16[8,256,256]{1,2,0:T(8,128)(2,1)S(1)}, u32[]{:S(2)}, u32[]{:S(2)}) async-start(bf16[8,256,256]{1,2,0:T(8,128)(2,1)} %broadcast_in_dim.31), calls=%async_computation | async-start | bytes 2097152 | tf_op jit(solution)/shard_map/all_to_all | solution.py:31
  141.5 2.3 %fusion.3 = f32[256,512]{1,0:T(8,128)S(1)} fusion(bf16[256,2048]{0,1:T(8,128)(2,1)S(1)} %bitcast.85, bf16[2048,1024]{1,0:T(8,128)(2,1)} %all-gather.5.cloned.1.call-done), kind=kOutput, calls=%fused_computation.5 | convolution fusion | flops 536870912 | bytes 3670016 | tf_op jit(solution)/shard_map/dot_general | solution.py:172
  143.8 12.7 %all-to-all-done = bf16[8,256,256]{1,2,0:T(8,128)(2,1)S(1)} async-done(((bf16[8,256,256]{1,2,0:T(8,128)(2,1)}), bf16[8,256,256]{1,2,0:T(8,128)(2,1)S(1)}, u32[]{:S(2)}, u32[]{:S(2)}) %all-to-all-start) | async-done | bytes 1048608 | tf_op jit(solution)/shard_map/all_to_all | solution.py:31
  156.5 3.0 %fusion.18 = bf16[256,512]{1,0:T(8,128)(2,1)} fusion(f32[256,512]{1,0:T(8,128)S(1)} %fusion.3, bf16[256,2048]{0,1:T(8,128)(2,1)S(1)} %bitcast.84, bf16[2048,1024]{1,0:T(8,128)(2,1)} %all-gather.5.cloned.1.call-done), kind=kOutput, calls=%fused_computation.19 | convolution fusion | flops 537133056 | bytes 3932160 | tf_op jit(solution)/shard_map/dot_general | solution.py:172
  (34 shorter events, 0.5 us)
Async XLA Ops:
  6.5 87.8 %copy-start = (bf16[31,256]{1,0:T(8,128)(2,1)S(1)}, bf16[31,256]{1,0:T(8,128)(2,1)}, u32[]{:S(2)}) copy-start(bf16[31,256]{1,0:T(8,128)(2,1)} %param.20) | copy-start | bytes 47620
  6.5 73.3 %copy-start.1 = (bf16[256,4096]{1,0:T(8,128)(2,1)S(1)}, bf16[256,4096]{1,0:T(8,128)(2,1)}, u32[]{:S(2)}) copy-start(bf16[256,4096]{1,0:T(8,128)(2,1)} %param.12) | copy-start | bytes 6291460
  6.5 73.3 %copy-start.5 = (f32[4096]{0:T(1024)S(1)}, f32[4096]{0:T(1024)}, u32[]{:S(2)}) copy-start(f32[4096]{0:T(1024)} %param.13) | copy-start | bytes 49156
  6.5 73.3 %all-gather.3.cloned.1.call-start = ((), (), s32[]{:S(2)}) async-start(), calls=%async_computation.4 | async-start | bytes 7798784 | tf_op jit(solution)/shard_map/all_gather | solution.py:19
  10.4 131.1 %all-gather.5.cloned.1.call-start = ((), (), s32[]{:S(2)}) async-start(), calls=%async_computation.5 | async-start | bytes 4456448 | tf_op jit(solution)/shard_map/all_gather | solution.py:19
  79.8 8.2 %copy-start.4 = (bf16[4096,896]{1,0:T(8,128)(2,1)S(1)}, bf16[4096,896]{1,0:T(8,128)(2,1)}, u32[]{:S(2)}) copy-start(bf16[4096,896]{1,0:T(8,128)(2,1)} %all-gather.3.cloned.1.call-done) | copy-start | bytes 22020100
  85.0 36.0 %collective-permute-start = (bf16[128,128]{0,1:T(8,128)(2,1)S(1)}, bf16[128,128]{0,1:T(8,128)(2,1)S(1)}, u32[]{:S(2)}, u32[]{:S(2)}) collective-permute-start(bf16[128,128]{0,1:T(8,128)(2,1)S(1)} %pad_maximum_fusion.4), channel_id=1, source_target_pairs={{0,8},{8,16},{16,24},{24,32},{32,40},{40,48},{48,56},{56,64},{64,7... | collective-permute-start | bytes 98312 | tf_op jit(solution)/shard_map/ppermute | solution.py:26
  89.7 4.6 %copy-start.6 = (pred[8,36]{0,1:T(8,128)(4,1)S(1)}, pred[8,36]{0,1:T(8,128)(4,1)}, u32[]{:S(2)}) copy-start(pred[8,36]{0,1:T(8,128)(4,1)} %constant.54) | copy-start | bytes 868
  89.8 4.4 %collective-permute-start.1 = (bf16[30,256]{1,0:T(8,128)(2,1)S(1)}, bf16[30,256]{1,0:T(8,128)(2,1)S(1)}, u32[]{:S(2)}, u32[]{:S(2)}) collective-permute-start(bf16[30,256]{1,0:T(8,128)(2,1)S(1)} %slice.73), channel_id=1, source_target_pairs={{0,8},{8,16},{16,24},{24,32},{32,40},{40,48},{48,56},{56,64},{64,7... | collective-permute-start | bytes 46088 | tf_op jit(solution)/shard_map/ppermute | solution.py:26
  94.3 21.1 %copy-start.3 = (f32[256]{0:T(256)S(1)}, f32[256]{0:T(256)}, u32[]{:S(2)}) copy-start(f32[256]{0:T(256)} %param.21) | copy-start | bytes 3076
  95.1 26.3 %copy-start.2 = (f32[4]{0:T(128)S(1)}, f32[4]{0:T(128)}, u32[]{:S(2)}) copy-start(f32[4]{0:T(128)} %param.19) | copy-start | bytes 52
  95.9 10.4 %all-to-all-start.1 = ((f32[8,1,256]{2,1,0:T(1,128)}), f32[8,1,256]{2,1,0:T(1,128)S(1)}, u32[]{:S(2)}, u32[]{:S(2)}) async-start(f32[8,1,256]{2,1,0:T(1,128)} %broadcast_in_dim.34), calls=%async_computation.1 | async-start | bytes 16384 | tf_op jit(solution)/shard_map/all_to_all | solution.py:31
  106.9 8.5 %all-to-all-start.2 = ((f32[8,1,256]{2,1,0:T(1,128)}), f32[8,1,256]{2,1,0:T(1,128)S(1)}, u32[]{:S(2)}, u32[]{:S(2)}) async-start(f32[8,1,256]{2,1,0:T(1,128)} %broadcast_in_dim.35), calls=%async_computation.2 | async-start | bytes 16384 | tf_op jit(solution)/shard_map/all_to_all | solution.py:31
  116.8 19.2 %all-to-all-start.3 = ((bf16[8,256,256]{1,2,0:T(8,128)(2,1)}), bf16[8,256,256]{1,2,0:T(8,128)(2,1)S(1)}, u32[]{:S(2)}, u32[]{:S(2)}) async-start(bf16[8,256,256]{1,2,0:T(8,128)(2,1)} %broadcast_in_dim.37), calls=%async_computation.3 | async-start | bytes 2097152 | tf_op jit(solution)/shard_map/all_to_all | solution.py:31
  137.0 19.4 %all-to-all-start = ((bf16[8,256,256]{1,2,0:T(8,128)(2,1)}), bf16[8,256,256]{1,2,0:T(8,128)(2,1)S(1)}, u32[]{:S(2)}, u32[]{:S(2)}) async-start(bf16[8,256,256]{1,2,0:T(8,128)(2,1)} %broadcast_in_dim.31), calls=%async_computation | async-start | bytes 2097152 | tf_op jit(solution)/shard_map/all_to_all | solution.py:31
Sparse Core Ops, SparseCore 0:
  10.5 69.2 all-gather.2
  82.0 51.2 all-gather.4
where the time goes:
time: 168 us; the launch traced here: 166 us
  waiting for transfers between devices  100 us (60%)
  starting transfers between devices  24.5 us (15%)
  matrix products  14.4 us (9%)
  between operations  13.8 us (8%)
  local copies, waits for them, and re-layouts  7.87 us (5%)
  other arithmetic  5.51 us (3%)
    all_gather x2, waiting for transfers between devices, in_one_piece(): result = lax.all_gather(both, axis, axis=dim, tiled=True)  64.9 us
    all_to_all x4, waiting for transfers between devices, from_everyone(): lax.all_to_all(jnp.broadcast_to(array[None], (devices, *array.shape)), ax...  35.3 us
    all_to_all x4, starting transfers between devices, from_everyone(): lax.all_to_all(jnp.broadcast_to(array[None], (devices, *array.shape)), ax...  18.3 us
    dot_general x5, matrix products, per_device(): jnp.dot(normed, weight_piece, preferred_element_type=jnp.float32)  7.67 us
    ppermute x2, starting transfers between devices, passed_along(): return lax.ppermute(block, axis, route)  6.22 us
    broadcast_in_dim x5, local copies, waits for them, and re-layouts, from_everyone(): jnp.broadcast_to(array[None], (devices, *array.shape))  3.39 us
  transfers between devices with their start and end apart: 8, of which 5 were waited for; matrix products, arithmetic and copies ran while one was open for 13% of the time, Pallas kernels for 0%

commit v1 on v0

v1 whole, which is shorter than its diff:
```python
import functools

import jax
import jax.numpy as jnp
import numpy as np
from jax import lax
from jax.experimental import pallas as pl
from jax.experimental.pallas import tpu as pltpu
from jax.sharding import PartitionSpec as P

MESH = pl.DeviceIdType.MESH
F32 = jnp.float32
BF16 = jnp.bfloat16

ROWS = 256
D = 4096
HEAD = 64
CONV = 2048
KSIZE = 31
WINDOW = 128
WIDTH = 896
KV0, GLU0, GATE0, Q0 = 0, 128, 384, 640
OUTW = 512
N_GATHER = 44


def rope_tables():
    freq = (10000.0 ** (-np.arange(32, dtype=np.float64) * 2.0 / HEAD)).astype(np.float32)
    lanes = np.tile(freq.astype(np.float64), 4)[None, :]
    inner = np.arange(ROWS, dtype=np.float64)[:, None] * lanes
    outer = np.arange(16, dtype=np.float64)[:, None] * ROWS * lanes
    return tuple(f(a).astype(np.float32) for a in (inner, outer) for f in (np.cos, np.sin))


class Gather:
    def __init__(self, piece, half_rows, send_sem, recv_sem, z, y, t):
        self.piece, self.half_rows = piece, half_rows
        self.send_sem, self.recv_sem = send_sem, recv_sem
        self.z, self.y, self.t = z, y, t
        self.index = {}
        self.sent = []

    def rel(self, h, o1, o2):
        dy, dz = (o1, o2) if h == 0 else (o2, o1)
        return lax.rem(self.z + (dz + 4), 4) * 4 + lax.rem(self.y + (dy + 4), 4)

    def rows(self, part):
        n = self.half_rows
        return {"full": (0, n), "lo": (0, n // 2), "hi": (n // 2, n // 2)}[part]

    def make(self, key, h, o1, o2, part, to):
        k = self.index.setdefault(key, len(self.index))
        ref = self.piece(self.rel(h, o1, o2), h, *self.rows(part))
        return pltpu.make_async_remote_copy(
            src_ref=ref,
            dst_ref=ref,
            send_sem=self.send_sem.at[k],
            recv_sem=self.recv_sem.at[k],
            device_id=(self.rel(h, *to), self.t),
            device_id_type=MESH,
        )

    def send(self, key, h, o1, o2, part, to):
        copy = self.make(key, h, o1, o2, part, to)
        copy.start()
        self.sent.append(copy)

    def t1_send(self):
        for h in (0, 1):
            for d in (1, -1):
                self.send(("T1", h, d), h, 0, 0, "full", (d, 0))

    def t1_wait(self):
        for h in (0, 1):
            for d in (1, -1):
                self.make(("T1", h, d), h, -d, 0, "full", (d, 0)).wait_recv()

    def f1_send(self):
        for h in (0, 1):
            for d in (1, -1):
                self.send(("F1", h, d), h, -d, 0, "lo" if d == 1 else "hi", (d, 0))

    def f1_wait(self):
        for h in (0, 1):
            for d in (1, -1):
                self.make(("F1", h, d), h, 2, 0, "lo" if d == 1 else "hi", (d, 0)).wait_recv()

    def t2_send(self, offsets):
        for o, part in offsets:
            for h in (0, 1):
                for d in (1, -1):
                    self.send(("T2", h, o, part, d), h, o, 0, part, (0, d))

    def t2_wait(self, offsets):
        for o, part in offsets:
            for h in (0, 1):
                for d in (1, -1):
                    self.make(("T2", h, o, part, d), h, o, -d, part, (0, d)).wait_recv()

    def f2_send(self, offsets):
        for o in offsets:
            for h in (0, 1):
                for d in (1, -1):
                    self.send(("F2", h, o, d), h, o, -d, "lo" if d == 1 else "hi", (0, d))

    def f2_wait(self, offsets):
        for o in offsets:
            for h in (0, 1):
                for d in (1, -1):
                    self.make(("F2", h, o, d), h, o, 2, "lo" if d == 1 else "hi", (0, d)).wait_recv()

    OWN = ((0, "full"),)
    SIDES = ((-1, "full"), (1, "full"))
    FAR = ((2, "lo"), (2, "hi"))

    def drain(self):
        for copy in self.sent:
            copy.wait_send()


def kernel(
    tokens_hbm,
    gain_ref,
    wq_hbm,
    wk_ref,
    wv_ref,
    wglu_hbm,
    wgate_hbm,
    sink_ref,
    taps_ref,
    cgain_ref,
    oa_hbm,
    oc_hbm,
    cos_in,
    sin_in,
    cos_out,
    sin_out,
    out_ref,
    win,
    wa,
    wc,
    tok,
    normed,
    acc,
    kvext,
    gtail,
    ghalo,
    gext,
    filt,
    taps,
    stat_own,
    stat_all,
    mixa,
    mixc,
    local_sem,
    in_send,
    in_recv,
    out_send,
    out_recv,
    halo_send,
    halo_recv,
    stat_send,
    stat_recv,
    mix_send,
    mix_recv,
):
    s = lax.axis_index("sp")
    t = lax.axis_index("tp")
    z, y = s // 4, lax.rem(s, 4)
    x, core = t // 2, lax.rem(t, 2)

    def al(v, m):
        return pl.multiple_of(v, m)

    own_rows = pl.ds(al(s * ROWS, ROWS), ROWS)
    half = pl.ds(al(s * 128, 128), 128)
    loads = []
    for i, (src, dst) in enumerate(
        (
            (wq_hbm, win.at[own_rows, Q0 : Q0 + 256]),
            (wglu_hbm, win.at[own_rows, GLU0 : GLU0 + 256]),
            (wgate_hbm, win.at[own_rows, GATE0 : GATE0 + 256]),
            (tokens_hbm, tok),
            (oa_hbm, wa.at[half, :]),
            (oc_hbm, wc.at[half, :]),
        )
    ):
        copy = pltpu.make_async_copy(src, dst, local_sem.at[i])
        copy.start()
        loads.append(copy)
    win[own_rows, KV0 : KV0 + 128] = jnp.concatenate([wk_ref[...], wv_ref[...]], axis=1)

    def sp_at(dz, dy):
        return lax.rem(z + (dz + 4), 4) * 4 + lax.rem(y + (dy + 4), 4)

    after, before = lax.rem(s + 1, 16), lax.rem(s + 15, 16)
    barrier = pltpu.get_barrier_semaphore()
    peers = [(sp_at(dz, dy), t) for dz, dy in ((0, 1), (0, -1), (1, 0), (-1, 0))]
    peers += [(after, t), (before, t)]
    peers += [(s, lax.rem(t + i, 8)) for i in range(1, 8)]
    for peer in peers:
        pl.semaphore_signal(barrier, inc=1, device_id=peer, device_id_type=MESH)
    pl.semaphore_wait(barrier, len(peers))
    for copy in loads[:3]:
        copy.wait()

    def in_piece(src, h, lo, n):
        return win.at[pl.ds(al(src * ROWS + (h * 128 + lo), 64), n), :]

    def out_piece(src, h, lo, n):
        return (wa, wc)[h].at[pl.ds(al(src * 128 + lo, 64), n), :]

    g_in = Gather(in_piece, 128, in_send, in_recv, z, y, t)
    g_out = Gather(out_piece, 128, out_send, out_recv, z, y, t)

    g_in.t1_send()
    g_in.t2_send(Gather.OWN)

    loads[3].wait()

    def norm_rows(i, carry):
        rows = pl.ds(al(i * 16, 16), 16)
        v = tok[rows, :].astype(F32)
        scale = lax.rsqrt(jnp.mean(v * v, axis=1, keepdims=True) + 1e-06)
        normed[rows, :] = (v * scale * gain_ref[...]).astype(BF16)
        return carry

    lax.fori_loop(0, ROWS // 16, norm_rows, 0)
    taps[...] = taps_ref[...].astype(F32)

    def block_dot(src, c0, c1):
        rows = pl.ds(al(src * ROWS, ROWS), ROWS)
        return jnp.dot(normed[:, rows], win[rows, c0:c1], preferred_element_type=F32)

    g_in.t1_wait()
    g_in.f1_send()
    acc[...] = block_dot(s, 0, WIDTH)
    g_in.t2_wait(Gather.OWN)
    g_in.f2_send((0,))
    g_in.t2_send(Gather.SIDES)

    def side_block(i, carry):
        d = 1 - 2 * lax.rem(i, 2)
        dz, dy = jnp.where(i < 2, d, 0), jnp.where(i < 2, 0, d)
        src = lax.rem(z + dz + 4, 4) * 4 + lax.rem(y + dy + 4, 4)
        acc[...] += block_dot(src, 0, WIDTH)
        return carry

    def corner_block(i, carry):
        dz, dy = 2 * (i // 2) - 1, 2 * lax.rem(i, 2) - 1
        src = lax.rem(z + dz + 4, 4) * 4 + lax.rem(y + dy + 4, 4)
        acc[...] += block_dot(src, 0, WIDTH)
        return carry

    g_in.f1_wait()
    g_in.t2_send(Gather.FAR)
    lax.fori_loop(0, 4, side_block, 0)
    g_in.t2_wait(Gather.SIDES)
    g_in.f2_send((-1, 1))
    g_in.t2_wait(Gather.FAR)
    g_in.f2_send((2,))
    for copy in loads[4:]:
        copy.wait()
    g_out.t1_send()
    lax.fori_loop(0, 4, corner_block, 0)

    lane = lax.broadcasted_iota(jnp.int32, (ROWS, 128), 1)
    first = lax.rem(lane, 64) < 32
    low = lane < 64
    co, so = cos_out[pl.ds(s, 1), :], sin_out[pl.ds(s, 1), :]
    cosine = co * cos_in[...] - so * sin_in[...]
    sine = so * cos_in[...] + co * sin_in[...]
    sine = jnp.where(first, -sine, sine)

    def rotate(v, cosine, sine):
        other = jnp.where(first, pltpu.roll(v, 96, 1), pltpu.roll(v, 32, 1))
        return v * cosine + other * sine

    g_in.f2_wait((0, -1, 1, 2))

    far_row = pl.ds(al(lax.rem(z + 2, 4) * 1024, 1024), 1024)

    def finish(c0, c1):
        v = acc[:, c0:c1] + jnp.dot(
            normed[:, far_row], win[far_row, c0:c1], preferred_element_type=F32
        )
        for o in (0, 1, -1):
            v = v + block_dot(sp_at(o, 2), c0, c1)
        return v

    halos = []

    def halo(i, src, dst):
        copy = pltpu.make_async_remote_copy(
            src_ref=src,
            dst_ref=dst,
            send_sem=halo_send.at[i],
            recv_sem=halo_recv.at[i],
            device_id=(after, t),
            device_id_type=MESH,
        )
        copy.start()
        halos.append(copy)

    kv = finish(KV0, KV0 + 128)
    kv = rotate(kv, jnp.where(low, cosine, 1.0), jnp.where(low, sine, 0.0))
    kvext[WINDOW:, :] = kv.astype(BF16)
    halo(0, kvext.at[pl.ds(ROWS, WINDOW), :], kvext.at[pl.ds(0, WINDOW), :])

    for c in (0, 128):
        glu = finish(GLU0 + c, GLU0 + c + 128)
        gate = finish(GATE0 + c, GATE0 + c + 128)
        gated = (glu * (1.0 / (1.0 + jnp.exp(-gate)))).astype(BF16)
        gext[32:, c : c + 128] = gated.astype(F32)
        gtail[:, c : c + 128] = gated[ROWS - 32 :, :]
    halo(1, gtail, ghalo)
    g_out.t2_send(Gather.OWN)

    queries = []
    for c in (0, 128):
        q = rotate(finish(Q0 + c, Q0 + c + 128), cosine, sine).astype(BF16)
        queries.append(q)

    halos[1].wait_recv()
    gext[:32, :] = jnp.where(s > 0, ghalo[...].astype(F32), 0.0)

    total = jnp.zeros((ROWS, 1), F32)
    for c in (0, 128):
        for r in range(0, ROWS, 64):
            f = jnp.zeros((64, 128), F32)
            for k in range(KSIZE):
                f = f + taps[k : k + 1, c : c + 128] * gext[r + 2 + k : r + 66 + k, c : c + 128]
            filt[r : r + 64, c : c + 128] = f
    f = filt[...]
    row_sum = jnp.sum(f, axis=1, keepdims=True)
    row_square = jnp.sum(f * f, axis=1, keepdims=True)
    stat = jnp.where(lane == 0, row_sum, jnp.where(lane == 1, row_square, 0.0))
    stat_own[...] = stat.T[:8, :]
    stats = []
    for i in range(1, 8):
        copy = pltpu.make_async_remote_copy(
            src_ref=stat_own,
            dst_ref=stat_all.at[i],
            send_sem=stat_send.at[i - 1],
            recv_sem=stat_recv.at[i - 1],
            device_id=(s, lax.rem(t + i, 8)),
            device_id_type=MESH,
        )
        copy.start()
        stats.append(copy)

    g_out.t1_wait()
    g_out.f1_send()

    halos[0].wait_recv()
    kvf = kvext[...].astype(F32)
    swapped = pltpu.roll(kvf, 64, 1)
    lane_e = lax.broadcasted_iota(jnp.int32, (ROWS + WINDOW, 128), 1)
    low_e = lane_e < 64
    keys = jnp.where(low_e, kvf, swapped).astype(BF16)
    vals = jnp.where(low_e, swapped, kvf).astype(BF16)
    zero = jnp.zeros((WINDOW, 128), BF16)
    low_b = low[:WINDOW, :]
    head = lax.broadcasted_iota(jnp.int32, (4 * WINDOW, 1), 0) // WINDOW
    sink = jnp.where(
        head == 0,
        sink_ref[0, 0],
        jnp.where(head == 1, sink_ref[0, 1], jnp.where(head == 2, sink_ref[0, 2], sink_ref[0, 3])),
    )
    own_cols = pl.ds(al(t * 256, 256), 256)

    row_i = lax.rem(lax.broadcasted_iota(jnp.int32, (4 * WINDOW, 2 * WINDOW), 0), WINDOW)
    col_j = lax.broadcasted_iota(jnp.int32, (4 * WINDOW, 2 * WINDOW), 1)
    distance = row_i + WINDOW - col_j
    for b in (1, 0):
        parts = []
        for q in queries:
            qb = q[b * WINDOW : (b + 1) * WINDOW, :]
            parts += [jnp.where(low_b, qb, zero), jnp.where(low_b, zero, qb)]
        stacked = jnp.concatenate(parts, axis=0)
        kb = keys[b * WINDOW : b * WINDOW + 2 * WINDOW, :]
        vb = vals[b * WINDOW : b * WINDOW + 2 * WINDOW, :]
        scores = lax.dot_general(
            stacked, kb, (((1,), (1,)), ((), ())), preferred_element_type=F32
        ) * 0.125
        key_pos = s * ROWS + (b - 1) * WINDOW + col_j
        allowed = (distance >= 0) & (distance < WINDOW) & (key_pos >= 0)
        scores = jnp.where(allowed, scores, -1e30)
        top = jnp.maximum(jnp.max(scores, axis=1, keepdims=True), sink)
        e = jnp.exp(scores - top)
        denom = jnp.sum(e, axis=1, keepdims=True) + jnp.exp(sink - top)
        probs = (e / denom).astype(BF16)
        att = jnp.dot(probs, vb, preferred_element_type=F32)
        for j in (0, 1):
            tile = jnp.where(
                low_b,
                att[2 * j * WINDOW : (2 * j + 1) * WINDOW, :],
                att[(2 * j + 1) * WINDOW : (2 * j + 2) * WINDOW, :],
            )
            cols = pl.ds(al(t * 256 + j * 128, 128), 128)
            mixa[b * WINDOW : (b + 1) * WINDOW, cols] = tile.astype(BF16)

    mix_sent = []

    def tp_at(dx, dc):
        return lax.rem(x + (dx + 4), 4) * 2 + (core if dc == 0 else 1 - core)

    def mix_make(m, key, dx, dc, part, to):
        order = ("X+", "X-", "P0", "F+", "F-", "P+", "P-", "Q+", "Q-")
        k = m * 9 + order.index(key)
        lo, n = {"full": (0, ROWS), "lo": (0, 128), "hi": (128, 128)}[part]
        ref = (mixa, mixc)[m].at[pl.ds(lo, n), pl.ds(al(tp_at(dx, dc) * 256, 256), 256)]
        return pltpu.make_async_remote_copy(
            src_ref=ref,
            dst_ref=ref,
            send_sem=mix_send.at[k],
            recv_sem=mix_recv.at[k],
            device_id=(s, tp_at(*to)),
            device_id_type=MESH,
        )

    def mix_send_one(*args):
        copy = mix_make(*args)
        copy.start()
        mix_sent.append(copy)

    def mix_first(m):
        mix_send_one(m, "X+", 0, 0, "full", (1, 0))
        mix_send_one(m, "X-", 0, 0, "full", (-1, 0))
        mix_send_one(m, "P0", 0, 0, "full", (0, 1))

    def mix_second(m):
        for key, fkey, pkey, d, part in (("X+", "F+", "P+", 1, "lo"), ("X-", "F-", "P-", -1, "hi")):
            mix_make(m, key, -d, 0, "full", (d, 0)).wait_recv()
            mix_send_one(m, fkey, -d, 0, part, (d, 0))
            mix_send_one(m, pkey, -d, 0, "full", (0, 1))

    def mix_third(m):
        for fkey, qkey, d, part in (("F+", "Q+", 1, "lo"), ("F-", "Q-", -1, "hi")):
            mix_make(m, fkey, 2, 0, part, (d, 0)).wait_recv()
            mix_send_one(m, qkey, 2, 0, part, (0, 1))

    def mix_last(m):
        mix_make(m, "P0", 0, 1, "full", (0, 1)).wait_recv()
        for pkey, qkey, d, part in (("P+", "Q+", 1, "lo"), ("P-", "Q-", -1, "hi")):
            mix_make(m, pkey, -d, 1, "full", (0, 1)).wait_recv()
            mix_make(m, qkey, 2, 1, part, (0, 1)).wait_recv()

    mix_first(0)

    g_out.t2_wait(Gather.OWN)
    g_out.f2_send((0,))
    g_out.t2_send(Gather.SIDES)
    g_out.f1_wait()
    g_out.t2_send(Gather.FAR)

    for copy in stats:
        copy.wait_recv()
    whole = stat_own[...]
    for i in range(1, 8):
        whole = whole + stat_all[i]
    whole = jnp.concatenate([whole, jnp.zeros((120, ROWS), F32)], axis=0).T
    mean_value = whole[:, 0:1] * (1.0 / CONV)
    variance = whole[:, 1:2] * (1.0 / CONV) - mean_value * mean_value
    scaled = (filt[...] - mean_value) * lax.rsqrt(variance + 1e-05) * cgain_ref[...]
    mixc[:, own_cols] = (scaled / (1.0 + jnp.exp(-scaled))).astype(BF16)
    mix_first(1)

    mix_second(0)
    g_out.t2_wait(Gather.SIDES)
    g_out.f2_send((-1, 1))
    mix_second(1)
    mix_third(0)
    g_out.t2_wait(Gather.FAR)
    g_out.f2_send((2,))
    mix_third(1)
    mix_last(0)
    mix_last(1)
    g_out.f2_wait((0, -1, 1, 2))

    for c in range(0, OUTW, 256):
        v = jnp.dot(mixa[...], wa[:, c : c + 256], preferred_element_type=F32)
        v = v + jnp.dot(mixc[...], wc[:, c : c + 256], preferred_element_type=F32)
        out_ref[:, c : c + 256] = v.astype(BF16)

    g_in.drain()
    g_out.drain()
    for copy in halos + stats + mix_sent:
        copy.wait_send()


def per_device(
    tokens,
    norm_gain,
    w_query,
    w_key,
    w_value,
    w_glu,
    w_gate,
    sink_logit,
    conv_taps,
    conv_gain,
    out_attn,
    out_conv,
):
    hbm = pl.BlockSpec(memory_space=pl.ANY)
    vmem = pl.BlockSpec(memory_space=pltpu.VMEM)
    smem = pl.BlockSpec(memory_space=pltpu.SMEM)
    dma = pltpu.SemaphoreType.DMA
    tables = [jnp.asarray(a) for a in rope_tables()]
    return pl.pallas_call(
        kernel,
        name="mixer_layer",
        out_shape=jax.ShapeDtypeStruct((ROWS, OUTW), BF16),
        in_specs=[hbm, vmem, hbm, vmem, vmem, hbm, hbm, smem, vmem, vmem, hbm, hbm] + [vmem] * 4,
        out_specs=vmem,
        scratch_shapes=[
            pltpu.VMEM((D, WIDTH), BF16),
            pltpu.VMEM((2048, OUTW), BF16),
            pltpu.VMEM((2048, OUTW), BF16),
            pltpu.VMEM((ROWS, D), BF16),
            pltpu.VMEM((ROWS, D), BF16),
            pltpu.VMEM((ROWS, WIDTH), F32),
            pltpu.VMEM((ROWS + WINDOW, 128), BF16),
            pltpu.VMEM((32, 256), BF16),
            pltpu.VMEM((32, 256), BF16),
            pltpu.VMEM((ROWS + 32, 256), F32),
            pltpu.VMEM((ROWS, 256), F32),
            pltpu.VMEM((KSIZE, 256), F32),
            pltpu.VMEM((8, ROWS), F32),
            pltpu.VMEM((8, 8, ROWS), F32),
            pltpu.VMEM((ROWS, 2048), BF16),
            pltpu.VMEM((ROWS, 2048), BF16),
            dma((6,)),
            dma((N_GATHER,)),
            dma((N_GATHER,)),
            dma((N_GATHER,)),
            dma((N_GATHER,)),
            dma((2,)),
            dma((2,)),
            dma((7,)),
            dma((7,)),
            dma((18,)),
            dma((18,)),
        ],
        compiler_params=pltpu.CompilerParams(
            collective_id=0, has_side_effects=True, vmem_limit_bytes=48 * 1024 * 1024
        ),
    )(
        tokens,
        norm_gain[None, :],
        w_query,
        w_key,
        w_value,
        w_glu,
        w_gate,
        sink_logit[None, :],
        conv_taps,
        conv_gain[None, :],
        out_attn,
        out_conv,
        *tables,
    )


def solution(mesh):
    return jax.shard_map(
        per_device,
        mesh=mesh,
        in_specs=(
            P("sp", None),
            P(),
            P("sp", "tp"),
            P("sp", "tp"),
            P("sp", "tp"),
            P("sp", "tp"),
            P("sp", "tp"),
            P("tp"),
            P(None, "tp"),
            P("tp"),
            P("sp", "tp"),
            P("sp", "tp"),
        ),
        out_specs=P("sp", "tp"),
        check_vma=False,
    )
```

time: 168 us -> 91.7 us (0.55)
  waiting for transfers between devices: 100 us -> 0 us
  Pallas kernels: 0 us -> 76.1 us
  starting transfers between devices: 24.5 us -> 0 us
  matrix products: 14.4 us -> 0 us
  between operations: 13.8 us -> 0.04 us
  local copies, waits for them, and re-layouts: 7.87 us -> 14.5 us
  other arithmetic: 5.51 us -> 0 us
    pallas_call x0 -> x1, Pallas kernels: none -> 76.1 us  [per_device(): pl.pallas_call(kernel, name='mixer_layer', out_shape=jax.ShapeDtypeStruct...]
    all_gather x2 -> x0, waiting for transfers between devices: 64.9 us -> none  [in_one_piece(): result = lax.all_gather(both, axis, axis=dim, tiled=True)]
    all_to_all x4 -> x0, waiting for transfers between devices: 35.3 us -> none  [from_everyone(): lax.all_to_all(jnp.broadcast_to(array[None], (devices, *array.shape)), ax...]
    all_to_all x4 -> x0, starting transfers between devices: 18.3 us -> none  [from_everyone(): lax.all_to_all(jnp.broadcast_to(array[None], (devices, *array.shape)), ax...]
    dot_general x9 -> x0, matrix products: 13.7 us -> none  [the longest x5 7.67 us: per_device(): jnp.dot(normed, weight_piece, preferred_element_type=jnp.float32)]
    unnamed x17 -> x31, local copies, waits for them, and re-layouts: 1.95 us -> 14.5 us
    ppermute x2 -> x0, starting transfers between devices: 6.22 us -> none  [passed_along(): return lax.ppermute(block, axis, route)]
    broadcast_in_dim x6 -> x0, local copies, waits for them, and re-layouts: 3.4 us -> none  [the longest x5 3.39 us: from_everyone(): jnp.broadcast_to(array[None], (devices, *array.shape))]
  transfers between devices with their start and end apart: 8 -> 0, of which waited for: 5 -> 0; matrix products, arithmetic and copies ran while one was open for 13% -> 0% of each run, Pallas kernels for 0% -> 0%
where the time goes in v1:
time: 91.7 us; the launch traced here: 90.7 us
  Pallas kernels  76.1 us (83%)
  local copies, waits for them, and re-layouts  14.5 us (16%)
    pallas_call x1, Pallas kernels, per_device(): pl.pallas_call(kernel, name='mixer_layer', out_shape=jax.ShapeDtypeStruct...  76.1 us
    unnamed x31, local copies, waits for them, and re-layouts  14.5 us

profile of v1, /device:TPU:1, one launch (start us, length us, event | category | flops | bytes accessed | tf_op | source)
XLA Modules:
  0.0 90.7 jit_solution(16211133524073973096)
XLA Ops:
  0.0 0.9 copy.17.wk_ref
  0.9 0.9 copy.18.wv_ref
  1.8 0.0 copy-start
  1.8 1.6 %copy-done = bf16[256,4096]{1,0:T(8,128)(2,1)S(1)} copy-done((bf16[256,4096]{1,0:T(8,128)(2,1)S(1)}, bf16[256,4096]{1,0:T(8,128)(2,1)}, u32[]{:S(2)}) %copy-start) | copy-done | bytes 2097176
  3.4 0.0 copy-start.1
  3.4 0.9 copy-done.1
  4.3 0.0 copy-start.2
  4.3 0.9 copy-done.2
  5.2 0.0 copy-start.3
  5.2 0.9 copy-done.3
  6.1 0.0 copy-start.4
  6.1 0.9 copy-done.4
  7.0 0.0 copy-start.5
  7.0 0.9 copy-done.5
  7.9 0.0 copy-start.6
  7.9 0.9 copy-done.6
  8.8 0.0 copy-start.7
  8.8 0.9 copy-done.7
  9.7 0.0 copy-start.8
  9.7 0.7 copy-done.8
  10.4 0.0 copy-start.9
  10.4 0.7 copy-done.9
  11.1 0.0 copy-start.10
  11.1 0.7 copy-done.10
  11.8 0.0 copy-start.11
  11.8 0.7 copy-done.11
  12.5 0.0 copy-start.12
  12.5 0.7 copy-done.12
  13.2 0.0 copy-start.13
  13.2 0.7 copy-done.13
  13.8 76.1 %mixer_layer.1 = bf16[256,512]{1,0:T(8,128)(2,1)S(1)} custom-call(bf16[256,4096]{1,0:T(8,128)(2,1)S(1)} %copy-done, f32[1,4096]{1,0:T(1,128)S(1)} %bitcast.3, bf16[256,256]{1,0:T(8,128)(2,1)S(1)} %copy-done.1, bf16[256,64]{1,0:T(8,128)(2,1)S(1)} %copy.17.wk_ref, bf16[256,64]{1,0:T(8,128)(2,1)S(1)} %copy.18.wv_ref, bf16[256,256]{1,0:T(8,128)(2,1)S(1)} %copy-done.2, ...), custom_call_target="tpu_custom_call" | custom-call | tf_op jit(solution)/shard_map/mixer_layer/pallas_call | solution.py:511
  90.0 0.7 copy.20
Async XLA Ops:
  1.8 1.6 %copy-start = (bf16[256,4096]{1,0:T(8,128)(2,1)S(1)}, bf16[256,4096]{1,0:T(8,128)(2,1)}, u32[]{:S(2)}) copy-start(bf16[256,4096]{1,0:T(8,128)(2,1)} %tokens_hbm.1) | copy-start | bytes 6291460
  3.4 0.9 copy-start.1
  4.3 0.9 copy-start.2
  5.2 0.9 copy-start.3
  6.1 0.9 copy-start.4
  7.0 0.9 copy-start.5
  7.9 0.9 copy-start.6
  8.8 0.9 copy-start.7
  9.7 0.7 copy-start.8
  10.4 0.7 copy-start.9
  11.1 0.7 copy-start.10
  11.8 0.7 copy-start.11
  12.5 0.7 copy-start.12
  13.2 0.7 copy-start.13

commit v2 on v1

--- a/solution.py
+++ b/solution.py
@@ -29,7 +29,9 @@
     lanes = np.tile(freq.astype(np.float64), 4)[None, :]
     inner = np.arange(ROWS, dtype=np.float64)[:, None] * lanes
     outer = np.arange(16, dtype=np.float64)[:, None] * ROWS * lanes
-    return tuple(f(a).astype(np.float32) for a in (inner, outer) for f in (np.cos, np.sin))
+    return tuple(
+        np.concatenate([np.cos(a), np.sin(a)], axis=1).astype(np.float32) for a in (inner, outer)
+    )
 
 
 class Gather:
@@ -120,21 +122,19 @@
 
 def kernel(
     tokens_hbm,
-    gain_ref,
+    gain_hbm,
     wq_hbm,
-    wk_ref,
-    wv_ref,
+    wk_hbm,
+    wv_hbm,
     wglu_hbm,
     wgate_hbm,
-    sink_ref,
-    taps_ref,
-    cgain_ref,
+    sink_hbm,
+    taps_hbm,
+    cgain_hbm,
     oa_hbm,
     oc_hbm,
-    cos_in,
-    sin_in,
-    cos_out,
-    sin_out,
+    inner_hbm,
+    outer_hbm,
     out_ref,
     win,
     wa,
@@ -147,6 +147,13 @@
     ghalo,
     gext,
     filt,
+    kvt,
+    gain_ref,
+    sink_ref,
+    taps_ref,
+    cgain_ref,
+    inner,
+    outer,
     taps,
     stat_own,
     stat_all,
@@ -180,7 +187,15 @@
             (wq_hbm, win.at[own_rows, Q0 : Q0 + 256]),
             (wglu_hbm, win.at[own_rows, GLU0 : GLU0 + 256]),
             (wgate_hbm, win.at[own_rows, GATE0 : GATE0 + 256]),
+            (wk_hbm, kvt.at[0:64, :]),
+            (wv_hbm, kvt.at[64:128, :]),
             (tokens_hbm, tok),
+            (gain_hbm, gain_ref),
+            (taps_hbm, taps_ref),
+            (cgain_hbm, cgain_ref),
+            (sink_hbm, sink_ref),
+            (inner_hbm, inner),
+            (outer_hbm.at[s], outer),
             (oa_hbm, wa.at[half, :]),
             (oc_hbm, wc.at[half, :]),
         )
@@ -188,8 +203,6 @@
         copy = pltpu.make_async_copy(src, dst, local_sem.at[i])
         copy.start()
         loads.append(copy)
-    win[own_rows, KV0 : KV0 + 128] = jnp.concatenate([wk_ref[...], wv_ref[...]], axis=1)
-
     def sp_at(dz, dy):
         return lax.rem(z + (dz + 4), 4) * 4 + lax.rem(y + (dy + 4), 4)
 
@@ -200,9 +213,10 @@
     peers += [(s, lax.rem(t + i, 8)) for i in range(1, 8)]
     for peer in peers:
         pl.semaphore_signal(barrier, inc=1, device_id=peer, device_id_type=MESH)
+    for copy in loads[:5]:
+        copy.wait()
+    win[own_rows, KV0 : KV0 + 128] = kvt[...].astype(F32).T.astype(BF16)
     pl.semaphore_wait(barrier, len(peers))
-    for copy in loads[:3]:
-        copy.wait()
 
     def in_piece(src, h, lo, n):
         return win.at[pl.ds(al(src * ROWS + (h * 128 + lo), 64), n), :]
@@ -216,7 +230,8 @@
     g_in.t1_send()
     g_in.t2_send(Gather.OWN)
 
-    loads[3].wait()
+    for copy in loads[5:12]:
+        copy.wait()
 
     def norm_rows(i, carry):
         rows = pl.ds(al(i * 16, 16), 16)
@@ -259,7 +274,7 @@
     g_in.f2_send((-1, 1))
     g_in.t2_wait(Gather.FAR)
     g_in.f2_send((2,))
-    for copy in loads[4:]:
+    for copy in loads[12:]:
         copy.wait()
     g_out.t1_send()
     lax.fori_loop(0, 4, corner_block, 0)
@@ -267,9 +282,9 @@
     lane = lax.broadcasted_iota(jnp.int32, (ROWS, 128), 1)
     first = lax.rem(lane, 64) < 32
     low = lane < 64
-    co, so = cos_out[pl.ds(s, 1), :], sin_out[pl.ds(s, 1), :]
-    cosine = co * cos_in[...] - so * sin_in[...]
-    sine = so * cos_in[...] + co * sin_in[...]
+    co, so = outer[:, 0:128], outer[:, 128:256]
+    cosine = co * inner[:, 0:128] - so * inner[:, 128:256]
+    sine = so * inner[:, 0:128] + co * inner[:, 128:256]
     sine = jnp.where(first, -sine, sine)
 
     def rotate(v, cosine, sine):
@@ -364,8 +379,12 @@
     head = lax.broadcasted_iota(jnp.int32, (4 * WINDOW, 1), 0) // WINDOW
     sink = jnp.where(
         head == 0,
-        sink_ref[0, 0],
-        jnp.where(head == 1, sink_ref[0, 1], jnp.where(head == 2, sink_ref[0, 2], sink_ref[0, 3])),
+        sink_ref[0:1, 0:1],
+        jnp.where(
+            head == 1,
+            sink_ref[0:1, 1:2],
+            jnp.where(head == 2, sink_ref[0:1, 2:3], sink_ref[0:1, 3:4]),
+        ),
     )
     own_cols = pl.ds(al(t * 256, 256), 256)
 
@@ -503,16 +522,16 @@
     out_attn,
     out_conv,
 ):
-    hbm = pl.BlockSpec(memory_space=pl.ANY)
+    hbm = pl.BlockSpec(memory_space=pltpu.HBM)
     vmem = pl.BlockSpec(memory_space=pltpu.VMEM)
-    smem = pl.BlockSpec(memory_space=pltpu.SMEM)
     dma = pltpu.SemaphoreType.DMA
-    tables = [jnp.asarray(a) for a in rope_tables()]
+    inner, outer = rope_tables()
+    tables = (jnp.asarray(inner), jnp.asarray(outer[:, None, :]))
     return pl.pallas_call(
         kernel,
         name="mixer_layer",
         out_shape=jax.ShapeDtypeStruct((ROWS, OUTW), BF16),
-        in_specs=[hbm, vmem, hbm, vmem, vmem, hbm, hbm, smem, vmem, vmem, hbm, hbm] + [vmem] * 4,
+        in_specs=[hbm] * 14,
         out_specs=vmem,
         scratch_shapes=[
             pltpu.VMEM((D, WIDTH), BF16),
@@ -526,12 +545,19 @@
             pltpu.VMEM((32, 256), BF16),
             pltpu.VMEM((ROWS + 32, 256), F32),
             pltpu.VMEM((ROWS, 256), F32),
+            pltpu.VMEM((128, ROWS), BF16),
+            pltpu.VMEM((1, D), F32),
+            pltpu.VMEM((1, 4), F32),
+            pltpu.VMEM((KSIZE, 256), BF16),
+            pltpu.VMEM((1, 256), F32),
+            pltpu.VMEM((ROWS, 256), F32),
+            pltpu.VMEM((1, 256), F32),
             pltpu.VMEM((KSIZE, 256), F32),
             pltpu.VMEM((8, ROWS), F32),
             pltpu.VMEM((8, 8, ROWS), F32),
             pltpu.VMEM((ROWS, 2048), BF16),
             pltpu.VMEM((ROWS, 2048), BF16),
-            dma((6,)),
+            dma((14,)),
             dma((N_GATHER,)),
             dma((N_GATHER,)),
             dma((N_GATHER,)),
@@ -544,14 +570,14 @@
             dma((18,)),
         ],
         compiler_params=pltpu.CompilerParams(
-            collective_id=0, has_side_effects=True, vmem_limit_bytes=48 * 1024 * 1024
+            collective_id=0, has_side_effects=True, vmem_limit_bytes=67043328
         ),
     )(
         tokens,
         norm_gain[None, :],
         w_query,
-        w_key,
-        w_value,
+        w_key.T,
+        w_value.T,
         w_glu,
         w_gate,
         sink_logit[None, :],

time: 91.7 us -> 79.8 us (0.87)
  local copies, waits for them, and re-layouts: 14.5 us -> 1.67 us
  Pallas kernels: 76.1 us -> 77.1 us
    unnamed x31 -> x1, local copies, waits for them, and re-layouts: 14.5 us -> 1.67 us
    pallas_call x1, Pallas kernels: 76.1 us -> 77.1 us  [per_device(): pl.pallas_call(kernel, name='mixer_layer', out_shape=jax.ShapeDtypeStruct...]
where the time goes in v2:
time: 79.8 us; the launch traced here: 78.8 us
  Pallas kernels  77.1 us (97%)
  local copies, waits for them, and re-layouts  1.67 us (2%)
    pallas_call x1, Pallas kernels, per_device(): pl.pallas_call(kernel, name='mixer_layer', out_shape=jax.ShapeDtypeStruct...  77.1 us
    unnamed x1, local copies, waits for them, and re-layouts  1.67 us

profile of v2, /device:TPU:1, one launch (start us, length us, event | category | flops | bytes accessed | tf_op | source)
XLA Modules:
  0.0 78.8 jit_solution(1675770370818329107)
XLA Ops:
  0.0 77.1 %mixer_layer.1 = bf16[256,512]{1,0:T(8,128)(2,1)} custom-call(bf16[256,4096]{1,0:T(8,128)(2,1)} %tokens_hbm.1, f32[1,4096]{1,0:T(1,128)} %bitcast.7, bf16[256,256]{1,0:T(8,128)(2,1)} %wq_hbm.1, bf16[64,256]{1,0:T(8,128)(2,1)} %bitcast.5, bf16[64,256]{1,0:T(8,128)(2,1)} %bitcast.6, bf16[256,256]{1,0:T(8,128)(2,1)} %wglu_hbm.1, bf16[256,256]{1,0:T(8,128)(2,1)} %wgate_hbm.1, ...), custom_call_target="tpu_custom_call" | custom-call | tf_op jit(solution)/shard_map/mixer_layer/pallas_call | solution.py:530
  77.1 1.7 %copy.16 = bf16[256,512]{1,0:T(8,128)(2,1)} copy(bf16[256,512]{1,0:T(8,128)(2,1)} %mixer_layer.1) | data formatting | bytes 524288

commit v3 on v0

v3 whole, which is shorter than its diff:
```python
import jax
import jax.numpy as jnp
import numpy as np
from jax import lax
from jax.experimental import pallas as pl
from jax.experimental.pallas import tpu as pltpu
from jax.sharding import PartitionSpec as P

MESH = pl.DeviceIdType.MESH
F32 = jnp.float32
BF16 = jnp.bfloat16

ROWS = 256
GROUP = 1024
D = 4096
HEAD = 64
CONV = 2048
KSIZE = 31
WINDOW = 128
WIDTH = 256
OUTW = 512
XCOLS = 384
DCOLS = 512
OUT_SPLIT = 160
SEMS = 64


def rope_tables():
    freq = (10000.0 ** (-np.arange(32, dtype=np.float64) * 2.0 / HEAD)).astype(np.float32)
    lanes = np.tile(freq.astype(np.float64), 4)[None, :]
    inner = np.arange(ROWS, dtype=np.float64)[:, None] * lanes
    outer = np.arange(16, dtype=np.float64)[:, None] * ROWS * lanes
    return tuple(
        np.concatenate([np.cos(a), np.sin(a)], axis=1).astype(np.float32) for a in (inner, outer)
    )


class Net:
    def __init__(self, send_sem, recv_sem, partner):
        self.send_sem, self.recv_sem, self.partner = send_sem, recv_sem, partner
        self.index, self.sent = {}, []

    def make(self, key, src, dst, device):
        k = self.index.setdefault(key, len(self.index))
        assert k < SEMS
        return pltpu.make_async_remote_copy(
            src_ref=src,
            dst_ref=dst,
            send_sem=self.send_sem.at[k],
            recv_sem=self.recv_sem.at[k],
            device_id=device,
            device_id_type=MESH,
        )

    def send(self, key, src, dst, device):
        copy = self.make(key, src, dst, device)
        copy.start()
        self.sent.append(copy)

    def wait(self, key, ref):
        self.make(key, ref, ref, self.partner).wait_recv()

    def drain(self):
        for copy in self.sent:
            copy.wait_send()


def side(d):
    return "lo" if d == 1 else "hi"


class Ring:
    def __init__(self, net, name, ref, device):
        self.net, self.name, self.ref, self.device = net, name, ref, device

    def first(self, items):
        for o, part in items:
            for d in (1, -1):
                r = self.ref(o, 0, part)
                self.net.send((self.name, "T", o, part, d), r, r, self.device(d))

    def first_wait(self, items):
        for o, part in items:
            for d in (1, -1):
                self.net.wait((self.name, "T", o, part, d), self.ref(o, -d, part))

    def second(self, pieces):
        for o in pieces:
            for d in (1, -1):
                r = self.ref(o, -d, side(d))
                self.net.send((self.name, "F", o, d), r, r, self.device(d))

    def second_wait(self, pieces):
        for o in pieces:
            for d in (1, -1):
                self.net.wait((self.name, "F", o, d), self.ref(o, 2, side(d)))

    def give(self, items):
        for o, off, part in items:
            r = self.ref(o, off, part)
            self.net.send((self.name, "P", o, off, part), r, r, self.net.partner)

    def give_wait(self, items):
        for o, off, part in items:
            self.net.wait((self.name, "P", o, off, part), self.ref(o, off, part, False))


OWN = ((0, "full"),)
SIDES = ((-1, "full"), (1, "full"))
FAR = ((2, "lo"), (2, "hi"))


def spread(items, offs):
    return tuple((o, off, part) for o, part in items for off in offs)


def kernel(
    tokens_hbm,
    gain_hbm,
    wq_hbm,
    wk_hbm,
    wv_hbm,
    wglu_hbm,
    wgate_hbm,
    sink_hbm,
    taps_hbm,
    cgain_hbm,
    oa_hbm,
    oc_hbm,
    inner_hbm,
    outer_hbm,
    out_ref,
    wst,
    transit,
    win,
    wo,
    tok,
    nrm,
    acc,
    qbuf,
    kvext,
    keys,
    vals,
    gtail,
    ghalo,
    gext,
    filt,
    kvt,
    gain_ref,
    sink_ref,
    taps_ref,
    cgain_ref,
    inner,
    outer,
    taps,
    stat_own,
    stat_all,
    mx,
    mtransit,
    mixall,
    local_sem,
    w_send,
    w_recv,
    t_send,
    t_recv,
    o_send,
    o_recv,
    m_send,
    m_recv,
    halo_send,
    halo_recv,
    stat_send,
    stat_recv,
):
    s = lax.axis_index("sp")
    t = lax.axis_index("tp")
    z, y = s // 4, lax.rem(s, 4)
    x, core = t // 2, lax.rem(t, 2)

    def al(v, m):
        return pl.multiple_of(v, m)

    def wrap(v, o):
        return lax.rem(v + (o + 4), 4)

    def sp_at(dz, dy):
        return wrap(z, dz) * 4 + wrap(y, dy)

    def tp_at(dx, mine=True):
        return wrap(x, dx) * 2 + (core if mine else 1 - core)

    partner = (s, tp_at(0, False))
    barrier = pltpu.get_barrier_semaphore()
    peers = [(sp_at(dz, dy), t) for dz, dy in ((0, 1), (0, -1), (1, 0), (-1, 0))]
    peers += [(s, tp_at(1)), (s, tp_at(-1)), partner]
    for peer in peers:
        pl.semaphore_signal(barrier, inc=1, device_id=peer, device_id_type=MESH)

    role_half = pl.ds(al(lax.rem(y, 2) * 128, 128), 128)
    loads = {}
    for name, src, dst in (
        ("tok", tokens_hbm, tok),
        ("gain", gain_hbm, gain_ref),
        ("wk", wk_hbm, kvt.at[0:64, :]),
        ("wv", wv_hbm, kvt.at[64:128, :]),
        ("q0", wq_hbm.at[:, 0:128], wst.at[0, :, 0:128]),
        ("q1", wq_hbm.at[:, 128:256], wst.at[1, :, 0:128]),
        ("glu0", wglu_hbm.at[:, 0:128], wst.at[2, :, 0:128]),
        ("glu1", wglu_hbm.at[:, 128:256], wst.at[3, :, 0:128]),
        ("gate0", wgate_hbm.at[:, 0:128], wst.at[2, :, 128:256]),
        ("gate1", wgate_hbm.at[:, 128:256], wst.at[3, :, 128:256]),
        ("oa", oa_hbm, wo.at[pl.ds(al(s * ROWS, ROWS), 128), :]),
        ("oc", oc_hbm, wo.at[pl.ds(al(s * ROWS + 128, 128), 128), :]),
        ("taps", taps_hbm.at[:, role_half], taps_ref),
        ("cgain", cgain_hbm.at[:, role_half], cgain_ref),
        ("sink", sink_hbm, sink_ref),
        ("inner", inner_hbm, inner),
        ("outer", outer_hbm.at[pl.ds(z * 4, 4)], outer),
    ):
        copy = pltpu.make_async_copy(src, dst, local_sem.at[len(loads)])
        copy.start()
        loads[name] = copy

    def loaded(*names):
        for name in names:
            loads[name].wait()

    loaded("wk", "wv")
    kv_t = kvt[...].astype(F32).T.astype(BF16)
    wst[0, :, 128:256] = kv_t
    wst[1, :, 128:256] = kv_t
    loaded("tok", "gain")

    def norm_rows(i, carry):
        v = tok[pl.ds(al(i * 16, 16), 16), :].astype(F32)
        scale = lax.rsqrt(jnp.mean(v * v, axis=1, keepdims=True) + 1e-06)
        nrm[pl.ds(al(y * ROWS + i * 16, 16), 16), :] = (v * scale * gain_ref[...]).astype(BF16)
        return carry

    lax.fori_loop(0, ROWS // 16, norm_rows, 0)
    loaded("q0", "q1", "glu0", "glu1", "gate0", "gate1")
    pl.semaphore_wait(barrier, len(peers))

    w_net = Net(w_send, w_recv, partner)
    t_net = Net(t_send, t_recv, partner)
    o_net = Net(o_send, o_recv, partner)
    m_net = Net(m_send, m_recv, partner)

    def y_dev(d):
        return (sp_at(0, d), t)

    def z_dev(d):
        return (sp_at(d, 0), t)

    def x_dev(d):
        return (s, tp_at(d))

    def part_of(part, n):
        return {"full": (0, n), "lo": (0, n // 2), "hi": (n // 2, n // 2)}[part]

    def win_ref(o, off, part, mine=True):
        lo, n = part_of(part, ROWS)
        return win.at[pl.ds(al(sp_at(off, o) * ROWS + lo, 128), n), :]

    def tok_rows(o, part):
        lo, n = part_of(part, ROWS)
        return pl.ds(al(wrap(y, o) * ROWS + lo, 128), n)

    def tokx_ref(o, off, part, mine=True):
        return nrm.at[tok_rows(o, part), pl.ds(al(tp_at(off, mine) * XCOLS, 128), XCOLS)]

    def tokd_ref(o, off, part, mine=True):
        c = core if mine else 1 - core
        return nrm.at[tok_rows(o, part), pl.ds(al(8 * XCOLS + c * DCOLS, 128), DCOLS)]

    def along_y(ref):
        return lambda o, off, part, mine=True: ref(off, 0, part, mine)

    tx_y = Ring(t_net, "txy", along_y(tokx_ref), y_dev)
    td_y = Ring(t_net, "tdy", along_y(tokd_ref), y_dev)
    tx_x = Ring(t_net, "txx", tokx_ref, x_dev)
    td_p = Ring(t_net, "tdp", tokd_ref, x_dev)
    w_z = Ring(w_net, "wz", win_ref, z_dev)

    def out_ref_of(h):
        base, size = ((0, OUT_SPLIT), (OUT_SPLIT, ROWS - OUT_SPLIT))[h]

        def first(o, off, part, mine=True):
            lo, n = part_of(part, size)
            src = sp_at(0, off) if h == 0 else sp_at(off, 0)
            return wo.at[pl.ds(al(src * ROWS + (base + lo), 16), n), :]

        def second(o, off, part, mine=True):
            lo, n = part_of(part, size)
            src = sp_at(off, o) if h == 0 else sp_at(o, off)
            return wo.at[pl.ds(al(src * ROWS + (base + lo), 16), n), :]

        return first, second

    o_first, o_second = [], []
    for h in (0, 1):
        f, g = out_ref_of(h)
        o_first.append(Ring(o_net, ("of", h), f, (y_dev, z_dev)[h]))
        o_second.append(Ring(o_net, ("os", h), g, (z_dev, y_dev)[h]))

    tx_y.first(OWN)
    for d in (1, -1):
        lo, n = part_of(side(d), ROWS)
        w_net.send(
            ("tr", d), wst.at[wrap(y, 2), pl.ds(lo, n), :], transit.at[(1 - d) // 2], y_dev(d)
        )
    for d in (1, -1):
        w_net.send(("w", d), wst.at[wrap(y, d)], win_ref(0, 0, "full"), y_dev(d))
    for d in (1, -1):
        w_net.send(("wz", "T", 0, "full", d), wst.at[y], win_ref(0, 0, "full"), z_dev(d))
    win[pl.ds(al(s * ROWS, ROWS), ROWS), :] = wst[y]
    loaded("oa", "oc")
    o_first[1].first(OWN)

    tx_y.first_wait(OWN)
    tx_y.second((0,))
    tx_x.first(SIDES)
    tx_x.give(spread(SIDES, (0,)))
    for d in (1, -1):
        lo, n = part_of(side(d), ROWS)
        buf = transit.at[(1 - d) // 2]
        w_net.wait(("tr", d), buf)
        w_net.send(("trf", d), buf, win_ref(-d, 0, side(d)), y_dev(d))
    td_y.first(OWN)
    for d in (1, -1):
        w_net.wait(("w", d), win_ref(-d, 0, "full"))
    w_z.first(SIDES)
    w_z.first_wait(OWN)
    w_z.second((0,))
    tx_y.second_wait((0,))
    tx_x.first(FAR)
    tx_x.give(spread(FAR, (0,)))
    for d in (1, -1):
        w_net.wait(("trf", d), win_ref(2, 0, side(d)))
    w_z.first(FAR)
    tx_x.first_wait(SIDES)
    tx_x.second((-1, 1))
    tx_x.give(spread(SIDES, (1, -1)))
    w_z.first_wait(SIDES)
    w_z.second((-1, 1))
    td_y.first_wait(OWN)
    td_y.second((0,))
    td_p.give(((-1, 0, "full"), (1, 0, "full")))
    o_first[0].first(OWN)
    w_z.first_wait(FAR)
    w_z.second((2,))
    o_second[0].first(OWN)
    tx_x.first_wait(FAR)
    tx_x.second((2,))
    tx_x.give(spread(FAR, (1, -1)))

    loaded("taps", "cgain", "sink", "inner", "outer")
    taps[...] = taps_ref[...].astype(F32)

    w_z.second_wait((0, -1, 1, 2))

    def project(o):
        rows = pl.ds(al(wrap(y, o) * ROWS, ROWS), ROWS)
        acc[rows, :] = jnp.dot(nrm[rows, :], win[...], preferred_element_type=F32)

    project(0)
    tx_x.second_wait((-1, 1))
    tx_x.give(((-1, 2, "lo"), (-1, 2, "hi"), (1, 2, "lo"), (1, 2, "hi")))
    o_first[1].first_wait(OWN)
    o_first[1].second((0,))
    td_y.second_wait((0,))
    td_p.give(((2, 0, "lo"), (2, 0, "hi")))
    o_second[1].first(OWN)
    tx_x.give_wait(spread(SIDES, (0, 1, -1)))
    tx_x.give_wait(((-1, 2, "lo"), (-1, 2, "hi"), (1, 2, "lo"), (1, 2, "hi")))
    td_p.give_wait(((-1, 0, "full"), (1, 0, "full")))
    project(-1)
    project(1)
    tx_x.second_wait((2,))
    tx_x.give(((2, 2, "lo"), (2, 2, "hi")))
    tx_x.give_wait(spread(FAR, (0, 1, -1)))
    tx_x.give_wait(((2, 2, "lo"), (2, 2, "hi")))
    td_p.give_wait(((2, 0, "lo"), (2, 0, "hi")))
    project(2)

    def halo_copy(i, src, dst):
        return pltpu.make_async_remote_copy(
            src_ref=src,
            dst_ref=dst,
            send_sem=halo_send.at[i],
            recv_sem=halo_recv.at[i],
            device_id=z_dev(1),
            device_id_type=MESH,
        )

    lane = lax.broadcasted_iota(jnp.int32, (ROWS, 128), 1)

    def attention():
        first = lax.rem(lane, 64) < 32
        low = lane < 64

        def rotate(v, cosine, sine):
            other = jnp.where(first, pltpu.roll(v, 96, 1), pltpu.roll(v, 32, 1))
            return v * cosine + other * sine

        def fill(b, carry):
            rows = pl.ds(al(b * ROWS, ROWS), ROWS)
            ext = pl.ds(al(b * ROWS + WINDOW, WINDOW), ROWS)
            edge = outer[b]
            co, so = edge[:, 0:128], edge[:, 128:256]
            cosine = co * inner[:, 0:128] - so * inner[:, 128:256]
            sine = so * inner[:, 0:128] + co * inner[:, 128:256]
            sine = jnp.where(first, -sine, sine)
            qbuf[rows, :] = rotate(acc[rows, 0:128], cosine, sine).astype(BF16)
            kv = rotate(
                acc[rows, 128:256], jnp.where(low, cosine, 1.0), jnp.where(low, sine, 0.0)
            )
            kv = kv.astype(BF16)
            kvext[ext, :] = kv
            kv = kv.astype(F32)
            swapped = pltpu.roll(kv, 64, 1)
            keys[ext, :] = jnp.where(low, kv, swapped).astype(BF16)
            vals[ext, :] = jnp.where(low, swapped, kv).astype(BF16)
            return carry

        fill(3, 0)
        halo = halo_copy(0, kvext.at[pl.ds(GROUP, WINDOW), :], kvext.at[pl.ds(0, WINDOW), :])
        halo.start()
        lax.fori_loop(0, 3, fill, 0)

        low_w = low[:WINDOW, :]
        zero = jnp.zeros((WINDOW, 128), BF16)
        second = lax.broadcasted_iota(jnp.int32, (2 * WINDOW, 1), 0) >= WINDOW
        sink_a = jnp.where(y == 0, sink_ref[0:1, 0:1], sink_ref[0:1, 2:3])
        sink_b = jnp.where(y == 0, sink_ref[0:1, 1:2], sink_ref[0:1, 3:4])
        sink = jnp.where(second, sink_b, sink_a)
        row_i = lax.rem(lax.broadcasted_iota(jnp.int32, (2 * WINDOW, 2 * WINDOW), 0), WINDOW)
        col_j = lax.broadcasted_iota(jnp.int32, (2 * WINDOW, 2 * WINDOW), 1)
        distance = row_i + WINDOW - col_j
        near = (distance >= 0) & (distance < WINDOW)

        def attend(b):
            at = al(b * WINDOW, WINDOW)
            q = qbuf[pl.ds(at, WINDOW), :]
            stacked = jnp.concatenate([jnp.where(low_w, q, zero), jnp.where(low_w, zero, q)], axis=0)
            scores = lax.dot_general(
                stacked,
                keys[pl.ds(at, 2 * WINDOW), :],
                (((1,), (1,)), ((), ())),
                preferred_element_type=F32,
            )
            key_pos = z * GROUP + (b - 1) * WINDOW + col_j
            scores = jnp.where(near & (key_pos >= 0), scores * 0.125, -1e30)
            top = jnp.maximum(jnp.max(scores, axis=1, keepdims=True), sink)
            e = jnp.exp(scores - top)
            denom = jnp.sum(e, axis=1, keepdims=True) + jnp.exp(sink - top)
            probs = (e / denom).astype(BF16)
            att = jnp.dot(probs, vals[pl.ds(at, 2 * WINDOW), :], preferred_element_type=F32)
            mx[pl.ds(at, WINDOW), :] = jnp.where(low_w, att[:WINDOW, :], att[WINDOW:, :]).astype(BF16)

        def attend_pair(i, carry):
            attend(2 * i + 2)
            attend(2 * i + 1)
            return carry

        lax.fori_loop(0, 3, attend_pair, 0)
        attend(7)
        halo.wait_recv()
        edge = kvext[0:WINDOW, :].astype(F32)
        swapped = pltpu.roll(edge, 64, 1)
        keys[0:WINDOW, :] = jnp.where(low_w, edge, swapped).astype(BF16)
        vals[0:WINDOW, :] = jnp.where(low_w, swapped, edge).astype(BF16)
        attend(0)
        halo.wait_send()

    def convolution():
        def gate_rows(b, carry):
            rows = pl.ds(al(b * ROWS, ROWS), ROWS)
            g = acc[rows, 0:128] * (1.0 / (1.0 + jnp.exp(-acc[rows, 128:256])))
            gext[pl.ds(al(b * ROWS + 32, 32), ROWS), :] = g.astype(BF16).astype(F32)
            return carry

        gate_rows(3, 0)
        gtail[...] = gext[GROUP : GROUP + 32, :].astype(BF16)
        halo = halo_copy(1, gtail, ghalo)
        halo.start()
        lax.fori_loop(0, 3, gate_rows, 0)

        def filter_rows(r):
            f = jnp.zeros((64, 128), F32)
            for k in range(KSIZE):
                f = f + taps[k : k + 1, :] * gext[r + 2 + k : r + 66 + k, :]
            filt[r : r + 64, :] = f

        for r in range(64, GROUP, 64):
            filter_rows(r)
        halo.wait_recv()
        gext[0:32, :] = jnp.where(z > 0, ghalo[...].astype(F32), 0.0)
        filter_rows(0)

        stat = jnp.zeros((ROWS, 128), F32)
        for b in range(4):
            f = filt[b * ROWS : (b + 1) * ROWS, :]
            stat = jnp.where(lane == 2 * b, jnp.sum(f, axis=1, keepdims=True), stat)
            stat = jnp.where(lane == 2 * b + 1, jnp.sum(f * f, axis=1, keepdims=True), stat)
        stat_own[...] = stat.T[:8, :]
        copies = []
        for dy in (0, 1):
            for i in range(8):
                if dy == 0 and i == 0:
                    continue
                k = dy * 8 + i - 1
                copy = pltpu.make_async_remote_copy(
                    src_ref=stat_own,
                    dst_ref=stat_all.at[k],
                    send_sem=stat_send.at[k],
                    recv_sem=stat_recv.at[k],
                    device_id=(z * 4 + (y if dy == 0 else 5 - y), lax.rem(t + i, 8)),
                    device_id_type=MESH,
                )
                copy.start()
                copies.append(copy)
        whole = stat_own[...]
        for k, copy in enumerate(copies):
            copy.wait_recv()
            whole = whole + stat_all[k]
        whole = jnp.concatenate([whole, jnp.zeros((120, ROWS), F32)], axis=0).T
        for b in range(4):
            rows = slice(b * ROWS, (b + 1) * ROWS)
            mean_value = whole[:, 2 * b : 2 * b + 1] * (1.0 / CONV)
            variance = whole[:, 2 * b + 1 : 2 * b + 2] * (1.0 / CONV) - mean_value * mean_value
            scaled = (filt[rows, :] - mean_value) * lax.rsqrt(variance + 1e-05) * cgain_ref[...]
            mx[rows, :] = (scaled / (1.0 + jnp.exp(-scaled))).astype(BF16)
        for copy in copies:
            copy.wait_send()
        halo.wait_send()

    pl.when(y < 2)(attention)
    pl.when(y >= 2)(convolution)

    def mix_cols(o, off, mine=True):
        yy = wrap(y, o)
        block = 2 * tp_at(off, mine) + lax.rem(yy, 2)
        return pl.ds(al(block * 256 + (yy // 2) * 128, 128), 128)

    def mix_ref(o, off, part, mine=True):
        lo, n = part_of(part, ROWS)
        return mixall.at[pl.ds(lo, n), mix_cols(o, off, mine)]

    m_x = Ring(m_net, "mx", mix_ref, x_dev)
    for d in (1, -1):
        lo, n = part_of(side(d), ROWS)
        src = mx.at[pl.ds(al(wrap(y, 2) * ROWS + lo, 128), n), :]
        m_net.send(("tr", d), src, mtransit.at[(1 - d) // 2], y_dev(d))
    for d in (1, -1):
        src = mx.at[pl.ds(al(wrap(y, d) * ROWS, 128), ROWS), :]
        m_net.send(("m", d), src, mix_ref(0, 0, "full"), y_dev(d))
    mixall[:, mix_cols(0, 0)] = mx[pl.ds(al(y * ROWS, ROWS), ROWS), :]
    m_x.first(OWN)
    m_x.give(spread(OWN, (0,)))

    o_first[0].first_wait(OWN)
    o_first[0].second((0,))
    for d in (1, -1):
        buf = mtransit.at[(1 - d) // 2]
        m_net.wait(("tr", d), buf)
        m_net.send(("trf", d), buf, mix_ref(-d, 0, side(d)), y_dev(d))
    for d in (1, -1):
        m_net.wait(("m", d), mix_ref(-d, 0, "full"))
    m_x.first(SIDES)
    m_x.give(spread(SIDES, (0,)))

    for h in (0, 1):
        o_second[h].first_wait(OWN)
        o_second[h].second((0,))
        o_second[h].first(SIDES)
    for h in (0, 1):
        o_first[h].second_wait((0,))
        o_second[h].first(FAR)
    m_x.first_wait(OWN)
    m_x.second((0,))
    m_x.give(spread(OWN, (1, -1)))
    for d in (1, -1):
        m_net.wait(("trf", d), mix_ref(2, 0, side(d)))
    m_x.first(FAR)
    m_x.give(spread(FAR, (0,)))
    m_x.first_wait(SIDES)
    m_x.second((-1, 1))
    m_x.give(spread(SIDES, (1, -1)))
    for h in (0, 1):
        o_second[h].first_wait(SIDES)
        o_second[h].second((-1, 1))
    m_x.first_wait(FAR)
    m_x.second((2,))
    m_x.give(spread(FAR, (1, -1)))
    for h in (0, 1):
        o_second[h].first_wait(FAR)
        o_second[h].second((2,))
    m_x.second_wait((0, -1, 1, 2))
    last = tuple((o, 2, part) for o in (0, -1, 1, 2) for part in ("lo", "hi"))
    m_x.give(last)
    m_x.give_wait(spread(OWN + SIDES + FAR, (0, 1, -1)))
    m_x.give_wait(last)
    for h in (0, 1):
        o_second[h].second_wait((0, -1, 1, 2))

    for c in range(0, OUTW, 256):
        out_ref[:, c : c + 256] = jnp.dot(
            mixall[...], wo[:, c : c + 256], preferred_element_type=F32
        ).astype(BF16)

    for net in (w_net, t_net, o_net, m_net):
        net.drain()


def per_device(
    tokens,
    norm_gain,
    w_query,
    w_key,
    w_value,
    w_glu,
    w_gate,
    sink_logit,
    conv_taps,
    conv_gain,
    out_attn,
    out_conv,
):
    hbm = pl.BlockSpec(memory_space=pltpu.HBM)
    vmem = pl.BlockSpec(memory_space=pltpu.VMEM)
    dma = pltpu.SemaphoreType.DMA
    inner, outer = rope_tables()
    tables = (jnp.asarray(inner), jnp.asarray(outer[:, None, :]))
    return pl.pallas_call(
        kernel,
        name="mixer_layer",
        out_shape=jax.ShapeDtypeStruct((ROWS, OUTW), BF16),
        in_specs=[hbm] * 14,
        out_specs=vmem,
        scratch_shapes=[
            pltpu.VMEM((4, ROWS, WIDTH), BF16),
            pltpu.VMEM((2, 128, WIDTH), BF16),
            pltpu.VMEM((D, WIDTH), BF16),
            pltpu.VMEM((D, OUTW), BF16),
            pltpu.VMEM((ROWS, D), BF16),
            pltpu.VMEM((GROUP, D), BF16),
            pltpu.VMEM((GROUP, WIDTH), F32),
            pltpu.VMEM((GROUP, 128), BF16),
            pltpu.VMEM((GROUP + WINDOW, 128), BF16),
            pltpu.VMEM((GROUP + WINDOW, 128), BF16),
            pltpu.VMEM((GROUP + WINDOW, 128), BF16),
            pltpu.VMEM((32, 128), BF16),
            pltpu.VMEM((32, 128), BF16),
            pltpu.VMEM((GROUP + 32, 128), F32),
            pltpu.VMEM((GROUP, 128), F32),
            pltpu.VMEM((128, ROWS), BF16),
            pltpu.VMEM((1, D), F32),
            pltpu.VMEM((1, 4), F32),
            pltpu.VMEM((KSIZE, 128), BF16),
            pltpu.VMEM((1, 128), F32),
            pltpu.VMEM((ROWS, 256), F32),
            pltpu.VMEM((4, 1, 256), F32),
            pltpu.VMEM((KSIZE, 128), F32),
            pltpu.VMEM((8, ROWS), F32),
            pltpu.VMEM((15, 8, ROWS), F32),
            pltpu.VMEM((GROUP, 128), BF16),
            pltpu.VMEM((2, 128, 128), BF16),
            pltpu.VMEM((ROWS, D), BF16),
            dma((17,)),
            dma((SEMS,)),
            dma((SEMS,)),
            dma((SEMS,)),
            dma((SEMS,)),
            dma((SEMS,)),
            dma((SEMS,)),
            dma((SEMS,)),
            dma((SEMS,)),
            dma((2,)),
            dma((2,)),
            dma((15,)),
            dma((15,)),
        ],
        compiler_params=pltpu.CompilerParams(
            collective_id=0, has_side_effects=True, vmem_limit_bytes=67043328
        ),
    )(
        tokens,
        norm_gain[None, :],
        w_query,
        w_key.T,
        w_value.T,
        w_glu,
        w_gate,
        sink_logit[None, :],
        conv_taps,
        conv_gain[None, :],
        out_attn,
        out_conv,
        *tables,
    )


def solution(mesh):
    return jax.shard_map(
        per_device,
        mesh=mesh,
        in_specs=(
            P("sp", None),
            P(),
            P("sp", "tp"),
            P("sp", "tp"),
            P("sp", "tp"),
            P("sp", "tp"),
            P("sp", "tp"),
            P("tp"),
            P(None, "tp"),
            P("tp"),
            P("sp", "tp"),
            P("sp", "tp"),
        ),
        out_specs=P("sp", "tp"),
        check_vma=False,
    )
```

time: 168 us -> 86.2 us (0.51)
  the two profiles are of different devices: /device:TPU:1 before, /device:TPU:0 now
where the time goes in v3:
time: 86.2 us; the launch traced here: 86.1 us
  Pallas kernels  84.4 us (98%)
  local copies, waits for them, and re-layouts  1.67 us (2%)
    pallas_call x1, Pallas kernels, per_device(): pl.pallas_call(kernel, name='mixer_layer', out_shape=jax.ShapeDtypeStruct...  84.4 us

profile of v3, /device:TPU:0, one launch (start us, length us, event | category | flops | bytes accessed | tf_op | source)
XLA Modules:
  0.0 86.1 jit_solution(1727916132176799398)
XLA Ops:
  0.0 84.4 %mixer_layer.1 = bf16[256,512]{1,0:T(8,128)(2,1)} custom-call(bf16[256,4096]{1,0:T(8,128)(2,1)} %tokens_hbm.1, f32[1,4096]{1,0:T(1,128)} %bitcast.7, bf16[256,256]{1,0:T(8,128)(2,1)} %wq_hbm.1, bf16[64,256]{1,0:T(8,128)(2,1)} %bitcast.5, bf16[64,256]{1,0:T(8,128)(2,1)} %bitcast.6, bf16[256,256]{1,0:T(8,128)(2,1)} %wglu_hbm.1, bf16[256,256]{1,0:T(8,128)(2,1)} %wgate_hbm.1, ...), custom_call_target="tpu_custom_call" | custom-call | tf_op jit(solution)/shard_map/mixer_layer/pallas_call | solution.py:635
  84.4 1.7 %copy.16 = bf16[256,512]{1,0:T(8,128)(2,1)} copy(bf16[256,512]{1,0:T(8,128)(2,1)} %mixer_layer.1) | data formatting | bytes 524288

commit v4 on v3

--- a/solution.py
+++ b/solution.py
@@ -22,7 +22,7 @@
 XCOLS = 384
 DCOLS = 512
 OUT_SPLIT = 160
-SEMS = 64
+SEMS = 20
 
 
 def rope_tables():
@@ -36,33 +36,40 @@
 
 
 class Net:
-    def __init__(self, send_sem, recv_sem, partner):
-        self.send_sem, self.recv_sem, self.partner = send_sem, recv_sem, partner
-        self.index, self.sent = {}, []
-
-    def make(self, key, src, dst, device):
-        k = self.index.setdefault(key, len(self.index))
+    def __init__(self, send_sem, recv_sem, meter, partner):
+        self.send_sem, self.recv_sem, self.meter, self.partner = send_sem, recv_sem, meter, partner
+        self.index, self.size, self.total = {}, {}, 0
+
+    def send(self, group, src, dst, device):
+        k = self.index.setdefault(group, len(self.index))
         assert k < SEMS
-        return pltpu.make_async_remote_copy(
+        count = src.dtype.itemsize
+        for n in src.shape:
+            count *= n
+        self.size[group] = self.size.get(group, 0) + count
+        self.total += count
+        pltpu.make_async_remote_copy(
             src_ref=src,
             dst_ref=dst,
-            send_sem=self.send_sem.at[k],
+            send_sem=self.send_sem.at[0],
             recv_sem=self.recv_sem.at[k],
             device_id=device,
             device_id_type=MESH,
-        )
-
-    def send(self, key, src, dst, device):
-        copy = self.make(key, src, dst, device)
-        copy.start()
-        self.sent.append(copy)
-
-    def wait(self, key, ref):
-        self.make(key, ref, ref, self.partner).wait_recv()
+        ).start()
+
+    def await_bytes(self, sem, count):
+        tiles = count // 2048
+        across = max(n for n in range(1, 33) if tiles % n == 0)
+        down = tiles // across
+        assert tiles * 2048 == count and down <= 128
+        counted = self.meter.at[0 : down * 8, 0 : across * 128]
+        pltpu.make_async_copy(counted, counted, sem).wait()
+
+    def wait(self, group):
+        self.await_bytes(self.recv_sem.at[self.index[group]], self.size[group])
 
     def drain(self):
-        for copy in self.sent:
-            copy.wait_send()
+        self.await_bytes(self.send_sem.at[0], self.total)
 
 
 def side(d):
@@ -77,32 +84,27 @@
         for o, part in items:
             for d in (1, -1):
                 r = self.ref(o, 0, part)
-                self.net.send((self.name, "T", o, part, d), r, r, self.device(d))
+                self.net.send((self.name, "T", items), r, r, self.device(d))
 
     def first_wait(self, items):
-        for o, part in items:
-            for d in (1, -1):
-                self.net.wait((self.name, "T", o, part, d), self.ref(o, -d, part))
+        self.net.wait((self.name, "T", items))
 
     def second(self, pieces):
         for o in pieces:
             for d in (1, -1):
                 r = self.ref(o, -d, side(d))
-                self.net.send((self.name, "F", o, d), r, r, self.device(d))
+                self.net.send((self.name, "F", pieces), r, r, self.device(d))
 
     def second_wait(self, pieces):
-        for o in pieces:
-            for d in (1, -1):
-                self.net.wait((self.name, "F", o, d), self.ref(o, 2, side(d)))
+        self.net.wait((self.name, "F", pieces))
 
     def give(self, items):
         for o, off, part in items:
             r = self.ref(o, off, part)
-            self.net.send((self.name, "P", o, off, part), r, r, self.net.partner)
+            self.net.send((self.name, "P", items), r, r, self.net.partner)
 
     def give_wait(self, items):
-        for o, off, part in items:
-            self.net.wait((self.name, "P", o, off, part), self.ref(o, off, part, False))
+        self.net.wait((self.name, "P", items))
 
 
 OWN = ((0, "full"),)
@@ -112,6 +114,13 @@
 
 def spread(items, offs):
     return tuple((o, off, part) for o, part in items for off in offs)
+
+
+HALVES = ("lo", "hi")
+OWN0, SIDES0, FAR0 = spread(OWN, (0,)), spread(SIDES, (0,)), spread(FAR, (0,))
+OWN2 = tuple((0, 2, part) for part in HALVES)
+SIDES2 = tuple((o, 2, part) for o in (-1, 1) for part in HALVES)
+FAR2 = tuple((2, 2, part) for part in HALVES)
 
 
 def kernel(
@@ -144,20 +153,20 @@
     gtail,
     ghalo,
     gext,
-    filt,
     kvt,
     gain_ref,
     sink_ref,
     taps_ref,
     cgain_ref,
+    gall,
+    gfull,
     inner,
     outer,
     taps,
-    stat_own,
-    stat_all,
     mx,
     mtransit,
     mixall,
+    convn,
     local_sem,
     w_send,
     w_recv,
@@ -167,10 +176,10 @@
     o_recv,
     m_send,
     m_recv,
+    g_send,
+    g_recv,
     halo_send,
     halo_recv,
-    stat_send,
-    stat_recv,
 ):
     s = lax.axis_index("sp")
     t = lax.axis_index("tp")
@@ -209,10 +218,10 @@
         ("glu1", wglu_hbm.at[:, 128:256], wst.at[3, :, 0:128]),
         ("gate0", wgate_hbm.at[:, 0:128], wst.at[2, :, 128:256]),
         ("gate1", wgate_hbm.at[:, 128:256], wst.at[3, :, 128:256]),
-        ("oa", oa_hbm, wo.at[pl.ds(al(s * ROWS, ROWS), 128), :]),
-        ("oc", oc_hbm, wo.at[pl.ds(al(s * ROWS + 128, 128), 128), :]),
+        ("oa", oa_hbm, wo.at[s, 0:128, :]),
+        ("oc", oc_hbm, wo.at[s, 128:256, :]),
         ("taps", taps_hbm.at[:, role_half], taps_ref),
-        ("cgain", cgain_hbm.at[:, role_half], cgain_ref),
+        ("cgain", cgain_hbm, cgain_ref),
         ("sink", sink_hbm, sink_ref),
         ("inner", inner_hbm, inner),
         ("outer", outer_hbm.at[pl.ds(z * 4, 4)], outer),
@@ -241,10 +250,11 @@
     loaded("q0", "q1", "glu0", "glu1", "gate0", "gate1")
     pl.semaphore_wait(barrier, len(peers))
 
-    w_net = Net(w_send, w_recv, partner)
-    t_net = Net(t_send, t_recv, partner)
-    o_net = Net(o_send, o_recv, partner)
-    m_net = Net(m_send, m_recv, partner)
+    w_net = Net(w_send, w_recv, nrm, partner)
+    t_net = Net(t_send, t_recv, nrm, partner)
+    o_net = Net(o_send, o_recv, nrm, partner)
+    m_net = Net(m_send, m_recv, nrm, partner)
+    g_net = Net(g_send, g_recv, nrm, partner)
 
     def y_dev(d):
         return (sp_at(0, d), t)
@@ -288,12 +298,12 @@
         def first(o, off, part, mine=True):
             lo, n = part_of(part, size)
             src = sp_at(0, off) if h == 0 else sp_at(off, 0)
-            return wo.at[pl.ds(al(src * ROWS + (base + lo), 16), n), :]
+            return wo.at[src, pl.ds(base + lo, n), :]
 
         def second(o, off, part, mine=True):
             lo, n = part_of(part, size)
             src = sp_at(off, o) if h == 0 else sp_at(o, off)
-            return wo.at[pl.ds(al(src * ROWS + (base + lo), 16), n), :]
+            return wo.at[src, pl.ds(base + lo, n), :]
 
         return first, second
 
@@ -306,37 +316,35 @@
     tx_y.first(OWN)
     for d in (1, -1):
         lo, n = part_of(side(d), ROWS)
-        w_net.send(
-            ("tr", d), wst.at[wrap(y, 2), pl.ds(lo, n), :], transit.at[(1 - d) // 2], y_dev(d)
-        )
+        w_net.send("tr", wst.at[wrap(y, 2), pl.ds(lo, n), :], transit.at[(1 - d) // 2], y_dev(d))
     for d in (1, -1):
-        w_net.send(("w", d), wst.at[wrap(y, d)], win_ref(0, 0, "full"), y_dev(d))
+        w_net.send("w", wst.at[wrap(y, d)], win_ref(0, 0, "full"), y_dev(d))
     for d in (1, -1):
-        w_net.send(("wz", "T", 0, "full", d), wst.at[y], win_ref(0, 0, "full"), z_dev(d))
+        w_net.send("wz", wst.at[y], win_ref(0, 0, "full"), z_dev(d))
     win[pl.ds(al(s * ROWS, ROWS), ROWS), :] = wst[y]
     loaded("oa", "oc")
     o_first[1].first(OWN)
+    o_second[0].first(OWN)
+    loaded("taps", "cgain", "sink", "inner", "outer")
+    taps[...] = taps_ref[...].astype(F32)
+    gall[t] = jnp.broadcast_to(cgain_ref[...], (8, 256))
 
     tx_y.first_wait(OWN)
     tx_y.second((0,))
     tx_x.first(SIDES)
-    tx_x.give(spread(SIDES, (0,)))
+    tx_x.give(SIDES0)
+    w_net.wait("tr")
     for d in (1, -1):
-        lo, n = part_of(side(d), ROWS)
-        buf = transit.at[(1 - d) // 2]
-        w_net.wait(("tr", d), buf)
-        w_net.send(("trf", d), buf, win_ref(-d, 0, side(d)), y_dev(d))
+        w_net.send("trf", transit.at[(1 - d) // 2], win_ref(-d, 0, side(d)), y_dev(d))
     td_y.first(OWN)
-    for d in (1, -1):
-        w_net.wait(("w", d), win_ref(-d, 0, "full"))
+    w_net.wait("w")
     w_z.first(SIDES)
-    w_z.first_wait(OWN)
+    w_net.wait("wz")
     w_z.second((0,))
     tx_y.second_wait((0,))
     tx_x.first(FAR)
-    tx_x.give(spread(FAR, (0,)))
-    for d in (1, -1):
-        w_net.wait(("trf", d), win_ref(2, 0, side(d)))
+    tx_x.give(FAR0)
+    w_net.wait("trf")
     w_z.first(FAR)
     tx_x.first_wait(SIDES)
     tx_x.second((-1, 1))
@@ -345,43 +353,56 @@
     w_z.second((-1, 1))
     td_y.first_wait(OWN)
     td_y.second((0,))
-    td_p.give(((-1, 0, "full"), (1, 0, "full")))
+    td_p.give(SIDES0)
     o_first[0].first(OWN)
-    w_z.first_wait(FAR)
-    w_z.second((2,))
-    o_second[0].first(OWN)
     tx_x.first_wait(FAR)
     tx_x.second((2,))
     tx_x.give(spread(FAR, (1, -1)))
-
-    loaded("taps", "cgain", "sink", "inner", "outer")
-    taps[...] = taps_ref[...].astype(F32)
-
-    w_z.second_wait((0, -1, 1, 2))
+    o_first[1].first_wait(OWN)
+    o_first[1].second((0,))
+    o_second[1].first(OWN)
+    o_second[1].first(SIDES)
+    w_z.first_wait(FAR)
+    w_z.second((2,))
+    tx_x.second_wait((-1, 1))
+    tx_x.give(SIDES2)
+    o_first[0].first_wait(OWN)
+    o_first[0].second((0,))
+    o_second[0].first_wait(OWN)
+    o_second[0].second((0,))
+    o_second[0].first(SIDES)
+    td_y.second_wait((0,))
+    td_p.give(FAR0)
+    tx_x.second_wait((2,))
+    tx_x.give(FAR2)
 
     def project(o):
         rows = pl.ds(al(wrap(y, o) * ROWS, ROWS), ROWS)
         acc[rows, :] = jnp.dot(nrm[rows, :], win[...], preferred_element_type=F32)
 
+    w_z.second_wait((0,))
+    w_z.second_wait((-1, 1))
+    w_z.second_wait((2,))
     project(0)
-    tx_x.second_wait((-1, 1))
-    tx_x.give(((-1, 2, "lo"), (-1, 2, "hi"), (1, 2, "lo"), (1, 2, "hi")))
-    o_first[1].first_wait(OWN)
-    o_first[1].second((0,))
-    td_y.second_wait((0,))
-    td_p.give(((2, 0, "lo"), (2, 0, "hi")))
-    o_second[1].first(OWN)
-    tx_x.give_wait(spread(SIDES, (0, 1, -1)))
-    tx_x.give_wait(((-1, 2, "lo"), (-1, 2, "hi"), (1, 2, "lo"), (1, 2, "hi")))
-    td_p.give_wait(((-1, 0, "full"), (1, 0, "full")))
+    tx_x.give_wait(SIDES0)
+    tx_x.give_wait(spread(SIDES, (1, -1)))
+    tx_x.give_wait(SIDES2)
+    td_p.give_wait(SIDES0)
     project(-1)
     project(1)
-    tx_x.second_wait((2,))
-    tx_x.give(((2, 2, "lo"), (2, 2, "hi")))
-    tx_x.give_wait(spread(FAR, (0, 1, -1)))
-    tx_x.give_wait(((2, 2, "lo"), (2, 2, "hi")))
-    td_p.give_wait(((2, 0, "lo"), (2, 0, "hi")))
+    o_first[1].second_wait((0,))
+    o_second[1].first(FAR)
+    o_second[1].first_wait(OWN)
+    o_second[1].second((0,))
+    tx_x.give_wait(FAR0)
+    tx_x.give_wait(spread(FAR, (1, -1)))
+    tx_x.give_wait(FAR2)
+    td_p.give_wait(FAR0)
     project(2)
+    o_first[0].second_wait((0,))
+    o_second[0].first(FAR)
+    for i in range(1, 8):
+        g_net.send("gain", gall.at[t], gall.at[t], (s, lax.rem(t + i, 8)))
 
     def halo_copy(i, src, dst):
         return pltpu.make_async_remote_copy(
@@ -490,7 +511,7 @@
             f = jnp.zeros((64, 128), F32)
             for k in range(KSIZE):
                 f = f + taps[k : k + 1, :] * gext[r + 2 + k : r + 66 + k, :]
-            filt[r : r + 64, :] = f
+            mx[r : r + 64, :] = f.astype(BF16)
 
         for r in range(64, GROUP, 64):
             filter_rows(r)
@@ -498,118 +519,91 @@
         gext[0:32, :] = jnp.where(z > 0, ghalo[...].astype(F32), 0.0)
         filter_rows(0)
 
-        stat = jnp.zeros((ROWS, 128), F32)
-        for b in range(4):
-            f = filt[b * ROWS : (b + 1) * ROWS, :]
-            stat = jnp.where(lane == 2 * b, jnp.sum(f, axis=1, keepdims=True), stat)
-            stat = jnp.where(lane == 2 * b + 1, jnp.sum(f * f, axis=1, keepdims=True), stat)
-        stat_own[...] = stat.T[:8, :]
-        copies = []
-        for dy in (0, 1):
-            for i in range(8):
-                if dy == 0 and i == 0:
-                    continue
-                k = dy * 8 + i - 1
-                copy = pltpu.make_async_remote_copy(
-                    src_ref=stat_own,
-                    dst_ref=stat_all.at[k],
-                    send_sem=stat_send.at[k],
-                    recv_sem=stat_recv.at[k],
-                    device_id=(z * 4 + (y if dy == 0 else 5 - y), lax.rem(t + i, 8)),
-                    device_id_type=MESH,
-                )
-                copy.start()
-                copies.append(copy)
-        whole = stat_own[...]
-        for k, copy in enumerate(copies):
-            copy.wait_recv()
-            whole = whole + stat_all[k]
-        whole = jnp.concatenate([whole, jnp.zeros((120, ROWS), F32)], axis=0).T
-        for b in range(4):
-            rows = slice(b * ROWS, (b + 1) * ROWS)
-            mean_value = whole[:, 2 * b : 2 * b + 1] * (1.0 / CONV)
-            variance = whole[:, 2 * b + 1 : 2 * b + 2] * (1.0 / CONV) - mean_value * mean_value
-            scaled = (filt[rows, :] - mean_value) * lax.rsqrt(variance + 1e-05) * cgain_ref[...]
-            mx[rows, :] = (scaled / (1.0 + jnp.exp(-scaled))).astype(BF16)
-        for copy in copies:
-            copy.wait_send()
         halo.wait_send()
 
     pl.when(y < 2)(attention)
     pl.when(y >= 2)(convolution)
 
-    def mix_cols(o, off, mine=True):
-        yy = wrap(y, o)
-        block = 2 * tp_at(off, mine) + lax.rem(yy, 2)
-        return pl.ds(al(block * 256 + (yy // 2) * 128, 128), 128)
-
     def mix_ref(o, off, part, mine=True):
         lo, n = part_of(part, ROWS)
-        return mixall.at[pl.ds(lo, n), mix_cols(o, off, mine)]
+        yy = wrap(y, o)
+        cols = pl.ds(al(tp_at(off, mine) * 256 + lax.rem(yy, 2) * 128, 128), 128)
+        return mixall.at[yy // 2, pl.ds(lo, n), cols]
 
     m_x = Ring(m_net, "mx", mix_ref, x_dev)
     for d in (1, -1):
         lo, n = part_of(side(d), ROWS)
         src = mx.at[pl.ds(al(wrap(y, 2) * ROWS + lo, 128), n), :]
-        m_net.send(("tr", d), src, mtransit.at[(1 - d) // 2], y_dev(d))
+        m_net.send("tr", src, mtransit.at[(1 - d) // 2], y_dev(d))
     for d in (1, -1):
         src = mx.at[pl.ds(al(wrap(y, d) * ROWS, 128), ROWS), :]
-        m_net.send(("m", d), src, mix_ref(0, 0, "full"), y_dev(d))
-    mixall[:, mix_cols(0, 0)] = mx[pl.ds(al(y * ROWS, ROWS), ROWS), :]
+        m_net.send("m", src, mix_ref(0, 0, "full"), y_dev(d))
+    own_cols = pl.ds(al(t * 256 + lax.rem(y, 2) * 128, 128), 128)
+    mixall[y // 2, :, own_cols] = mx[pl.ds(al(y * ROWS, ROWS), ROWS), :]
     m_x.first(OWN)
-    m_x.give(spread(OWN, (0,)))
-
-    o_first[0].first_wait(OWN)
-    o_first[0].second((0,))
+    m_x.give(OWN0)
+    m_net.wait("tr")
     for d in (1, -1):
-        buf = mtransit.at[(1 - d) // 2]
-        m_net.wait(("tr", d), buf)
-        m_net.send(("trf", d), buf, mix_ref(-d, 0, side(d)), y_dev(d))
-    for d in (1, -1):
-        m_net.wait(("m", d), mix_ref(-d, 0, "full"))
+        m_net.send("trf", mtransit.at[(1 - d) // 2], mix_ref(-d, 0, side(d)), y_dev(d))
+    o_second[0].first_wait(SIDES)
+    o_second[0].second((-1, 1))
+    m_net.wait("m")
     m_x.first(SIDES)
-    m_x.give(spread(SIDES, (0,)))
-
-    for h in (0, 1):
-        o_second[h].first_wait(OWN)
-        o_second[h].second((0,))
-        o_second[h].first(SIDES)
-    for h in (0, 1):
-        o_first[h].second_wait((0,))
-        o_second[h].first(FAR)
+    m_x.give(SIDES0)
+    o_second[1].first_wait(SIDES)
+    o_second[1].second((-1, 1))
     m_x.first_wait(OWN)
     m_x.second((0,))
     m_x.give(spread(OWN, (1, -1)))
-    for d in (1, -1):
-        m_net.wait(("trf", d), mix_ref(2, 0, side(d)))
+    m_net.wait("trf")
     m_x.first(FAR)
-    m_x.give(spread(FAR, (0,)))
+    m_x.give(FAR0)
     m_x.first_wait(SIDES)
     m_x.second((-1, 1))
     m_x.give(spread(SIDES, (1, -1)))
-    for h in (0, 1):
-        o_second[h].first_wait(SIDES)
-        o_second[h].second((-1, 1))
+    o_second[1].first_wait(FAR)
+    o_second[1].second((2,))
+    o_second[0].first_wait(FAR)
+    o_second[0].second((2,))
+    m_x.second_wait((0,))
+    m_x.give(OWN2)
     m_x.first_wait(FAR)
     m_x.second((2,))
     m_x.give(spread(FAR, (1, -1)))
-    for h in (0, 1):
-        o_second[h].first_wait(FAR)
-        o_second[h].second((2,))
-    m_x.second_wait((0, -1, 1, 2))
-    last = tuple((o, 2, part) for o in (0, -1, 1, 2) for part in ("lo", "hi"))
-    m_x.give(last)
-    m_x.give_wait(spread(OWN + SIDES + FAR, (0, 1, -1)))
-    m_x.give_wait(last)
-    for h in (0, 1):
-        o_second[h].second_wait((0, -1, 1, 2))
+    m_x.second_wait((-1, 1))
+    m_x.give(SIDES2)
+    g_net.wait("gain")
+    for i in range(8):
+        gfull[:, i * 256 : (i + 1) * 256] = gall[i, 0:1, :]
+    m_x.second_wait((2,))
+    m_x.give(FAR2)
+    for items in (OWN0, spread(OWN, (1, -1)), OWN2, SIDES0, spread(SIDES, (1, -1)), SIDES2):
+        m_x.give_wait(items)
+    for items in (FAR0, spread(FAR, (1, -1)), FAR2):
+        m_x.give_wait(items)
+
+    def channel_norm(i, carry):
+        rows = pl.ds(al(i * 16, 16), 16)
+        f = mixall[1, rows, :].astype(F32)
+        mean_value = jnp.sum(f, axis=1, keepdims=True) * (1.0 / CONV)
+        variance = jnp.sum(f * f, axis=1, keepdims=True) * (1.0 / CONV) - mean_value * mean_value
+        scaled = (f - mean_value) * lax.rsqrt(variance + 1e-05) * gfull[...]
+        convn[rows, :] = (scaled / (1.0 + jnp.exp(-scaled))).astype(BF16)
+        return carry
+
+    lax.fori_loop(0, ROWS // 16, channel_norm, 0)
+    for ring in o_second:
+        for pieces in ((0,), (-1, 1), (2,)):
+            ring.second_wait(pieces)
 
     for c in range(0, OUTW, 256):
-        out_ref[:, c : c + 256] = jnp.dot(
-            mixall[...], wo[:, c : c + 256], preferred_element_type=F32
-        ).astype(BF16)
-
-    for net in (w_net, t_net, o_net, m_net):
+        w_attn = wo[:, 0:128, c : c + 256].reshape(2048, 256)
+        w_conv = wo[:, 128:256, c : c + 256].reshape(2048, 256)
+        v = jnp.dot(mixall[0], w_attn, preferred_element_type=F32)
+        v = v + jnp.dot(convn[...], w_conv, preferred_element_type=F32)
+        out_ref[:, c : c + 256] = v.astype(BF16)
+
+    for net in (w_net, t_net, o_net, m_net, g_net):
         net.drain()
 
 
@@ -642,7 +636,7 @@
             pltpu.VMEM((4, ROWS, WIDTH), BF16),
             pltpu.VMEM((2, 128, WIDTH), BF16),
             pltpu.VMEM((D, WIDTH), BF16),
-            pltpu.VMEM((D, OUTW), BF16),
+            pltpu.VMEM((16, ROWS, OUTW), BF16),
             pltpu.VMEM((ROWS, D), BF16),
             pltpu.VMEM((GROUP, D), BF16),
             pltpu.VMEM((GROUP, WIDTH), F32),
@@ -653,33 +647,33 @@
             pltpu.VMEM((32, 128), BF16),
             pltpu.VMEM((32, 128), BF16),
             pltpu.VMEM((GROUP + 32, 128), F32),
-            pltpu.VMEM((GROUP, 128), F32),
             pltpu.VMEM((128, ROWS), BF16),
             pltpu.VMEM((1, D), F32),
             pltpu.VMEM((1, 4), F32),
             pltpu.VMEM((KSIZE, 128), BF16),
-            pltpu.VMEM((1, 128), F32),
+            pltpu.VMEM((1, 256), F32),
+            pltpu.VMEM((8, 8, 256), F32),
+            pltpu.VMEM((1, 2048), F32),
             pltpu.VMEM((ROWS, 256), F32),
             pltpu.VMEM((4, 1, 256), F32),
             pltpu.VMEM((KSIZE, 128), F32),
-            pltpu.VMEM((8, ROWS), F32),
-            pltpu.VMEM((15, 8, ROWS), F32),
             pltpu.VMEM((GROUP, 128), BF16),
             pltpu.VMEM((2, 128, 128), BF16),
-            pltpu.VMEM((ROWS, D), BF16),
+            pltpu.VMEM((2, ROWS, 2048), BF16),
+            pltpu.VMEM((ROWS, 2048), BF16),
             dma((17,)),
+            dma((1,)),
             dma((SEMS,)),
+            dma((1,)),
             dma((SEMS,)),
+            dma((1,)),
             dma((SEMS,)),
+            dma((1,)),
             dma((SEMS,)),
-            dma((SEMS,)),
-            dma((SEMS,)),
-            dma((SEMS,)),
-            dma((SEMS,)),
+            dma((1,)),
+            dma((1,)),
             dma((2,)),
             dma((2,)),
-            dma((15,)),
-            dma((15,)),
         ],
         compiler_params=pltpu.CompilerParams(
             collective_id=0, has_side_effects=True, vmem_limit_bytes=67043328

time: 86.2 us -> 75.1 us (0.87)
  the two profiles are of different devices: /device:TPU:0 before, /device:TPU:1 now
where the time goes in v4:
time: 75.1 us; the launch traced here: 74.9 us
  Pallas kernels  73.2 us (97%)
  local copies, waits for them, and re-layouts  1.67 us (2%)
    pallas_call x1, Pallas kernels, per_device(): pl.pallas_call(kernel, name='mixer_layer', out_shape=jax.ShapeDtypeStruct...  73.2 us
    unnamed x1, local copies, waits for them, and re-layouts  1.67 us

profile of v4, /device:TPU:1, one launch (start us, length us, event | category | flops | bytes accessed | tf_op | source)
XLA Modules:
  0.0 74.9 jit_solution(2500779879440827761)
XLA Ops:
  0.0 73.2 %mixer_layer.1 = bf16[256,512]{1,0:T(8,128)(2,1)} custom-call(bf16[256,4096]{1,0:T(8,128)(2,1)} %tokens_hbm.1, f32[1,4096]{1,0:T(1,128)} %bitcast.7, bf16[256,256]{1,0:T(8,128)(2,1)} %wq_hbm.1, bf16[64,256]{1,0:T(8,128)(2,1)} %bitcast.5, bf16[64,256]{1,0:T(8,128)(2,1)} %bitcast.6, bf16[256,256]{1,0:T(8,128)(2,1)} %wglu_hbm.1, bf16[256,256]{1,0:T(8,128)(2,1)} %wgate_hbm.1, ...), custom_call_target="tpu_custom_call" | custom-call | tf_op jit(solution)/shard_map/mixer_layer/pallas_call | solution.py:629
  73.2 1.7 %copy.16 = bf16[256,512]{1,0:T(8,128)(2,1)} copy(bf16[256,512]{1,0:T(8,128)(2,1)} %mixer_layer.1) | data formatting | bytes 524288

commit v5 on v4

--- a/solution.py
+++ b/solution.py
@@ -22,7 +22,7 @@
 XCOLS = 384
 DCOLS = 512
 OUT_SPLIT = 160
-SEMS = 20
+SEMS = 26
 
 
 def rope_tables():
@@ -80,47 +80,53 @@
     def __init__(self, net, name, ref, device):
         self.net, self.name, self.ref, self.device = net, name, ref, device
 
-    def first(self, items):
-        for o, part in items:
-            for d in (1, -1):
+    def first(self, *groups):
+        for sends in groups:
+            for o, part, d in sends:
                 r = self.ref(o, 0, part)
-                self.net.send((self.name, "T", items), r, r, self.device(d))
-
-    def first_wait(self, items):
-        self.net.wait((self.name, "T", items))
-
-    def second(self, pieces):
-        for o in pieces:
-            for d in (1, -1):
+                self.net.send((self.name, "T", sends), r, r, self.device(d))
+
+    def first_wait(self, *groups):
+        for sends in groups:
+            self.net.wait((self.name, "T", sends))
+
+    def second(self, *groups):
+        for sends in groups:
+            for o, d in sends:
                 r = self.ref(o, -d, side(d))
-                self.net.send((self.name, "F", pieces), r, r, self.device(d))
-
-    def second_wait(self, pieces):
-        self.net.wait((self.name, "F", pieces))
-
-    def give(self, items):
-        for o, off, part in items:
-            r = self.ref(o, off, part)
-            self.net.send((self.name, "P", items), r, r, self.net.partner)
-
-    def give_wait(self, items):
-        self.net.wait((self.name, "P", items))
-
-
-OWN = ((0, "full"),)
-SIDES = ((-1, "full"), (1, "full"))
-FAR = ((2, "lo"), (2, "hi"))
-
-
-def spread(items, offs):
-    return tuple((o, off, part) for o, part in items for off in offs)
-
-
-HALVES = ("lo", "hi")
-OWN0, SIDES0, FAR0 = spread(OWN, (0,)), spread(SIDES, (0,)), spread(FAR, (0,))
-OWN2 = tuple((0, 2, part) for part in HALVES)
-SIDES2 = tuple((o, 2, part) for o in (-1, 1) for part in HALVES)
-FAR2 = tuple((2, 2, part) for part in HALVES)
+                self.net.send((self.name, "F", sends), r, r, self.device(d))
+
+    def second_wait(self, *groups):
+        for sends in groups:
+            self.net.wait((self.name, "F", sends))
+
+    def give(self, *groups):
+        for items in groups:
+            for o, off in items:
+                r = self.ref(o, off, "full")
+                self.net.send((self.name, "P", items), r, r, self.net.partner)
+
+    def give_wait(self, *groups):
+        for items in groups:
+            self.net.wait((self.name, "P", items))
+
+
+def both(*items):
+    return tuple((o, part, d) for o, part in items for d in (1, -1))
+
+
+OWN_A = ((0, "lo", 1), (0, "hi", -1))
+OWN_B = ((0, "hi", 1), (0, "lo", -1))
+SIDES_A = both((-1, "lo"), (1, "hi"))
+SIDES_B = both((-1, "hi"), (1, "lo"))
+FAR = both((2, "lo"), (2, "hi"))
+OWN_F = ((0, 1), (0, -1))
+SIDES_AF = ((-1, 1), (1, -1))
+SIDES_BF = ((-1, -1), (1, 1))
+FAR_F = ((2, 1), (2, -1))
+OWN0, OWN1, OWN2 = ((0, 0),), ((0, 1), (0, -1)), ((0, 2),)
+SIDES0, SIDES1, SIDES2 = ((-1, 0), (1, 0)), ((-1, 1), (-1, -1), (1, 1), (1, -1)), ((-1, 2), (1, 2))
+FAR0, FAR1, FAR2 = ((2, 0),), ((2, 1), (2, -1)), ((2, 2),)
 
 
 def kernel(
@@ -313,93 +319,110 @@
         o_first.append(Ring(o_net, ("of", h), f, (y_dev, z_dev)[h]))
         o_second.append(Ring(o_net, ("os", h), g, (z_dev, y_dev)[h]))
 
-    tx_y.first(OWN)
+    def w_first(name, parts):
+        for d, part in zip((1, -1), parts):
+            lo, n = part_of(part, ROWS)
+            src = wst.at[wrap(y, d), pl.ds(lo, n), :]
+            w_net.send(name, src, win_ref(0, 0, part), y_dev(d))
+
+    tx_y.first(OWN_A)
     for d in (1, -1):
         lo, n = part_of(side(d), ROWS)
         w_net.send("tr", wst.at[wrap(y, 2), pl.ds(lo, n), :], transit.at[(1 - d) // 2], y_dev(d))
-    for d in (1, -1):
-        w_net.send("w", wst.at[wrap(y, d)], win_ref(0, 0, "full"), y_dev(d))
-    for d in (1, -1):
-        w_net.send("wz", wst.at[y], win_ref(0, 0, "full"), z_dev(d))
+    tx_y.first(OWN_B)
+    for name, sends in (("wz_a", OWN_A), ("wz_b", OWN_B)):
+        for o, part, d in sends:
+            lo, n = part_of(part, ROWS)
+            w_net.send(name, wst.at[y, pl.ds(lo, n), :], win_ref(0, 0, part), z_dev(d))
     win[pl.ds(al(s * ROWS, ROWS), ROWS), :] = wst[y]
     loaded("oa", "oc")
-    o_first[1].first(OWN)
-    o_second[0].first(OWN)
+    o_first[1].first(OWN_A, OWN_B)
+    o_second[0].first(OWN_A, OWN_B)
+
+    tx_y.first_wait(OWN_A)
+    tx_y.second(OWN_F)
+    tx_x.first(SIDES_A)
+    w_first("w_a", ("lo", "hi"))
+    w_first("w_b", ("hi", "lo"))
+    w_net.wait("tr")
+    for d in (1, -1):
+        w_net.send("trf", transit.at[(1 - d) // 2], win_ref(-d, 0, side(d)), y_dev(d))
+    td_y.first(OWN_A, OWN_B)
+    tx_y.first_wait(OWN_B)
+    tx_x.first(SIDES_B)
+    tx_x.give(SIDES0)
     loaded("taps", "cgain", "sink", "inner", "outer")
     taps[...] = taps_ref[...].astype(F32)
     gall[t] = jnp.broadcast_to(cgain_ref[...], (8, 256))
-
-    tx_y.first_wait(OWN)
-    tx_y.second((0,))
-    tx_x.first(SIDES)
-    tx_x.give(SIDES0)
-    w_net.wait("tr")
-    for d in (1, -1):
-        w_net.send("trf", transit.at[(1 - d) // 2], win_ref(-d, 0, side(d)), y_dev(d))
-    td_y.first(OWN)
-    w_net.wait("w")
-    w_z.first(SIDES)
-    w_net.wait("wz")
-    w_z.second((0,))
-    tx_y.second_wait((0,))
+    w_net.wait("wz_a")
+    w_z.second(OWN_F)
+    tx_y.second_wait(OWN_F)
+    tx_x.first_wait(SIDES_A)
+    tx_x.second(SIDES_AF)
     tx_x.first(FAR)
     tx_x.give(FAR0)
+    w_net.wait("w_a")
+    w_z.first(SIDES_A)
+    w_net.wait("w_b")
+    w_z.first(SIDES_B)
     w_net.wait("trf")
     w_z.first(FAR)
-    tx_x.first_wait(SIDES)
-    tx_x.second((-1, 1))
-    tx_x.give(spread(SIDES, (1, -1)))
-    w_z.first_wait(SIDES)
-    w_z.second((-1, 1))
-    td_y.first_wait(OWN)
-    td_y.second((0,))
+    tx_x.first_wait(SIDES_B)
+    tx_x.second(SIDES_BF)
+    tx_x.give(SIDES1)
+    w_net.wait("wz_b")
+    td_y.first_wait(OWN_A)
+    td_y.second(OWN_F)
+    o_first[0].first(OWN_A, OWN_B)
+    w_z.first_wait(SIDES_A)
+    w_z.second(SIDES_AF)
+    o_first[1].first_wait(OWN_A)
+    o_first[1].second(OWN_F)
+    w_z.first_wait(SIDES_B)
+    w_z.second(SIDES_BF)
+    tx_x.first_wait(FAR)
+    tx_x.second(FAR_F)
+    tx_x.give(FAR1)
+    td_y.first_wait(OWN_B)
     td_p.give(SIDES0)
-    o_first[0].first(OWN)
-    tx_x.first_wait(FAR)
-    tx_x.second((2,))
-    tx_x.give(spread(FAR, (1, -1)))
-    o_first[1].first_wait(OWN)
-    o_first[1].second((0,))
-    o_second[1].first(OWN)
-    o_second[1].first(SIDES)
+    o_first[1].first_wait(OWN_B)
+    o_second[1].first(OWN_A, OWN_B, SIDES_A, SIDES_B)
     w_z.first_wait(FAR)
-    w_z.second((2,))
-    tx_x.second_wait((-1, 1))
+    w_z.second(FAR_F)
+    o_second[0].first_wait(OWN_A)
+    o_second[0].second(OWN_F)
+    o_second[0].first_wait(OWN_B)
+    tx_x.second_wait(SIDES_AF, SIDES_BF)
     tx_x.give(SIDES2)
-    o_first[0].first_wait(OWN)
-    o_first[0].second((0,))
-    o_second[0].first_wait(OWN)
-    o_second[0].second((0,))
-    o_second[0].first(SIDES)
-    td_y.second_wait((0,))
+    td_y.second_wait(OWN_F)
     td_p.give(FAR0)
-    tx_x.second_wait((2,))
+    o_first[0].first_wait(OWN_A)
+    o_first[0].second(OWN_F)
+    o_second[0].first(SIDES_A)
+    tx_x.second_wait(FAR_F)
     tx_x.give(FAR2)
+    o_first[0].first_wait(OWN_B)
+    o_second[0].first(SIDES_B)
 
     def project(o):
         rows = pl.ds(al(wrap(y, o) * ROWS, ROWS), ROWS)
         acc[rows, :] = jnp.dot(nrm[rows, :], win[...], preferred_element_type=F32)
 
-    w_z.second_wait((0,))
-    w_z.second_wait((-1, 1))
-    w_z.second_wait((2,))
+    w_z.second_wait(OWN_F, SIDES_AF, SIDES_BF, FAR_F)
     project(0)
-    tx_x.give_wait(SIDES0)
-    tx_x.give_wait(spread(SIDES, (1, -1)))
-    tx_x.give_wait(SIDES2)
+    tx_x.give_wait(SIDES0, SIDES1, SIDES2)
     td_p.give_wait(SIDES0)
     project(-1)
     project(1)
-    o_first[1].second_wait((0,))
-    o_second[1].first(FAR)
-    o_second[1].first_wait(OWN)
-    o_second[1].second((0,))
-    tx_x.give_wait(FAR0)
-    tx_x.give_wait(spread(FAR, (1, -1)))
-    tx_x.give_wait(FAR2)
+    tx_x.give_wait(FAR0, FAR1, FAR2)
     td_p.give_wait(FAR0)
     project(2)
-    o_first[0].second_wait((0,))
+    o_first[1].second_wait(OWN_F)
+    o_second[1].first(FAR)
+    o_second[1].first_wait(OWN_A)
+    o_second[1].second(OWN_F)
+    o_second[1].first_wait(OWN_B)
+    o_first[0].second_wait(OWN_F)
     o_second[0].first(FAR)
     for i in range(1, 8):
         g_net.send("gain", gall.at[t], gall.at[t], (s, lax.rem(t + i, 8)))
@@ -531,56 +554,65 @@
         return mixall.at[yy // 2, pl.ds(lo, n), cols]
 
     m_x = Ring(m_net, "mx", mix_ref, x_dev)
-    for d in (1, -1):
-        lo, n = part_of(side(d), ROWS)
-        src = mx.at[pl.ds(al(wrap(y, 2) * ROWS + lo, 128), n), :]
-        m_net.send("tr", src, mtransit.at[(1 - d) // 2], y_dev(d))
-    for d in (1, -1):
-        src = mx.at[pl.ds(al(wrap(y, d) * ROWS, 128), ROWS), :]
-        m_net.send("m", src, mix_ref(0, 0, "full"), y_dev(d))
     own_cols = pl.ds(al(t * 256 + lax.rem(y, 2) * 128, 128), 128)
     mixall[y // 2, :, own_cols] = mx[pl.ds(al(y * ROWS, ROWS), ROWS), :]
-    m_x.first(OWN)
+
+    def m_rows(o, part):
+        lo, n = part_of(part, ROWS)
+        return mx.at[pl.ds(al(wrap(y, o) * ROWS + lo, 128), n), :]
+
+    for d in (1, -1):
+        m_net.send("tr", m_rows(2, side(d)), mtransit.at[(1 - d) // 2], y_dev(d))
+    for name, parts in (("m_a", ("lo", "hi")), ("m_b", ("hi", "lo"))):
+        for d, part in zip((1, -1), parts):
+            m_net.send(name, m_rows(d, part), mix_ref(0, 0, part), y_dev(d))
+    m_x.first(OWN_A, OWN_B)
     m_x.give(OWN0)
     m_net.wait("tr")
     for d in (1, -1):
         m_net.send("trf", mtransit.at[(1 - d) // 2], mix_ref(-d, 0, side(d)), y_dev(d))
-    o_second[0].first_wait(SIDES)
-    o_second[0].second((-1, 1))
-    m_net.wait("m")
-    m_x.first(SIDES)
+    m_net.wait("m_a")
+    m_x.first(SIDES_A)
+    m_net.wait("m_b")
+    m_x.first(SIDES_B)
     m_x.give(SIDES0)
-    o_second[1].first_wait(SIDES)
-    o_second[1].second((-1, 1))
-    m_x.first_wait(OWN)
-    m_x.second((0,))
-    m_x.give(spread(OWN, (1, -1)))
+    o_second[0].first_wait(SIDES_A)
+    o_second[0].second(SIDES_AF)
+    o_second[1].first_wait(SIDES_A)
+    o_second[1].second(SIDES_AF)
+    m_x.first_wait(OWN_A)
+    m_x.second(OWN_F)
+    m_x.first_wait(OWN_B)
+    m_x.give(OWN1)
     m_net.wait("trf")
     m_x.first(FAR)
     m_x.give(FAR0)
-    m_x.first_wait(SIDES)
-    m_x.second((-1, 1))
-    m_x.give(spread(SIDES, (1, -1)))
+    o_second[0].first_wait(SIDES_B)
+    o_second[0].second(SIDES_BF)
+    o_second[1].first_wait(SIDES_B)
+    o_second[1].second(SIDES_BF)
+    m_x.first_wait(SIDES_A)
+    m_x.second(SIDES_AF)
+    m_x.first_wait(SIDES_B)
+    m_x.second(SIDES_BF)
+    m_x.give(SIDES1)
+    m_x.second_wait(OWN_F)
+    m_x.give(OWN2)
     o_second[1].first_wait(FAR)
-    o_second[1].second((2,))
+    o_second[1].second(FAR_F)
+    m_x.first_wait(FAR)
+    m_x.second(FAR_F)
+    m_x.give(FAR1)
     o_second[0].first_wait(FAR)
-    o_second[0].second((2,))
-    m_x.second_wait((0,))
-    m_x.give(OWN2)
-    m_x.first_wait(FAR)
-    m_x.second((2,))
-    m_x.give(spread(FAR, (1, -1)))
-    m_x.second_wait((-1, 1))
+    o_second[0].second(FAR_F)
+    m_x.second_wait(SIDES_AF, SIDES_BF)
     m_x.give(SIDES2)
     g_net.wait("gain")
     for i in range(8):
         gfull[:, i * 256 : (i + 1) * 256] = gall[i, 0:1, :]
-    m_x.second_wait((2,))
+    m_x.second_wait(FAR_F)
     m_x.give(FAR2)
-    for items in (OWN0, spread(OWN, (1, -1)), OWN2, SIDES0, spread(SIDES, (1, -1)), SIDES2):
-        m_x.give_wait(items)
-    for items in (FAR0, spread(FAR, (1, -1)), FAR2):
-        m_x.give_wait(items)
+    m_x.give_wait(OWN0, OWN1, OWN2, SIDES0, SIDES1, SIDES2, FAR0, FAR1, FAR2)
 
     def channel_norm(i, carry):
         rows = pl.ds(al(i * 16, 16), 16)
@@ -593,8 +625,7 @@
 
     lax.fori_loop(0, ROWS // 16, channel_norm, 0)
     for ring in o_second:
-        for pieces in ((0,), (-1, 1), (2,)):
-            ring.second_wait(pieces)
+        ring.second_wait(OWN_F, SIDES_AF, SIDES_BF, FAR_F)
 
     for c in range(0, OUTW, 256):
         w_attn = wo[:, 0:128, c : c + 256].reshape(2048, 256)

time: 75.1 us -> 73.4 us (0.977)
  Pallas kernels: 73.2 us -> 71.5 us
    pallas_call x1, Pallas kernels: 73.2 us -> 71.5 us  [per_device(): pl.pallas_call(kernel, name='mixer_layer', out_shape=jax.ShapeDtypeStruct...]
where the time goes in v5:
time: 73.4 us; the launch traced here: 73.2 us
  Pallas kernels  71.5 us (97%)
  local copies, waits for them, and re-layouts  1.67 us (2%)
    pallas_call x1, Pallas kernels, per_device(): pl.pallas_call(kernel, name='mixer_layer', out_shape=jax.ShapeDtypeStruct...  71.5 us
    unnamed x1, local copies, waits for them, and re-layouts  1.67 us

profile of v5, /device:TPU:1, one launch (start us, length us, event | category | flops | bytes accessed | tf_op | source)
XLA Modules:
  0.0 73.2 jit_solution(2338735618238808599)
XLA Ops:
  0.0 71.5 %mixer_layer.1 = bf16[256,512]{1,0:T(8,128)(2,1)} custom-call(bf16[256,4096]{1,0:T(8,128)(2,1)} %tokens_hbm.1, f32[1,4096]{1,0:T(1,128)} %bitcast.7, bf16[256,256]{1,0:T(8,128)(2,1)} %wq_hbm.1, bf16[64,256]{1,0:T(8,128)(2,1)} %bitcast.5, bf16[64,256]{1,0:T(8,128)(2,1)} %bitcast.6, bf16[256,256]{1,0:T(8,128)(2,1)} %wglu_hbm.1, bf16[256,256]{1,0:T(8,128)(2,1)} %wgate_hbm.1, ...), custom_call_target="tpu_custom_call" | custom-call | tf_op jit(solution)/shard_map/mixer_layer/pallas_call | solution.py:660
  71.5 1.7 %copy.16 = bf16[256,512]{1,0:T(8,128)(2,1)} copy(bf16[256,512]{1,0:T(8,128)(2,1)} %mixer_layer.1) | data formatting | bytes 524288

commit v6 on v5

--- a/solution.py
+++ b/solution.py
@@ -150,7 +150,9 @@
     win,
     wo,
     tok,
-    nrm,
+    nrmx,
+    nrmd,
+    meter,
     acc,
     qbuf,
     kvext,
@@ -170,7 +172,6 @@
     outer,
     taps,
     mx,
-    mtransit,
     mixall,
     convn,
     local_sem,
@@ -218,12 +219,12 @@
         ("gain", gain_hbm, gain_ref),
         ("wk", wk_hbm, kvt.at[0:64, :]),
         ("wv", wv_hbm, kvt.at[64:128, :]),
-        ("q0", wq_hbm.at[:, 0:128], wst.at[0, :, 0:128]),
-        ("q1", wq_hbm.at[:, 128:256], wst.at[1, :, 0:128]),
-        ("glu0", wglu_hbm.at[:, 0:128], wst.at[2, :, 0:128]),
-        ("glu1", wglu_hbm.at[:, 128:256], wst.at[3, :, 0:128]),
-        ("gate0", wgate_hbm.at[:, 0:128], wst.at[2, :, 128:256]),
-        ("gate1", wgate_hbm.at[:, 128:256], wst.at[3, :, 128:256]),
+        ("q0", wq_hbm.at[:, 0:128], wst.at[2, :, 0:128]),
+        ("q1", wq_hbm.at[:, 128:256], wst.at[3, :, 0:128]),
+        ("glu0", wglu_hbm.at[:, 0:128], wst.at[0, :, 0:128]),
+        ("glu1", wglu_hbm.at[:, 128:256], wst.at[1, :, 0:128]),
+        ("gate0", wgate_hbm.at[:, 0:128], wst.at[0, :, 128:256]),
+        ("gate1", wgate_hbm.at[:, 128:256], wst.at[1, :, 128:256]),
         ("oa", oa_hbm, wo.at[s, 0:128, :]),
         ("oc", oc_hbm, wo.at[s, 128:256, :]),
         ("taps", taps_hbm.at[:, role_half], taps_ref),
@@ -242,25 +243,30 @@
 
     loaded("wk", "wv")
     kv_t = kvt[...].astype(F32).T.astype(BF16)
-    wst[0, :, 128:256] = kv_t
-    wst[1, :, 128:256] = kv_t
+    wst[2, :, 128:256] = kv_t
+    wst[3, :, 128:256] = kv_t
     loaded("tok", "gain")
 
     def norm_rows(i, carry):
         v = tok[pl.ds(al(i * 16, 16), 16), :].astype(F32)
         scale = lax.rsqrt(jnp.mean(v * v, axis=1, keepdims=True) + 1e-06)
-        nrm[pl.ds(al(y * ROWS + i * 16, 16), 16), :] = (v * scale * gain_ref[...]).astype(BF16)
+        v = (v * scale * gain_ref[...]).astype(BF16)
+        rows = pl.ds(al(y * ROWS + i * 16, 16), 16)
+        for c in range(8):
+            nrmx[c, rows, :] = v[:, c * XCOLS : (c + 1) * XCOLS]
+        for c in range(2):
+            nrmd[c, rows, :] = v[:, 8 * XCOLS + c * DCOLS : 8 * XCOLS + (c + 1) * DCOLS]
         return carry
 
     lax.fori_loop(0, ROWS // 16, norm_rows, 0)
     loaded("q0", "q1", "glu0", "glu1", "gate0", "gate1")
     pl.semaphore_wait(barrier, len(peers))
 
-    w_net = Net(w_send, w_recv, nrm, partner)
-    t_net = Net(t_send, t_recv, nrm, partner)
-    o_net = Net(o_send, o_recv, nrm, partner)
-    m_net = Net(m_send, m_recv, nrm, partner)
-    g_net = Net(g_send, g_recv, nrm, partner)
+    w_net = Net(w_send, w_recv, meter, partner)
+    t_net = Net(t_send, t_recv, meter, partner)
+    o_net = Net(o_send, o_recv, meter, partner)
+    m_net = Net(m_send, m_recv, meter, partner)
+    g_net = Net(g_send, g_recv, meter, partner)
 
     def y_dev(d):
         return (sp_at(0, d), t)
@@ -283,11 +289,10 @@
         return pl.ds(al(wrap(y, o) * ROWS + lo, 128), n)
 
     def tokx_ref(o, off, part, mine=True):
-        return nrm.at[tok_rows(o, part), pl.ds(al(tp_at(off, mine) * XCOLS, 128), XCOLS)]
+        return nrmx.at[tp_at(off, mine), tok_rows(o, part), :]
 
     def tokd_ref(o, off, part, mine=True):
-        c = core if mine else 1 - core
-        return nrm.at[tok_rows(o, part), pl.ds(al(8 * XCOLS + c * DCOLS, 128), DCOLS)]
+        return nrmd.at[core if mine else 1 - core, tok_rows(o, part), :]
 
     def along_y(ref):
         return lambda o, off, part, mine=True: ref(off, 0, part, mine)
@@ -399,14 +404,180 @@
     o_first[0].first_wait(OWN_A)
     o_first[0].second(OWN_F)
     o_second[0].first(SIDES_A)
-    tx_x.second_wait(FAR_F)
-    tx_x.give(FAR2)
-    o_first[0].first_wait(OWN_B)
-    o_second[0].first(SIDES_B)
 
     def project(o):
         rows = pl.ds(al(wrap(y, o) * ROWS, ROWS), ROWS)
-        acc[rows, :] = jnp.dot(nrm[rows, :], win[...], preferred_element_type=F32)
+        parts = [nrmx[c, rows, :] for c in range(8)] + [nrmd[c, rows, :] for c in range(2)]
+        whole = jnp.concatenate(parts, axis=1)
+        acc[rows, :] = jnp.dot(whole, win[...], preferred_element_type=F32)
+
+    def halo_copy(src, dst):
+        return pltpu.make_async_remote_copy(
+            src_ref=src,
+            dst_ref=dst,
+            send_sem=halo_send.at[0],
+            recv_sem=halo_recv.at[0],
+            device_id=z_dev(1),
+            device_id_type=MESH,
+        )
+
+    lane = lax.broadcasted_iota(jnp.int32, (ROWS, 128), 1)
+    first = lax.rem(lane, 64) < 32
+    low = lane < 64
+    low_w = low[:WINDOW, :]
+    kv_halo = halo_copy(kvext.at[pl.ds(GROUP, WINDOW), :], kvext.at[pl.ds(0, WINDOW), :])
+    gate_halo = halo_copy(gtail, ghalo)
+
+    def rotate(v, cosine, sine):
+        other = jnp.where(first, pltpu.roll(v, 96, 1), pltpu.roll(v, 32, 1))
+        return v * cosine + other * sine
+
+    def fill(b):
+        rows = slice(b * ROWS, (b + 1) * ROWS)
+        ext = slice(b * ROWS + WINDOW, (b + 1) * ROWS + WINDOW)
+        edge = outer[b]
+        co, so = edge[:, 0:128], edge[:, 128:256]
+        cosine = co * inner[:, 0:128] - so * inner[:, 128:256]
+        sine = so * inner[:, 0:128] + co * inner[:, 128:256]
+        sine = jnp.where(first, -sine, sine)
+        q = rotate(acc[rows, 0:128], cosine, sine).astype(BF16).astype(F32)
+        qbuf[rows, :] = (q * 0.125).astype(BF16)
+        kv = rotate(acc[rows, 128:256], jnp.where(low, cosine, 1.0), jnp.where(low, sine, 0.0))
+        kv = kv.astype(BF16)
+        kvext[ext, :] = kv
+        kv = kv.astype(F32)
+        swapped = pltpu.roll(kv, 64, 1)
+        keys[ext, :] = jnp.where(low, kv, swapped).astype(BF16)
+        vals[ext, :] = jnp.where(low, swapped, kv).astype(BF16)
+
+    def attend(role, b):
+        zero = jnp.zeros((WINDOW, 128), BF16)
+        second = lax.broadcasted_iota(jnp.int32, (2 * WINDOW, 1), 0) >= WINDOW
+        i = 2 * (role - 2)
+        sink = jnp.where(second, sink_ref[0:1, i + 1 : i + 2], sink_ref[0:1, i : i + 1])
+        row_i = lax.rem(lax.broadcasted_iota(jnp.int32, (2 * WINDOW, 2 * WINDOW), 0), WINDOW)
+        col_j = lax.broadcasted_iota(jnp.int32, (2 * WINDOW, 2 * WINDOW), 1)
+        distance = row_i + WINDOW - col_j
+        near = (distance >= 0) & (distance < WINDOW)
+        if b == 0:
+            near = near & (z * GROUP - WINDOW + col_j >= 0)
+        q = qbuf[b * WINDOW : (b + 1) * WINDOW, :]
+        stacked = jnp.concatenate([jnp.where(low_w, q, zero), jnp.where(low_w, zero, q)], axis=0)
+        scores = lax.dot_general(
+            stacked,
+            keys[b * WINDOW : (b + 2) * WINDOW, :],
+            (((1,), (1,)), ((), ())),
+            preferred_element_type=F32,
+        )
+        scores = jnp.where(near, scores, -1e30)
+        top = jnp.maximum(jnp.max(scores, axis=1, keepdims=True), sink)
+        e = jnp.exp(scores - top)
+        denom = jnp.sum(e, axis=1, keepdims=True) + jnp.exp(sink - top)
+        probs = (e * (1.0 / denom)).astype(BF16)
+        att = jnp.dot(probs, vals[b * WINDOW : (b + 2) * WINDOW, :], preferred_element_type=F32)
+        mx[b * WINDOW : (b + 1) * WINDOW, :] = jnp.where(
+            low_w, att[:WINDOW, :], att[WINDOW:, :]
+        ).astype(BF16)
+
+    def late_windows(far):
+        return [(2 * far + i) % 8 for i in range(3)]
+
+    def attend_first(role):
+        kv_halo.wait_recv()
+        edge = kvext[0:WINDOW, :].astype(F32)
+        swapped = pltpu.roll(edge, 64, 1)
+        keys[0:WINDOW, :] = jnp.where(low_w, edge, swapped).astype(BF16)
+        vals[0:WINDOW, :] = jnp.where(low_w, swapped, edge).astype(BF16)
+        attend(role, 0)
+        kv_halo.wait_send()
+
+    def attend_early(role):
+        far = (role + 2) % 4
+        fill(3)
+        kv_halo.start()
+        for b in range(3):
+            if b != far:
+                fill(b)
+        for b in range(7, 0, -1):
+            if b not in late_windows(far):
+                attend(role, b)
+        if 0 not in late_windows(far):
+            attend_first(role)
+
+    def attend_late(role):
+        far = (role + 2) % 4
+        fill(far)
+        for b in range(7, 0, -1):
+            if b in late_windows(far):
+                attend(role, b)
+        if 0 in late_windows(far):
+            attend_first(role)
+
+    def gate_rows(b):
+        rows = slice(b * ROWS, (b + 1) * ROWS)
+        g = acc[rows, 0:128] * (0.5 + 0.5 * jnp.tanh(0.5 * acc[rows, 128:256]))
+        gext[b * ROWS + 32 : (b + 1) * ROWS + 32, :] = g.astype(BF16).astype(F32)
+
+    def send_tail():
+        gtail[...] = gext[GROUP : GROUP + 32, :].astype(BF16)
+        gate_halo.start()
+
+    def filter_rows(r):
+        f = jnp.zeros((64, 128), F32)
+        for k in range(KSIZE):
+            f = f + taps[k : k + 1, :] * gext[r + 2 + k : r + 66 + k, :]
+        mx[r : r + 64, :] = f.astype(BF16)
+
+    def late_rows(far):
+        return [(far * ROWS + i * 64) % GROUP for i in range(5)]
+
+    def filter_first():
+        gate_halo.wait_recv()
+        gext[0:32, :] = jnp.where(z > 0, ghalo[...].astype(F32), 0.0)
+        filter_rows(0)
+        gate_halo.wait_send()
+
+    def filter_early(role):
+        far = (role + 2) % 4
+        for b in (3, 0, 1, 2):
+            if b != far:
+                gate_rows(b)
+                if b == 3:
+                    send_tail()
+        for r in range(64, GROUP, 64):
+            if r not in late_rows(far):
+                filter_rows(r)
+        if 0 not in late_rows(far):
+            filter_first()
+
+    def filter_late(role):
+        far = (role + 2) % 4
+        gate_rows(far)
+        if far == 3:
+            send_tail()
+        for r in range(64, GROUP, 64):
+            if r in late_rows(far):
+                filter_rows(r)
+        if 0 in late_rows(far):
+            filter_first()
+
+    def by_role(conv, attention):
+        for role in range(4):
+            pl.when(y == role)(lambda role=role: (conv if role < 2 else attention)(role))
+
+    def mix_ref(o, off, part, mine=True):
+        lo, n = part_of(part, ROWS)
+        yy = wrap(y, o)
+        cols = pl.ds(al(tp_at(off, mine) * 256 + lax.rem(yy, 2) * 128, 128), 128)
+        return mixall.at[yy // 2, pl.ds(lo, n), cols]
+
+    m_x = Ring(m_net, "mx", mix_ref, x_dev)
+    own_cols = pl.ds(al(t * 256 + lax.rem(y, 2) * 128, 128), 128)
+
+    def m_send(name, o, part):
+        lo, n = part_of(part, ROWS)
+        src = mx.at[pl.ds(al(wrap(y, o) * ROWS + lo, 128), n), :]
+        m_net.send(name, src, mix_ref(0, 0, part), y_dev(o))
 
     w_z.second_wait(OWN_F, SIDES_AF, SIDES_BF, FAR_F)
     project(0)
@@ -414,9 +585,19 @@
     td_p.give_wait(SIDES0)
     project(-1)
     project(1)
+    tx_x.second_wait(FAR_F)
+    tx_x.give(FAR2)
+    o_first[0].first_wait(OWN_B)
+    o_second[0].first(SIDES_B)
+    by_role(filter_early, attend_early)
+    m_send("m_a", 1, "lo")
+    m_send("m_a", -1, "hi")
     tx_x.give_wait(FAR0, FAR1, FAR2)
     td_p.give_wait(FAR0)
     project(2)
+    mixall[y // 2, :, own_cols] = mx[pl.ds(al(y * ROWS, ROWS), ROWS), :]
+    m_x.first(OWN_A, OWN_B)
+    m_x.give(OWN0)
     o_first[1].second_wait(OWN_F)
     o_second[1].first(FAR)
     o_second[1].first_wait(OWN_A)
@@ -426,211 +607,70 @@
     o_second[0].first(FAR)
     for i in range(1, 8):
         g_net.send("gain", gall.at[t], gall.at[t], (s, lax.rem(t + i, 8)))
-
-    def halo_copy(i, src, dst):
-        return pltpu.make_async_remote_copy(
-            src_ref=src,
-            dst_ref=dst,
-            send_sem=halo_send.at[i],
-            recv_sem=halo_recv.at[i],
-            device_id=z_dev(1),
-            device_id_type=MESH,
-        )
-
-    lane = lax.broadcasted_iota(jnp.int32, (ROWS, 128), 1)
-
-    def attention():
-        first = lax.rem(lane, 64) < 32
-        low = lane < 64
-
-        def rotate(v, cosine, sine):
-            other = jnp.where(first, pltpu.roll(v, 96, 1), pltpu.roll(v, 32, 1))
-            return v * cosine + other * sine
-
-        def fill(b, carry):
-            rows = pl.ds(al(b * ROWS, ROWS), ROWS)
-            ext = pl.ds(al(b * ROWS + WINDOW, WINDOW), ROWS)
-            edge = outer[b]
-            co, so = edge[:, 0:128], edge[:, 128:256]
-            cosine = co * inner[:, 0:128] - so * inner[:, 128:256]
-            sine = so * inner[:, 0:128] + co * inner[:, 128:256]
-            sine = jnp.where(first, -sine, sine)
-            qbuf[rows, :] = rotate(acc[rows, 0:128], cosine, sine).astype(BF16)
-            kv = rotate(
-                acc[rows, 128:256], jnp.where(low, cosine, 1.0), jnp.where(low, sine, 0.0)
-            )
-            kv = kv.astype(BF16)
-            kvext[ext, :] = kv
-            kv = kv.astype(F32)
-            swapped = pltpu.roll(kv, 64, 1)
-            keys[ext, :] = jnp.where(low, kv, swapped).astype(BF16)
-            vals[ext, :] = jnp.where(low, swapped, kv).astype(BF16)
-            return carry
-
-        fill(3, 0)
-        halo = halo_copy(0, kvext.at[pl.ds(GROUP, WINDOW), :], kvext.at[pl.ds(0, WINDOW), :])
-        halo.start()
-        lax.fori_loop(0, 3, fill, 0)
-
-        low_w = low[:WINDOW, :]
-        zero = jnp.zeros((WINDOW, 128), BF16)
-        second = lax.broadcasted_iota(jnp.int32, (2 * WINDOW, 1), 0) >= WINDOW
-        sink_a = jnp.where(y == 0, sink_ref[0:1, 0:1], sink_ref[0:1, 2:3])
-        sink_b = jnp.where(y == 0, sink_ref[0:1, 1:2], sink_ref[0:1, 3:4])
-        sink = jnp.where(second, sink_b, sink_a)
-        row_i = lax.rem(lax.broadcasted_iota(jnp.int32, (2 * WINDOW, 2 * WINDOW), 0), WINDOW)
-        col_j = lax.broadcasted_iota(jnp.int32, (2 * WINDOW, 2 * WINDOW), 1)
-        distance = row_i + WINDOW - col_j
-        near = (distance >= 0) & (distance < WINDOW)
-
-        def attend(b):
-            at = al(b * WINDOW, WINDOW)
-            q = qbuf[pl.ds(at, WINDOW), :]
-            stacked = jnp.concatenate([jnp.where(low_w, q, zero), jnp.where(low_w, zero, q)], axis=0)
-            scores = lax.dot_general(
-                stacked,
-                keys[pl.ds(at, 2 * WINDOW), :],
-                (((1,), (1,)), ((), ())),
-                preferred_element_type=F32,
-            )
-            key_pos = z * GROUP + (b - 1) * WINDOW + col_j
-            scores = jnp.where(near & (key_pos >= 0), scores * 0.125, -1e30)
-            top = jnp.maximum(jnp.max(scores, axis=1, keepdims=True), sink)
-            e = jnp.exp(scores - top)
-            denom = jnp.sum(e, axis=1, keepdims=True) + jnp.exp(sink - top)
-            probs = (e / denom).astype(BF16)
-            att = jnp.dot(probs, vals[pl.ds(at, 2 * WINDOW), :], preferred_element_type=F32)
-            mx[pl.ds(at, WINDOW), :] = jnp.where(low_w, att[:WINDOW, :], att[WINDOW:, :]).astype(BF16)
-
-        def attend_pair(i, carry):
-            attend(2 * i + 2)
-            attend(2 * i + 1)
-            return carry
-
-        lax.fori_loop(0, 3, attend_pair, 0)
-        attend(7)
-        halo.wait_recv()
-        edge = kvext[0:WINDOW, :].astype(F32)
-        swapped = pltpu.roll(edge, 64, 1)
-        keys[0:WINDOW, :] = jnp.where(low_w, edge, swapped).astype(BF16)
-        vals[0:WINDOW, :] = jnp.where(low_w, swapped, edge).astype(BF16)
-        attend(0)
-        halo.wait_send()
-
-    def convolution():
-        def gate_rows(b, carry):
-            rows = pl.ds(al(b * ROWS, ROWS), ROWS)
-            g = acc[rows, 0:128] * (1.0 / (1.0 + jnp.exp(-acc[rows, 128:256])))
-            gext[pl.ds(al(b * ROWS + 32, 32), ROWS), :] = g.astype(BF16).astype(F32)
-            return carry
-
-        gate_rows(3, 0)
-        gtail[...] = gext[GROUP : GROUP + 32, :].astype(BF16)
-        halo = halo_copy(1, gtail, ghalo)
-        halo.start()
-        lax.fori_loop(0, 3, gate_rows, 0)
-
-        def filter_rows(r):
-            f = jnp.zeros((64, 128), F32)
-            for k in range(KSIZE):
-                f = f + taps[k : k + 1, :] * gext[r + 2 + k : r + 66 + k, :]
-            mx[r : r + 64, :] = f.astype(BF16)
-
-        for r in range(64, GROUP, 64):
-            filter_rows(r)
-        halo.wait_recv()
-        gext[0:32, :] = jnp.where(z > 0, ghalo[...].astype(F32), 0.0)
-        filter_rows(0)
-
-        halo.wait_send()
-
-    pl.when(y < 2)(attention)
-    pl.when(y >= 2)(convolution)
-
-    def mix_ref(o, off, part, mine=True):
-        lo, n = part_of(part, ROWS)
-        yy = wrap(y, o)
-        cols = pl.ds(al(tp_at(off, mine) * 256 + lax.rem(yy, 2) * 128, 128), 128)
-        return mixall.at[yy // 2, pl.ds(lo, n), cols]
-
-    m_x = Ring(m_net, "mx", mix_ref, x_dev)
-    own_cols = pl.ds(al(t * 256 + lax.rem(y, 2) * 128, 128), 128)
-    mixall[y // 2, :, own_cols] = mx[pl.ds(al(y * ROWS, ROWS), ROWS), :]
-
-    def m_rows(o, part):
-        lo, n = part_of(part, ROWS)
-        return mx.at[pl.ds(al(wrap(y, o) * ROWS + lo, 128), n), :]
-
-    for d in (1, -1):
-        m_net.send("tr", m_rows(2, side(d)), mtransit.at[(1 - d) // 2], y_dev(d))
-    for name, parts in (("m_a", ("lo", "hi")), ("m_b", ("hi", "lo"))):
-        for d, part in zip((1, -1), parts):
-            m_net.send(name, m_rows(d, part), mix_ref(0, 0, part), y_dev(d))
-    m_x.first(OWN_A, OWN_B)
-    m_x.give(OWN0)
-    m_net.wait("tr")
-    for d in (1, -1):
-        m_net.send("trf", mtransit.at[(1 - d) // 2], mix_ref(-d, 0, side(d)), y_dev(d))
+    by_role(filter_late, attend_late)
+    m_send("m_far", 2, "full")
+    m_send("m_b", -1, "lo")
+    m_send("m_b", 1, "hi")
     m_net.wait("m_a")
     m_x.first(SIDES_A)
-    m_net.wait("m_b")
-    m_x.first(SIDES_B)
-    m_x.give(SIDES0)
+    m_x.first_wait(OWN_A)
+    m_x.second(OWN_F)
+    m_x.first_wait(OWN_B)
+    m_x.give(OWN1)
     o_second[0].first_wait(SIDES_A)
     o_second[0].second(SIDES_AF)
     o_second[1].first_wait(SIDES_A)
     o_second[1].second(SIDES_AF)
-    m_x.first_wait(OWN_A)
-    m_x.second(OWN_F)
-    m_x.first_wait(OWN_B)
-    m_x.give(OWN1)
-    m_net.wait("trf")
-    m_x.first(FAR)
-    m_x.give(FAR0)
     o_second[0].first_wait(SIDES_B)
     o_second[0].second(SIDES_BF)
     o_second[1].first_wait(SIDES_B)
     o_second[1].second(SIDES_BF)
+    m_net.wait("m_b")
+    m_x.first(SIDES_B)
+    m_x.give(SIDES0)
+    m_net.wait("m_far")
+    m_net.send("m_far_x", mix_ref(2, 0, "full"), mix_ref(2, 0, "full"), x_dev(2))
+    m_x.first(FAR)
+    m_x.give(FAR0)
+    m_x.second_wait(OWN_F)
+    m_x.give(OWN2)
     m_x.first_wait(SIDES_A)
     m_x.second(SIDES_AF)
+    o_second[1].first_wait(FAR)
+    o_second[1].second(FAR_F)
     m_x.first_wait(SIDES_B)
     m_x.second(SIDES_BF)
     m_x.give(SIDES1)
-    m_x.second_wait(OWN_F)
-    m_x.give(OWN2)
-    o_second[1].first_wait(FAR)
-    o_second[1].second(FAR_F)
-    m_x.first_wait(FAR)
-    m_x.second(FAR_F)
-    m_x.give(FAR1)
     o_second[0].first_wait(FAR)
     o_second[0].second(FAR_F)
-    m_x.second_wait(SIDES_AF, SIDES_BF)
-    m_x.give(SIDES2)
+    m_x.first_wait(FAR)
+    m_x.give(FAR1)
+    m_net.wait("m_far_x")
+    m_x.give(FAR2)
     g_net.wait("gain")
     for i in range(8):
         gfull[:, i * 256 : (i + 1) * 256] = gall[i, 0:1, :]
-    m_x.second_wait(FAR_F)
-    m_x.give(FAR2)
+    m_x.second_wait(SIDES_AF, SIDES_BF)
+    m_x.give(SIDES2)
     m_x.give_wait(OWN0, OWN1, OWN2, SIDES0, SIDES1, SIDES2, FAR0, FAR1, FAR2)
 
     def channel_norm(i, carry):
-        rows = pl.ds(al(i * 16, 16), 16)
-        f = mixall[1, rows, :].astype(F32)
+        rows = pl.ds(al(i * 32, 32), 32)
+        f = mixall[0, rows, :].astype(F32)
         mean_value = jnp.sum(f, axis=1, keepdims=True) * (1.0 / CONV)
         variance = jnp.sum(f * f, axis=1, keepdims=True) * (1.0 / CONV) - mean_value * mean_value
         scaled = (f - mean_value) * lax.rsqrt(variance + 1e-05) * gfull[...]
-        convn[rows, :] = (scaled / (1.0 + jnp.exp(-scaled))).astype(BF16)
+        convn[rows, :] = (scaled * (0.5 + 0.5 * jnp.tanh(0.5 * scaled))).astype(BF16)
         return carry
 
-    lax.fori_loop(0, ROWS // 16, channel_norm, 0)
+    lax.fori_loop(0, ROWS // 32, channel_norm, 0)
     for ring in o_second:
         ring.second_wait(OWN_F, SIDES_AF, SIDES_BF, FAR_F)
 
     for c in range(0, OUTW, 256):
         w_attn = wo[:, 0:128, c : c + 256].reshape(2048, 256)
         w_conv = wo[:, 128:256, c : c + 256].reshape(2048, 256)
-        v = jnp.dot(mixall[0], w_attn, preferred_element_type=F32)
+        v = jnp.dot(mixall[1], w_attn, preferred_element_type=F32)
         v = v + jnp.dot(convn[...], w_conv, preferred_element_type=F32)
         out_ref[:, c : c + 256] = v.astype(BF16)
 
@@ -669,6 +709,8 @@
             pltpu.VMEM((D, WIDTH), BF16),
             pltpu.VMEM((16, ROWS, OUTW), BF16),
             pltpu.VMEM((ROWS, D), BF16),
+            pltpu.VMEM((8, GROUP, XCOLS), BF16),
+            pltpu.VMEM((2, GROUP, DCOLS), BF16),
             pltpu.VMEM((GROUP, D), BF16),
             pltpu.VMEM((GROUP, WIDTH), F32),
             pltpu.VMEM((GROUP, 128), BF16),
@@ -689,7 +731,6 @@
             pltpu.VMEM((4, 1, 256), F32),
             pltpu.VMEM((KSIZE, 128), F32),
             pltpu.VMEM((GROUP, 128), BF16),
-            pltpu.VMEM((2, 128, 128), BF16),
             pltpu.VMEM((2, ROWS, 2048), BF16),
             pltpu.VMEM((ROWS, 2048), BF16),
             dma((17,)),
@@ -703,8 +744,8 @@
             dma((SEMS,)),
             dma((1,)),
             dma((1,)),
-            dma((2,)),
-            dma((2,)),
+            dma((1,)),
+            dma((1,)),
         ],
         compiler_params=pltpu.CompilerParams(
             collective_id=0, has_side_effects=True, vmem_limit_bytes=67043328

time: 73.4 us -> 69 us (0.940)
  Pallas kernels: 71.5 us -> 67.2 us
    pallas_call x1, Pallas kernels: 71.5 us -> 67.2 us  [per_device(): pl.pallas_call(kernel, name='mixer_layer', out_shape=jax.ShapeDtypeStruct...]
where the time goes in v6:
time: 69 us; the launch traced here: 68.9 us
  Pallas kernels  67.2 us (97%)
  local copies, waits for them, and re-layouts  1.67 us (2%)
    pallas_call x1, Pallas kernels, per_device(): pl.pallas_call(kernel, name='mixer_layer', out_shape=jax.ShapeDtypeStruct...  67.2 us
    unnamed x1, local copies, waits for them, and re-layouts  1.67 us

profile of v6, /device:TPU:1, one launch (start us, length us, event | category | flops | bytes accessed | tf_op | source)
XLA Modules:
  0.0 68.9 jit_solution(1211861866121667584)
XLA Ops:
  0.0 67.2 %mixer_layer.1 = bf16[256,512]{1,0:T(8,128)(2,1)} custom-call(bf16[256,4096]{1,0:T(8,128)(2,1)} %tokens_hbm.1, f32[1,4096]{1,0:T(1,128)} %bitcast.7, bf16[256,256]{1,0:T(8,128)(2,1)} %wq_hbm.1, bf16[64,256]{1,0:T(8,128)(2,1)} %bitcast.5, bf16[64,256]{1,0:T(8,128)(2,1)} %bitcast.6, bf16[256,256]{1,0:T(8,128)(2,1)} %wglu_hbm.1, bf16[256,256]{1,0:T(8,128)(2,1)} %wgate_hbm.1, ...), custom_call_target="tpu_custom_call" | custom-call | tf_op jit(solution)/shard_map/mixer_layer/pallas_call | solution.py:700
  67.2 1.7 %copy.16 = bf16[256,512]{1,0:T(8,128)(2,1)} copy(bf16[256,512]{1,0:T(8,128)(2,1)} %mixer_layer.1) | data formatting | bytes 524288

commit v7 on v6

--- a/solution.py
+++ b/solution.py
@@ -331,10 +331,12 @@
             w_net.send(name, src, win_ref(0, 0, part), y_dev(d))
 
     tx_y.first(OWN_A)
+    w_first("w_a", ("lo", "hi"))
+    tx_y.first(OWN_B)
+    w_first("w_b", ("hi", "lo"))
     for d in (1, -1):
         lo, n = part_of(side(d), ROWS)
         w_net.send("tr", wst.at[wrap(y, 2), pl.ds(lo, n), :], transit.at[(1 - d) // 2], y_dev(d))
-    tx_y.first(OWN_B)
     for name, sends in (("wz_a", OWN_A), ("wz_b", OWN_B)):
         for o, part, d in sends:
             lo, n = part_of(part, ROWS)
@@ -342,68 +344,63 @@
     win[pl.ds(al(s * ROWS, ROWS), ROWS), :] = wst[y]
     loaded("oa", "oc")
     o_first[1].first(OWN_A, OWN_B)
-    o_second[0].first(OWN_A, OWN_B)
 
     tx_y.first_wait(OWN_A)
     tx_y.second(OWN_F)
     tx_x.first(SIDES_A)
-    w_first("w_a", ("lo", "hi"))
-    w_first("w_b", ("hi", "lo"))
+    w_net.wait("w_a")
+    w_z.first(SIDES_A)
+    tx_y.first_wait(OWN_B)
+    tx_x.first(SIDES_B)
+    tx_x.give(SIDES0)
+    w_net.wait("w_b")
+    w_z.first(SIDES_B)
+    w_net.wait("wz_a")
+    w_z.second(OWN_F)
+    o_second[0].first(OWN_A, OWN_B)
     w_net.wait("tr")
     for d in (1, -1):
         w_net.send("trf", transit.at[(1 - d) // 2], win_ref(-d, 0, side(d)), y_dev(d))
     td_y.first(OWN_A, OWN_B)
-    tx_y.first_wait(OWN_B)
-    tx_x.first(SIDES_B)
-    tx_x.give(SIDES0)
-    loaded("taps", "cgain", "sink", "inner", "outer")
-    taps[...] = taps_ref[...].astype(F32)
-    gall[t] = jnp.broadcast_to(cgain_ref[...], (8, 256))
-    w_net.wait("wz_a")
-    w_z.second(OWN_F)
     tx_y.second_wait(OWN_F)
+    tx_x.first(FAR)
+    tx_x.give(FAR0)
     tx_x.first_wait(SIDES_A)
     tx_x.second(SIDES_AF)
-    tx_x.first(FAR)
-    tx_x.give(FAR0)
-    w_net.wait("w_a")
-    w_z.first(SIDES_A)
-    w_net.wait("w_b")
-    w_z.first(SIDES_B)
     w_net.wait("trf")
     w_z.first(FAR)
+    w_z.first_wait(SIDES_A)
+    w_z.second(SIDES_AF)
+    w_z.first_wait(SIDES_B)
+    w_z.second(SIDES_BF)
     tx_x.first_wait(SIDES_B)
     tx_x.second(SIDES_BF)
     tx_x.give(SIDES1)
     w_net.wait("wz_b")
+    loaded("taps", "cgain", "sink", "inner", "outer")
+    taps[...] = taps_ref[...].astype(F32)
+    gall[t] = jnp.broadcast_to(cgain_ref[...], (8, 256))
     td_y.first_wait(OWN_A)
     td_y.second(OWN_F)
     o_first[0].first(OWN_A, OWN_B)
-    w_z.first_wait(SIDES_A)
-    w_z.second(SIDES_AF)
-    o_first[1].first_wait(OWN_A)
-    o_first[1].second(OWN_F)
-    w_z.first_wait(SIDES_B)
-    w_z.second(SIDES_BF)
+    w_z.first_wait(FAR)
+    w_z.second(FAR_F)
     tx_x.first_wait(FAR)
     tx_x.second(FAR_F)
     tx_x.give(FAR1)
     td_y.first_wait(OWN_B)
     td_p.give(SIDES0)
+    o_first[1].first_wait(OWN_A)
+    o_first[1].second(OWN_F)
     o_first[1].first_wait(OWN_B)
     o_second[1].first(OWN_A, OWN_B, SIDES_A, SIDES_B)
-    w_z.first_wait(FAR)
-    w_z.second(FAR_F)
     o_second[0].first_wait(OWN_A)
     o_second[0].second(OWN_F)
     o_second[0].first_wait(OWN_B)
+    td_y.second_wait(OWN_F)
+    td_p.give(FAR0)
     tx_x.second_wait(SIDES_AF, SIDES_BF)
     tx_x.give(SIDES2)
-    td_y.second_wait(OWN_F)
-    td_p.give(FAR0)
-    o_first[0].first_wait(OWN_A)
-    o_first[0].second(OWN_F)
-    o_second[0].first(SIDES_A)
 
     def project(o):
         rows = pl.ds(al(wrap(y, o) * ROWS, ROWS), ROWS)
@@ -433,8 +430,8 @@
         return v * cosine + other * sine
 
     def fill(b):
-        rows = slice(b * ROWS, (b + 1) * ROWS)
-        ext = slice(b * ROWS + WINDOW, (b + 1) * ROWS + WINDOW)
+        rows = pl.ds(al(b * ROWS, ROWS), ROWS)
+        ext = pl.ds(al(b * ROWS + WINDOW, WINDOW), ROWS)
         edge = outer[b]
         co, so = edge[:, 0:128], edge[:, 128:256]
         cosine = co * inner[:, 0:128] - so * inner[:, 128:256]
@@ -450,22 +447,23 @@
         keys[ext, :] = jnp.where(low, kv, swapped).astype(BF16)
         vals[ext, :] = jnp.where(low, swapped, kv).astype(BF16)
 
-    def attend(role, b):
+    def attend(b):
         zero = jnp.zeros((WINDOW, 128), BF16)
         second = lax.broadcasted_iota(jnp.int32, (2 * WINDOW, 1), 0) >= WINDOW
-        i = 2 * (role - 2)
-        sink = jnp.where(second, sink_ref[0:1, i + 1 : i + 2], sink_ref[0:1, i : i + 1])
+        sink_a = jnp.where(y == 2, sink_ref[0:1, 0:1], sink_ref[0:1, 2:3])
+        sink_b = jnp.where(y == 2, sink_ref[0:1, 1:2], sink_ref[0:1, 3:4])
+        sink = jnp.where(second, sink_b, sink_a)
         row_i = lax.rem(lax.broadcasted_iota(jnp.int32, (2 * WINDOW, 2 * WINDOW), 0), WINDOW)
         col_j = lax.broadcasted_iota(jnp.int32, (2 * WINDOW, 2 * WINDOW), 1)
         distance = row_i + WINDOW - col_j
         near = (distance >= 0) & (distance < WINDOW)
-        if b == 0:
-            near = near & (z * GROUP - WINDOW + col_j >= 0)
-        q = qbuf[b * WINDOW : (b + 1) * WINDOW, :]
+        near = near & (z * GROUP + (b - 1) * WINDOW + col_j >= 0)
+        at = al(b * WINDOW, WINDOW)
+        q = qbuf[pl.ds(at, WINDOW), :]
         stacked = jnp.concatenate([jnp.where(low_w, q, zero), jnp.where(low_w, zero, q)], axis=0)
         scores = lax.dot_general(
             stacked,
-            keys[b * WINDOW : (b + 2) * WINDOW, :],
+            keys[pl.ds(at, 2 * WINDOW), :],
             (((1,), (1,)), ((), ())),
             preferred_element_type=F32,
         )
@@ -474,44 +472,42 @@
         e = jnp.exp(scores - top)
         denom = jnp.sum(e, axis=1, keepdims=True) + jnp.exp(sink - top)
         probs = (e * (1.0 / denom)).astype(BF16)
-        att = jnp.dot(probs, vals[b * WINDOW : (b + 2) * WINDOW, :], preferred_element_type=F32)
-        mx[b * WINDOW : (b + 1) * WINDOW, :] = jnp.where(
-            low_w, att[:WINDOW, :], att[WINDOW:, :]
-        ).astype(BF16)
-
-    def late_windows(far):
-        return [(2 * far + i) % 8 for i in range(3)]
-
-    def attend_first(role):
+        att = jnp.dot(probs, vals[pl.ds(at, 2 * WINDOW), :], preferred_element_type=F32)
+        mx[pl.ds(at, WINDOW), :] = jnp.where(low_w, att[:WINDOW, :], att[WINDOW:, :]).astype(BF16)
+
+    def take_halo():
         kv_halo.wait_recv()
         edge = kvext[0:WINDOW, :].astype(F32)
         swapped = pltpu.roll(edge, 64, 1)
         keys[0:WINDOW, :] = jnp.where(low_w, edge, swapped).astype(BF16)
         vals[0:WINDOW, :] = jnp.where(low_w, swapped, edge).astype(BF16)
-        attend(role, 0)
         kv_halo.wait_send()
 
-    def attend_early(role):
-        far = (role + 2) % 4
+    def attend_early():
         fill(3)
         kv_halo.start()
-        for b in range(3):
-            if b != far:
-                fill(b)
-        for b in range(7, 0, -1):
-            if b not in late_windows(far):
-                attend(role, b)
-        if 0 not in late_windows(far):
-            attend_first(role)
-
-    def attend_late(role):
-        far = (role + 2) % 4
-        fill(far)
-        for b in range(7, 0, -1):
-            if b in late_windows(far):
-                attend(role, b)
-        if 0 in late_windows(far):
-            attend_first(role)
+
+        def fill_others(i, carry):
+            fill(jnp.where(i == 0, 3 - y, 0) + 2 * i)
+            return carry
+
+        lax.fori_loop(0, 2, fill_others, 0)
+
+        def pair(i, carry):
+            attend(jnp.where(y == 2, 3 + 2 * i, 1 + 5 * i))
+            attend(jnp.where(y == 2, 4 + 2 * i, 5 + 2 * i))
+            return carry
+
+        lax.fori_loop(0, 2, pair, 0)
+        pl.when(y == 3)(take_halo)
+        attend(jnp.where(y == 2, 7, 0))
+
+    def attend_late():
+        fill(y - 2)
+        attend(y)
+        attend(jnp.where(y == 2, 1, 4))
+        pl.when(y == 2)(take_halo)
+        attend(jnp.where(y == 2, 0, 2))
 
     def gate_rows(b):
         rows = slice(b * ROWS, (b + 1) * ROWS)
@@ -562,8 +558,9 @@
             filter_first()
 
     def by_role(conv, attention):
-        for role in range(4):
-            pl.when(y == role)(lambda role=role: (conv if role < 2 else attention)(role))
+        for role in range(2):
+            pl.when(y == role)(lambda role=role: conv(role))
+        pl.when(y >= 2)(attention)
 
     def mix_ref(o, off, part, mine=True):
         lo, n = part_of(part, ROWS)
@@ -581,12 +578,15 @@
 
     w_z.second_wait(OWN_F, SIDES_AF, SIDES_BF, FAR_F)
     project(0)
+    o_first[0].first_wait(OWN_A)
+    o_first[0].second(OWN_F)
+    o_second[0].first(SIDES_A)
+    tx_x.second_wait(FAR_F)
+    tx_x.give(FAR2)
     tx_x.give_wait(SIDES0, SIDES1, SIDES2)
     td_p.give_wait(SIDES0)
     project(-1)
     project(1)
-    tx_x.second_wait(FAR_F)
-    tx_x.give(FAR2)
     o_first[0].first_wait(OWN_B)
     o_second[0].first(SIDES_B)
     by_role(filter_early, attend_early)
@@ -617,14 +617,11 @@
     m_x.second(OWN_F)
     m_x.first_wait(OWN_B)
     m_x.give(OWN1)
-    o_second[0].first_wait(SIDES_A)
-    o_second[0].second(SIDES_AF)
-    o_second[1].first_wait(SIDES_A)
-    o_second[1].second(SIDES_AF)
-    o_second[0].first_wait(SIDES_B)
-    o_second[0].second(SIDES_BF)
-    o_second[1].first_wait(SIDES_B)
-    o_second[1].second(SIDES_BF)
+    for ring in o_second:
+        ring.first_wait(SIDES_A)
+        ring.second(SIDES_AF)
+        ring.first_wait(SIDES_B)
+        ring.second(SIDES_BF)
     m_net.wait("m_b")
     m_x.first(SIDES_B)
     m_x.give(SIDES0)

time: 69 us -> 68.6 us (level)
  no operation moved by 1% of the time
where the time goes in v7:
time: 68.6 us; the launch traced here: 68.5 us
  Pallas kernels  66.8 us (97%)
  local copies, waits for them, and re-layouts  1.67 us (2%)
    pallas_call x1, Pallas kernels, per_device(): pl.pallas_call(kernel, name='mixer_layer', out_shape=jax.ShapeDtypeStruct...  66.8 us
    unnamed x1, local copies, waits for them, and re-layouts  1.67 us

profile of v7, /device:TPU:1, one launch (start us, length us, event | category | flops | bytes accessed | tf_op | source)
XLA Modules:
  0.0 68.5 jit_solution(655814153147414139)
XLA Ops:
  0.0 66.8 %mixer_layer.1 = bf16[256,512]{1,0:T(8,128)(2,1)} custom-call(bf16[256,4096]{1,0:T(8,128)(2,1)} %tokens_hbm.1, f32[1,4096]{1,0:T(1,128)} %bitcast.7, bf16[256,256]{1,0:T(8,128)(2,1)} %wq_hbm.1, bf16[64,256]{1,0:T(8,128)(2,1)} %bitcast.5, bf16[64,256]{1,0:T(8,128)(2,1)} %bitcast.6, bf16[256,256]{1,0:T(8,128)(2,1)} %wglu_hbm.1, bf16[256,256]{1,0:T(8,128)(2,1)} %wgate_hbm.1, ...), custom_call_target="tpu_custom_call" | custom-call | tf_op jit(solution)/shard_map/mixer_layer/pallas_call | solution.py:697
  66.8 1.7 %copy.16 = bf16[256,512]{1,0:T(8,128)(2,1)} copy(bf16[256,512]{1,0:T(8,128)(2,1)} %mixer_layer.1) | data formatting | bytes 524288

commit v8 on v7

--- a/solution.py
+++ b/solution.py
@@ -22,7 +22,7 @@
 XCOLS = 384
 DCOLS = 512
 OUT_SPLIT = 160
-SEMS = 26
+SEMS = {"w": 10, "t": 13, "o": 17, "m": 14}
 
 
 def rope_tables():
@@ -39,10 +39,17 @@
     def __init__(self, send_sem, recv_sem, meter, partner):
         self.send_sem, self.recv_sem, self.meter, self.partner = send_sem, recv_sem, meter, partner
         self.index, self.size, self.total = {}, {}, 0
+        self.joined, self.done = {}, set()
+
+    def join(self, name, *groups):
+        for group in groups:
+            self.joined[group] = name
 
     def send(self, group, src, dst, device):
+        group = self.joined.get(group, group)
+        assert group not in self.done
         k = self.index.setdefault(group, len(self.index))
-        assert k < SEMS
+        assert k < self.recv_sem.shape[0]
         count = src.dtype.itemsize
         for n in src.shape:
             count *= n
@@ -66,6 +73,10 @@
         pltpu.make_async_copy(counted, counted, sem).wait()
 
     def wait(self, group):
+        group = self.joined.get(group, group)
+        if group in self.done:
+            return
+        self.done.add(group)
         self.await_bytes(self.recv_sem.at[self.index[group]], self.size[group])
 
     def drain(self):
@@ -120,6 +131,8 @@
 SIDES_A = both((-1, "lo"), (1, "hi"))
 SIDES_B = both((-1, "hi"), (1, "lo"))
 FAR = both((2, "lo"), (2, "hi"))
+FAR_HI, FAR_LO = both((2, "hi")), both((2, "lo"))
+FAR_HF = ((2, -1),)
 OWN_F = ((0, 1), (0, -1))
 SIDES_AF = ((-1, 1), (1, -1))
 SIDES_BF = ((-1, -1), (1, 1))
@@ -330,6 +343,21 @@
             src = wst.at[wrap(y, d), pl.ds(lo, n), :]
             w_net.send(name, src, win_ref(0, 0, part), y_dev(d))
 
+    for items in (SIDES0, SIDES1, SIDES2):
+        t_net.join("sides", ("txx", "P", items), ("tdp", "P", items))
+        m_net.join("give", ("mx", "P", items))
+    for items in (FAR0, FAR1, FAR2):
+        t_net.join("far", ("txx", "P", items), ("tdp", "P", items))
+        m_net.join("give", ("mx", "P", items))
+    for items in (OWN0, OWN1, OWN2):
+        m_net.join("give", ("mx", "P", items))
+    for sends in (OWN_F, SIDES_AF, SIDES_BF, FAR_F):
+        w_net.join("second", ("wz", "F", sends))
+        o_net.join("second", (("os", 0), "F", sends), (("os", 1), "F", sends))
+    for sends in (SIDES_AF, SIDES_BF):
+        t_net.join("second", ("txx", "F", sends))
+        m_net.join("second", ("mx", "F", sends))
+
     tx_y.first(OWN_A)
     w_first("w_a", ("lo", "hi"))
     tx_y.first(OWN_B)
@@ -617,18 +645,18 @@
     m_x.second(OWN_F)
     m_x.first_wait(OWN_B)
     m_x.give(OWN1)
+    m_net.wait("m_b")
+    m_x.first(SIDES_B)
+    m_x.give(SIDES0)
+    m_net.wait("m_far")
+    m_x.first(FAR_HI, FAR_LO)
+    m_net.send("m_far_x", mix_ref(2, 0, "lo"), mix_ref(2, 0, "lo"), x_dev(2))
+    m_x.give(FAR0)
     for ring in o_second:
         ring.first_wait(SIDES_A)
         ring.second(SIDES_AF)
         ring.first_wait(SIDES_B)
         ring.second(SIDES_BF)
-    m_net.wait("m_b")
-    m_x.first(SIDES_B)
-    m_x.give(SIDES0)
-    m_net.wait("m_far")
-    m_net.send("m_far_x", mix_ref(2, 0, "full"), mix_ref(2, 0, "full"), x_dev(2))
-    m_x.first(FAR)
-    m_x.give(FAR0)
     m_x.second_wait(OWN_F)
     m_x.give(OWN2)
     m_x.first_wait(SIDES_A)
@@ -640,9 +668,12 @@
     m_x.give(SIDES1)
     o_second[0].first_wait(FAR)
     o_second[0].second(FAR_F)
-    m_x.first_wait(FAR)
+    m_x.first_wait(FAR_HI)
+    m_x.second(FAR_HF)
+    m_x.first_wait(FAR_LO)
     m_x.give(FAR1)
     m_net.wait("m_far_x")
+    m_x.second_wait(FAR_HF)
     m_x.give(FAR2)
     g_net.wait("gain")
     for i in range(8):
@@ -732,13 +763,13 @@
             pltpu.VMEM((ROWS, 2048), BF16),
             dma((17,)),
             dma((1,)),
-            dma((SEMS,)),
+            dma((SEMS["w"],)),
             dma((1,)),
-            dma((SEMS,)),
+            dma((SEMS["t"],)),
             dma((1,)),
-            dma((SEMS,)),
+            dma((SEMS["o"],)),
             dma((1,)),
-            dma((SEMS,)),
+            dma((SEMS["m"],)),
             dma((1,)),
             dma((1,)),
             dma((1,)),

time: 68.6 us -> 67.6 us (0.985)
  Pallas kernels: 66.8 us -> 65.7 us
    pallas_call x1, Pallas kernels: 66.8 us -> 65.7 us  [per_device(): pl.pallas_call(kernel, name='mixer_layer', out_shape=jax.ShapeDtypeStruct...]
where the time goes in v8:
time: 67.6 us; the launch traced here: 67.4 us
  Pallas kernels  65.7 us (97%)
  local copies, waits for them, and re-layouts  1.67 us (2%)
    pallas_call x1, Pallas kernels, per_device(): pl.pallas_call(kernel, name='mixer_layer', out_shape=jax.ShapeDtypeStruct...  65.7 us
    unnamed x1, local copies, waits for them, and re-layouts  1.67 us

profile of v8, /device:TPU:1, one launch (start us, length us, event | category | flops | bytes accessed | tf_op | source)
XLA Modules:
  0.0 67.4 jit_solution(5447049989724970668)
XLA Ops:
  0.0 65.7 %mixer_layer.1 = bf16[256,512]{1,0:T(8,128)(2,1)} custom-call(bf16[256,4096]{1,0:T(8,128)(2,1)} %tokens_hbm.1, f32[1,4096]{1,0:T(1,128)} %bitcast.7, bf16[256,256]{1,0:T(8,128)(2,1)} %wq_hbm.1, bf16[64,256]{1,0:T(8,128)(2,1)} %bitcast.5, bf16[64,256]{1,0:T(8,128)(2,1)} %bitcast.6, bf16[256,256]{1,0:T(8,128)(2,1)} %wglu_hbm.1, bf16[256,256]{1,0:T(8,128)(2,1)} %wgate_hbm.1, ...), custom_call_target="tpu_custom_call" | custom-call | tf_op jit(solution)/shard_map/mixer_layer/pallas_call | solution.py:728
  65.7 1.7 %copy.16 = bf16[256,512]{1,0:T(8,128)(2,1)} copy(bf16[256,512]{1,0:T(8,128)(2,1)} %mixer_layer.1) | data formatting | bytes 524288

commit v9 on v8

--- a/solution.py
+++ b/solution.py
@@ -22,7 +22,7 @@
 XCOLS = 384
 DCOLS = 512
 OUT_SPLIT = 160
-SEMS = {"w": 10, "t": 13, "o": 17, "m": 14}
+SEMS = {"w": 10, "t": 13, "o": 17, "m": 15}
 
 
 def rope_tables():
@@ -133,6 +133,9 @@
 FAR = both((2, "lo"), (2, "hi"))
 FAR_HI, FAR_LO = both((2, "hi")), both((2, "lo"))
 FAR_HF = ((2, -1),)
+SOON = both((-1, "lo"), (1, "hi"), (-1, "hi"))
+SOON_F = ((-1, 1), (1, -1), (-1, -1))
+LATE, LATE_F = both((1, "lo")), ((1, 1),)
 OWN_F = ((0, 1), (0, -1))
 SIDES_AF = ((-1, 1), (1, -1))
 SIDES_BF = ((-1, -1), (1, 1))
@@ -354,9 +357,9 @@
     for sends in (OWN_F, SIDES_AF, SIDES_BF, FAR_F):
         w_net.join("second", ("wz", "F", sends))
         o_net.join("second", (("os", 0), "F", sends), (("os", 1), "F", sends))
+    m_net.join("second", ("mx", "F", SOON_F), ("mx", "F", LATE_F))
     for sends in (SIDES_AF, SIDES_BF):
         t_net.join("second", ("txx", "F", sends))
-        m_net.join("second", ("mx", "F", sends))
 
     tx_y.first(OWN_A)
     w_first("w_a", ("lo", "hi"))
@@ -620,6 +623,7 @@
     by_role(filter_early, attend_early)
     m_send("m_a", 1, "lo")
     m_send("m_a", -1, "hi")
+    m_send("m_a", 1, "hi")
     tx_x.give_wait(FAR0, FAR1, FAR2)
     td_p.give_wait(FAR0)
     project(2)
@@ -636,20 +640,22 @@
     for i in range(1, 8):
         g_net.send("gain", gall.at[t], gall.at[t], (s, lax.rem(t + i, 8)))
     by_role(filter_late, attend_late)
-    m_send("m_far", 2, "full")
+    m_send("m_far_hi", 2, "hi")
     m_send("m_b", -1, "lo")
-    m_send("m_b", 1, "hi")
+    m_send("m_far_lo", 2, "lo")
     m_net.wait("m_a")
-    m_x.first(SIDES_A)
+    m_x.first(SOON)
     m_x.first_wait(OWN_A)
     m_x.second(OWN_F)
     m_x.first_wait(OWN_B)
     m_x.give(OWN1)
     m_net.wait("m_b")
-    m_x.first(SIDES_B)
+    m_x.first(LATE)
     m_x.give(SIDES0)
-    m_net.wait("m_far")
-    m_x.first(FAR_HI, FAR_LO)
+    m_net.wait("m_far_hi")
+    m_x.first(FAR_HI)
+    m_net.wait("m_far_lo")
+    m_x.first(FAR_LO)
     m_net.send("m_far_x", mix_ref(2, 0, "lo"), mix_ref(2, 0, "lo"), x_dev(2))
     m_x.give(FAR0)
     for ring in o_second:
@@ -659,27 +665,27 @@
         ring.second(SIDES_BF)
     m_x.second_wait(OWN_F)
     m_x.give(OWN2)
-    m_x.first_wait(SIDES_A)
-    m_x.second(SIDES_AF)
+    m_x.first_wait(SOON)
+    m_x.second(SOON_F)
+    m_x.first_wait(LATE)
+    m_x.second(LATE_F)
+    m_x.give(SIDES1)
+    m_x.first_wait(FAR_HI)
+    m_x.second(FAR_HF)
     o_second[1].first_wait(FAR)
     o_second[1].second(FAR_F)
-    m_x.first_wait(SIDES_B)
-    m_x.second(SIDES_BF)
-    m_x.give(SIDES1)
     o_second[0].first_wait(FAR)
     o_second[0].second(FAR_F)
-    m_x.first_wait(FAR_HI)
-    m_x.second(FAR_HF)
     m_x.first_wait(FAR_LO)
     m_x.give(FAR1)
+    g_net.wait("gain")
+    for i in range(8):
+        gfull[:, i * 256 : (i + 1) * 256] = gall[i, 0:1, :]
+    m_x.second_wait(SOON_F, LATE_F)
+    m_x.give(SIDES2)
     m_net.wait("m_far_x")
     m_x.second_wait(FAR_HF)
     m_x.give(FAR2)
-    g_net.wait("gain")
-    for i in range(8):
-        gfull[:, i * 256 : (i + 1) * 256] = gall[i, 0:1, :]
-    m_x.second_wait(SIDES_AF, SIDES_BF)
-    m_x.give(SIDES2)
     m_x.give_wait(OWN0, OWN1, OWN2, SIDES0, SIDES1, SIDES2, FAR0, FAR1, FAR2)
 
     def channel_norm(i, carry):

time: 67.6 us -> 66.8 us (0.988)
  Pallas kernels: 65.7 us -> 65 us
    pallas_call x1, Pallas kernels: 65.7 us -> 65 us  [per_device(): pl.pallas_call(kernel, name='mixer_layer', out_shape=jax.ShapeDtypeStruct...]
where the time goes in v9:
time: 66.8 us; the launch traced here: 66.7 us
  Pallas kernels  65 us (97%)
  local copies, waits for them, and re-layouts  1.67 us (2%)
    pallas_call x1, Pallas kernels, per_device(): pl.pallas_call(kernel, name='mixer_layer', out_shape=jax.ShapeDtypeStruct...  65 us
    unnamed x1, local copies, waits for them, and re-layouts  1.67 us

profile of v9, /device:TPU:1, one launch (start us, length us, event | category | flops | bytes accessed | tf_op | source)
XLA Modules:
  0.0 66.7 jit_solution(13956318775463892328)
XLA Ops:
  0.0 65.0 %mixer_layer.1 = bf16[256,512]{1,0:T(8,128)(2,1)} custom-call(bf16[256,4096]{1,0:T(8,128)(2,1)} %tokens_hbm.1, f32[1,4096]{1,0:T(1,128)} %bitcast.7, bf16[256,256]{1,0:T(8,128)(2,1)} %wq_hbm.1, bf16[64,256]{1,0:T(8,128)(2,1)} %bitcast.5, bf16[64,256]{1,0:T(8,128)(2,1)} %bitcast.6, bf16[256,256]{1,0:T(8,128)(2,1)} %wglu_hbm.1, bf16[256,256]{1,0:T(8,128)(2,1)} %wgate_hbm.1, ...), custom_call_target="tpu_custom_call" | custom-call | tf_op jit(solution)/shard_map/mixer_layer/pallas_call | solution.py:734
  65.0 1.7 %copy.16 = bf16[256,512]{1,0:T(8,128)(2,1)} copy(bf16[256,512]{1,0:T(8,128)(2,1)} %mixer_layer.1) | data formatting | bytes 524288

commit v10 on v9

--- a/solution.py
+++ b/solution.py
@@ -635,14 +635,14 @@
     o_second[1].first_wait(OWN_A)
     o_second[1].second(OWN_F)
     o_second[1].first_wait(OWN_B)
-    o_first[0].second_wait(OWN_F)
-    o_second[0].first(FAR)
     for i in range(1, 8):
         g_net.send("gain", gall.at[t], gall.at[t], (s, lax.rem(t + i, 8)))
     by_role(filter_late, attend_late)
     m_send("m_far_hi", 2, "hi")
     m_send("m_b", -1, "lo")
     m_send("m_far_lo", 2, "lo")
+    o_first[0].second_wait(OWN_F)
+    o_second[0].first(FAR)
     m_net.wait("m_a")
     m_x.first(SOON)
     m_x.first_wait(OWN_A)

time: 66.8 us -> 66.3 us (level)
  no operation moved by 1% of the time
where the time goes in v10:
time: 66.3 us; the launch traced here: 66.1 us
  Pallas kernels  64.5 us (97%)
  local copies, waits for them, and re-layouts  1.67 us (3%)
    pallas_call x1, Pallas kernels, per_device(): pl.pallas_call(kernel, name='mixer_layer', out_shape=jax.ShapeDtypeStruct...  64.5 us
    unnamed x1, local copies, waits for them, and re-layouts  1.67 us

profile of v10, /device:TPU:1, one launch (start us, length us, event | category | flops | bytes accessed | tf_op | source)
XLA Modules:
  0.0 66.1 jit_solution(4218765297049576416)
XLA Ops:
  0.0 64.5 %mixer_layer.1 = bf16[256,512]{1,0:T(8,128)(2,1)} custom-call(bf16[256,4096]{1,0:T(8,128)(2,1)} %tokens_hbm.1, f32[1,4096]{1,0:T(1,128)} %bitcast.7, bf16[256,256]{1,0:T(8,128)(2,1)} %wq_hbm.1, bf16[64,256]{1,0:T(8,128)(2,1)} %bitcast.5, bf16[64,256]{1,0:T(8,128)(2,1)} %bitcast.6, bf16[256,256]{1,0:T(8,128)(2,1)} %wglu_hbm.1, bf16[256,256]{1,0:T(8,128)(2,1)} %wgate_hbm.1, ...), custom_call_target="tpu_custom_call" | custom-call | tf_op jit(solution)/shard_map/mixer_layer/pallas_call | solution.py:734
  64.5 1.7 %copy.16 = bf16[256,512]{1,0:T(8,128)(2,1)} copy(bf16[256,512]{1,0:T(8,128)(2,1)} %mixer_layer.1) | data formatting | bytes 524288
